TPU v7x, 256 devices: a whole 4x4x8 slice. The times are simulated.
256 devices in a mesh: sp: 32 (over z, x), tp: 8 (over y, core).
Axes of the slice: x: 4, y: 4, z: 8, core: 2. Of those that a mesh axis runs over, the one named last changes fastest.
Arguments:
- out_grad: bfloat16 [4096, 2048], P('sp', 'tp'), may hold values from -6 to 6
- moe_input: bfloat16 [4096, 2048], P('sp', 'tp'), may hold values from -6 to 6
- route_weight: float32 [4096, 2], P('sp'), may hold values from 0.2 to 1
- route_ids: int32 [4096, 2], P('sp'), may hold values from 0 to 31, all different within a row; in each aligned block of 128 rows (0 to 127, 128 to 255, ...) at most 16 rows name the same one
- gate_proj: bfloat16 [32, 2048, 2816], P('sp', None, 'tp'), may hold values from -0.125 to 0.125
- up_proj: bfloat16 [32, 2048, 2816], P('sp', None, 'tp'), may hold values from -0.125 to 0.125
- down_proj: bfloat16 [32, 2816, 2048], P('sp', 'tp'), may hold values from -0.109375 to 0.109375
- out_proj: bfloat16 [2048, 2048], P(None, 'tp'), may hold values from -0.125 to 0.125
- conv_out: bfloat16 [4096, 2048], P('sp', 'tp'), may hold values from -6 to 6
- gate_b: bfloat16 [4096, 2048], P('sp', 'tp'), may hold values from -6 to 6
- gate_c: bfloat16 [4096, 2048], P('sp', 'tp'), may hold values from -6 to 6
- value_v: bfloat16 [4096, 2048], P('sp', 'tp'), may hold values from -6 to 6
- conv_taps: float32 [3, 2048], P(None, 'tp'), may hold values from -3 to 3
Outputs:
- grad_gate: bfloat16 [32, 2048, 2816], P('sp', None, 'tp')
- grad_up: bfloat16 [32, 2048, 2816], P('sp', None, 'tp')
- grad_down: bfloat16 [32, 2816, 2048], P('sp', 'tp')
- grad_out: float32 [2048, 2048], P('sp', 'tp')
- grad_b: bfloat16 [4096, 2048], P('sp', 'tp')
- grad_c: bfloat16 [4096, 2048], P('sp', 'tp')
- grad_v: bfloat16 [4096, 2048], P('sp', 'tp')
Inputs may be any that keep to these rules, and one draw needn't show every extreme that they name: `route_ids`: each row names two different experts; within the 128 rows of one index of sp no expert is named by more than 16 rows, a bound that some block reaches.
All inputs are finite; a program needn't handle non-finite values.
Results may differ from a plain program's by a relative error of at most 0.019.
Values may be sent and summed in bfloat16 or wider, within the bound.
No kernel may reach another device: no remote copies, remote signals or barrier semaphores. Data moves between devices by JAX's collectives and lax.ppermute only.
A program may use at most 64 MiB of HBM per device.

v0:
```python
import jax
import jax.numpy as jnp
from jax import lax
from jax.experimental import pallas as pl
from jax.experimental.pallas import tpu as pltpu
from jax.sharding import Mesh
from jax.sharding import PartitionSpec as P

SP = ("z", "x")
TP = ("y", "c")
BF = jnp.bfloat16
F32 = jnp.float32

VMEM = pl.BlockSpec(memory_space=pltpu.VMEM)
SMEM = pl.BlockSpec(memory_space=pltpu.SMEM)
ANY = pl.BlockSpec(memory_space=pltpu.HBM)


def call(body, outs, n_smem, args, scratch=(), flops=0, hbm_outs=(), limit=8, hbm_args=(), any_args=(), kind=BF):
    args = [
        a if i < n_smem else pltpu.with_memory_space_constraint(a, pltpu.HBM if i in hbm_args or i in any_args else pltpu.VMEM)
        for i, a in enumerate(args)
    ]
    outs = [
        jax.ShapeDtypeStruct(shape, kind) if i in hbm_outs else pltpu.VMEM(shape, BF)
        for i, shape in enumerate(outs)
    ]
    return pl.pallas_call(
        body,
        out_shape=outs,
        in_specs=[SMEM if i < n_smem else ANY if i in any_args else VMEM for i in range(len(args))],
        out_specs=[VMEM] * len(outs),
        scratch_shapes=list(scratch),
        cost_estimate=pl.CostEstimate(flops=flops, bytes_accessed=0, transcendentals=0),
        compiler_params=pltpu.CompilerParams(vmem_limit_bytes=limit << 20),
    )(*args)


def nt(a, b):
    return lax.dot_general(a, b, (((1,), (1,)), ((), ())), preferred_element_type=F32)


def tn(a, b):
    return lax.dot_general(a, b, (((0,), (0,)), ((), ())), preferred_element_type=F32)


def nn(a, b):
    return jnp.dot(a, b, preferred_element_type=F32)


def shift(x, axis, n, k):
    return lax.ppermute(x, axis, [(i, (i + k) % n) for i in range(n)])


def dispatch_kernel(x_ref, og_ref, w_ref, ids_ref, send_ref, sel_ref):
    tok, ch = x_ref.shape
    n_exp, cap2, _ = send_ref.shape
    cap = cap2 // 2
    total = n_exp * cap
    up = (
        lax.broadcasted_iota(jnp.int32, (tok, tok), 0)
        < lax.broadcasted_iota(jnp.int32, (tok, tok), 1)
    ).astype(F32).astype(BF)
    expert = lax.broadcasted_iota(jnp.int32, (n_exp, tok), 0)
    ids = [ids_ref[k : k + 1, :] for k in range(2)]
    hot = [(i == expert).astype(F32) for i in ids]
    before = nn((hot[0] + hot[1]).astype(BF), up)
    slot_iota = lax.broadcasted_iota(jnp.int32, (total, tok), 0)
    lane = lax.broadcasted_iota(jnp.int32, (tok, tok), 1)
    place, sent, cols = [], [], []
    for k in range(2):
        slot = jnp.sum(before * hot[k], axis=0, keepdims=True)
        dest = ids[k].astype(F32) * cap + slot
        cols.append(jnp.broadcast_to(dest, (tok, tok)).T.astype(jnp.int32))
        place.append((slot_iota == dest.astype(jnp.int32)).astype(F32).astype(BF))
        weight = jnp.broadcast_to(w_ref[k : k + 1, :], (tok, tok)).T
        sent.append(
            jnp.concatenate(
                [(weight * og_ref[:, j : j + tok].astype(F32)).astype(BF) for j in range(0, ch, tok)], axis=1
            )
        )
    sx = nn(place[0] + place[1], x_ref[...]).astype(BF)
    sy = (nn(place[0], sent[0]) + nn(place[1], sent[1])).astype(BF)
    send_ref[:, :cap, :] = sx.reshape(n_exp, cap, ch)
    send_ref[:, cap:, :] = sy.reshape(n_exp, cap, ch)
    for j in range(total // tok):
        hit = (cols[0] == lane + j * tok) | (cols[1] == lane + j * tok)
        sel_ref[:, j * tok : (j + 1) * tok] = hit.astype(F32).astype(BF)


def mixed_kernel(b_ref, co_ref, mixed_ref):
    mixed_ref[...] = (b_ref[...].astype(F32) * co_ref[...].astype(F32)).astype(BF)


def load_kernel(gate_ref, up_ref, down_ref, w_ref, wd_ref, sems):
    width = wd_ref.shape[0]
    loads = [
        pltpu.make_async_copy(gate_ref, w_ref.at[pl.ds(0, width)], sems.at[0]),
        pltpu.make_async_copy(up_ref, w_ref.at[pl.ds(width, width)], sems.at[1]),
        pltpu.make_async_copy(down_ref, wd_ref, sems.at[2]),
    ]
    for load in loads:
        load.start()
    for load in loads:
        load.wait()


def expert_kernel(y_ref, c_ref, *refs):
    pieces, w_ref, wd_ref = refs[:16], refs[16], refs[17]
    theirs_ref, x_ref, dy_ref, hid_ref, dgu_ref, d_ref, gu_s, h_s = refs[18:]
    y, c = y_ref[0], c_ref[0]
    ch = pieces[0].shape[1]
    f = hid_ref.shape[0]
    for d in range(4):
        for other in range(2):
            o = channels(y, d, c if other == 0 else 1 - c, ch)
            x_ref[:, pl.ds(o, ch)] = pieces[4 * d + 2 * other][...]
            dy_ref[:, pl.ds(o, ch)] = pieces[4 * d + 2 * other + 1][...]
    gu_s[...] = nt(w_ref[...], x_ref[...])
    h_s[...] = nt(wd_ref[...], dy_ref[...])
    step = 32
    for r in range(0, f, step):
        g, u, dh = gu_s[r : r + step], gu_s[f + r : f + r + step], h_s[r : r + step]
        sig = jax.nn.sigmoid(g)
        act = g * sig
        hid_ref[r : r + step] = (act * u).astype(BF)
        dgu_ref[r : r + step] = (dh * u * (sig * (1.0 + g * (1.0 - sig)))).astype(BF)
        dgu_ref[f + r : f + r + step] = (dh * act).astype(BF)
    d_ref[...] = dgu_ref[...].T
    for d in range(4):
        o = channels(y, d, 1 - c, ch)
        theirs_ref[d] = nn(d_ref[...], w_ref[:, pl.ds(o, ch)]).astype(BF)


def channels(y, d, core, ch):
    return pl.multiple_of(ch * (2 * lax.rem(y + d, 4) + core), ch)


def own_half_kernel(y_ref, c_ref, d_ref, w_ref, mine_ref):
    y, c = y_ref[0], c_ref[0]
    ch = mine_ref.shape[2]
    for d in range(4):
        o = channels(y, d, c, ch)
        mine_ref[d] = nn(d_ref[...], w_ref[:, pl.ds(o, ch)]).astype(BF)


def pair_kernel(mine_ref, got_ref, *out_refs):
    for d in range(4):
        out_refs[d][...] = (mine_ref[d].astype(F32) + got_ref[d].astype(F32)).astype(BF)


def sum_kernel(*refs):
    total = refs[0][...].astype(F32)
    for ref in refs[1:-1]:
        total = total + ref[...].astype(F32)
    refs[-1][...] = total.astype(refs[-1].dtype)


def weights_kernel(x_ref, dy_ref, hid_ref, dgu_ref, gg_ref, gu_ref, gd_ref):
    f = hid_ref.shape[0]
    gg_ref[...] = nn(dgu_ref[:f], x_ref[...]).astype(BF)
    gu_ref[...] = nn(dgu_ref[f:], x_ref[...]).astype(BF)
    gd_ref[...] = nn(hid_ref[...], dy_ref[...]).astype(BF)


def combine_kernel(sel_ref, back_ref, og_ref, b_ref, dh_ref, first_ref, last_ref):
    dh = (og_ref[...].astype(F32) + nn(sel_ref[...], back_ref[...])).astype(BF)
    dh_ref[...] = dh
    tok = dh.shape[0]
    first_ref[0:1] = dh[:1]
    first_ref[1:2] = b_ref[0:1]
    last_ref[0:1] = dh[tok - 1 :]
    last_ref[1:2] = b_ref[tok - 1 :]


def stack_kernel(turned_ref, low_ref, high_ref, out_ref):
    tok, ch = turned_ref.shape
    out_ref[:tok] = turned_ref[...]
    row = lax.broadcasted_iota(jnp.int32, (16, ch), 0)
    low, high = low_ref[0:1].astype(F32), high_ref[0:1].astype(F32)
    out_ref[tok:] = jnp.where(row == 0, low, jnp.where(row == 1, high, 0.0)).astype(BF)


def mixer_kernel(
    y_ref, c_ref, own_ref, part_ref, edge_own_ref, edge_part_ref, w_ref, b_ref, co_ref, bl_ref, bh_ref, t_ref, v_ref, g_ref,
    gb_ref, gc_ref, gv_ref,
):
    y, c = y_ref[0], c_ref[0]
    tok, ch = b_ref.shape
    size = edge_own_ref.shape[0] // 4
    acc = jnp.zeros((size, ch), F32)
    for d in range(4):
        for ref, edge, core in ((own_ref, edge_own_ref, c), (part_ref, edge_part_ref, 1 - c)):
            rows = jnp.concatenate([ref[d * tok : (d + 1) * tok], edge[d * size + tok : (d + 1) * size]], axis=0)
            acc = acc + nn(rows, w_ref[pl.ds(channels(y, d, core, ch), ch), :])
    gb_ref[...] = (acc[:tok] * co_ref[...].astype(F32)).astype(BF)
    dc = (acc[:tok] * b_ref[...].astype(F32)).astype(BF).astype(F32)
    low = (acc[tok : tok + 1] * bl_ref[1:2].astype(F32)).astype(BF).astype(F32)
    high = (acc[tok + 1 : tok + 2] * bh_ref[1:2].astype(F32)).astype(BF).astype(F32)
    row = lax.broadcasted_iota(jnp.int32, dc.shape, 0)
    nxt = jnp.where(row == tok - 1, high, pltpu.roll(dc, tok - 1, 0))
    prv = jnp.where(row == 0, low, pltpu.roll(dc, 1, 0))
    du = t_ref[0:1, :] * nxt + t_ref[1:2, :] * dc + t_ref[2:3, :] * prv
    gc_ref[...] = (du * v_ref[...].astype(F32)).astype(BF)
    gv_ref[...] = (du * g_ref[...].astype(F32)).astype(BF)


def outer_kernel(y_ref, c_ref, z_ref, xi_ref, own_ref, part_ref, mix_ref, *refs):
    out_refs, (a_s, b_s, o_s) = refs[:4], refs[4:]
    y, c, z = y_ref[0], c_ref[0], z_ref[0]
    tok = mix_ref.shape[0] // 8
    size = own_ref.shape[0] // 4
    for d in range(4):
        for ref, core in ((own_ref, c), (part_ref, 1 - c)):
            a_s[pl.ds(channels(y, d, core, tok), tok), :] = ref[d * size : d * size + tok, :]
    for d, bits in enumerate((0, 4, 2, 6, 1, 5, 3, 7)):
        o = pl.multiple_of(tok * (z ^ bits), tok)
        b_s[pl.ds(o, tok), :] = mix_ref[d * tok : (d + 1) * tok, :]
    o_s[...] = tn(a_s[...], b_s[...])
    rows = out_refs[0].shape[0]
    for k, ref in enumerate(out_refs):
        ref[...] = o_s[pl.ds(pl.multiple_of(rows * lax.rem(xi_ref[0] + k, 4), rows), rows), :].astype(BF)


def over_tp(x):
    parts = [x] + [shift(x, "y", 4, 4 - k) for k in (1, 2, 3)]
    own = jnp.concatenate(parts, axis=0)
    return own, shift(own, "c", 2, 1)


def edges(first, last):
    n = lax.axis_size(SP)
    low = lax.ppermute(last, SP, [(i, i + 1) for i in range(n - 1)])
    high = lax.ppermute(first, SP, [(i + 1, i) for i in range(n - 1)])
    return low, high


def widen(x, bit):
    return jnp.concatenate([x, lax.ppermute(x, "z", [(i, i ^ bit) for i in range(8)])], axis=0)


def local(
    out_grad, moe_input, route_weight, route_ids, gate_proj, up_proj, down_proj,
    out_proj, conv_out, gate_b, gate_c, value_v, conv_taps,
):
    tok, ch = out_grad.shape
    n_exp = lax.axis_size(SP)
    cap = 4 * tok // n_exp
    total = n_exp * cap
    yi = lax.axis_index("y").astype(jnp.int32).reshape(1)
    ci = lax.axis_index("c").astype(jnp.int32).reshape(1)
    zi = lax.axis_index("z").astype(jnp.int32).reshape(1)
    xi = lax.axis_index("x").astype(jnp.int32).reshape(1)
    yi, ci, zi, xi, moe_input = lax.optimization_barrier((yi, ci, zi, xi, moe_input))
    send, sel = call(
        dispatch_kernel,
        [(n_exp, 2 * cap, ch), (tok, total)],
        0,
        (moe_input, out_grad, route_weight.T, route_ids.T),
        hbm_args=(0, 1, 2, 3),
    )
    recv = lax.all_to_all(send, SP, 0, 0, tiled=True)
    recv, gate_b, conv_out, gate_proj, up_proj, down_proj = lax.optimization_barrier(
        (recv, gate_b, conv_out, gate_proj, up_proj, down_proj)
    )
    (mixed,) = call(mixed_kernel, [(tok, ch)], 0, (gate_b, conv_out), hbm_args=(0, 1))
    hx = recv[:, :cap].reshape(total, ch)
    hy = recv[:, cap:].reshape(total, ch)
    ax = shift(hx, "y", 4, 1)
    by = shift(hy, "y", 4, 3)
    ay = shift(hy, "y", 4, 1)
    bx = shift(hx, "y", 4, 3)
    mix = widen(mixed, 4)
    f, d = down_proj.shape[1:]
    w_pair, w_down = call(
        load_kernel,
        [(2 * f, d), (f, d)],
        0,
        (gate_proj[0].T, up_proj[0].T, down_proj[0]),
        scratch=[pltpu.SemaphoreType.DMA((3,))],
        any_args=(0, 1, 2),
    )
    ax, by, w_pair, w_down = lax.optimization_barrier((ax, by, w_pair, w_down))
    fx = shift(ax, "y", 4, 1)
    fy = shift(by, "y", 4, 3)
    mix = widen(mix, 2)
    pieces = []
    for px, py in ((hx, hy), (bx, by), (fx, fy), (ax, ay)):
        pieces += [px, py, shift(px, "c", 2, 1), shift(py, "c", 2, 1)]
    mix = widen(mix, 1)
    theirs, xin, dyin, hidden, dgu, dgu_rows = call(
        expert_kernel,
        [(4, total, ch), (total, d), (total, d), (f, total), (2 * f, total), (total, 2 * f)],
        2,
        (yi, ci, *pieces, w_pair, w_down),
        scratch=[pltpu.VMEM((2 * f, total), F32), pltpu.VMEM((f, total), F32)],
        flops=8 * total * d * f,
        limit=24,
    )
    got = shift(theirs, "c", 2, 1)
    (mine,) = call(own_half_kernel, [(4, total, ch)], 2, (yi, ci, dgu_rows, w_pair), flops=2 * total * d * f)
    pair = call(pair_kernel, [(total, ch)] * 4, 0, (mine, got))
    parts = [shift(pair[k], "y", 4, k) for k in (1, 3, 2)]
    gate_t, up_t, grad_down = call(
        weights_kernel,
        [(f, d)] * 3,
        0,
        (xin, dyin, hidden, dgu),
        flops=6 * total * d * f,
        hbm_outs=(0, 1, 2),
        limit=24,
    )
    parts, mix, gate_t, up_t, grad_down = lax.optimization_barrier((parts, mix, gate_t, up_t, grad_down))
    (summed,) = call(sum_kernel, [(total, ch)], 0, (pair[0], *parts))
    back = lax.all_to_all(summed.reshape(n_exp, cap, ch), SP, 0, 0, tiled=True)
    dh, first, last = call(
        combine_kernel, [(tok, ch), (2, ch), (2, ch)], 0, (sel, back.reshape(total, ch), out_grad, gate_b)
    )
    swap = [(z * 8 + y * 2 + c, (y * 2 + c) * 8 + z) for z in range(8) for y in range(4) for c in range(2)]
    turned = lax.ppermute(dh, ("z", "y", "c"), swap)
    low, high = edges(first, last)
    h_own, h_part = over_tp(dh)
    (stack,) = call(stack_kernel, [(tok + 16, ch)], 0, (turned, low, high))
    t_own, t_part = over_tp(stack)
    terms = call(
        outer_kernel,
        [(ch // 4, ch)] * 4,
        4,
        (yi, ci, zi, xi, t_own, t_part, mix),
        scratch=[pltpu.VMEM((8 * tok, ch), BF)] * 2 + [pltpu.VMEM((ch, ch), F32)],
        flops=16 * tok * ch * ch,
    )
    came = [shift(terms[k], "x", 4, k) for k in (1, 3, 2)]
    grad_b, grad_c, grad_v = call(
        mixer_kernel,
        [(tok, ch)] * 3,
        2,
        (yi, ci, h_own, h_part, t_own, t_part, out_proj, gate_b, conv_out, low, high, conv_taps, value_v, gate_c),
        flops=2 * tok * d * ch,
        hbm_outs=(0, 1, 2),
    )
    (grad_out,) = call(sum_kernel, [(ch // 4, ch)], 0, (terms[0], *came), hbm_outs=(0,), kind=F32)
    return (gate_t.T[None], up_t.T[None], grad_down[None], grad_out, grad_b, grad_c, grad_v)


def solution(mesh):
    split = Mesh(mesh.devices.reshape(8, 4, 4, 2), ("z", "x", "y", "c"))
    return jax.shard_map(
        local,
        mesh=split,
        in_specs=(
            P(SP, TP), P(SP, TP), P(SP, None), P(SP, None), P(SP, None, TP), P(SP, None, TP),
            P(SP, TP, None), P(None, TP), P(SP, TP), P(SP, TP), P(SP, TP), P(SP, TP), P(None, TP),
        ),
        out_specs=(
            P(SP, None, TP), P(SP, None, TP), P(SP, TP, None), P(SP, TP), P(SP, TP), P(SP, TP), P(SP, TP),
        ),
        check_vma=False,
    )
```

profile of v0, /device:TPU:2, one launch (start us, length us, event | category | flops | bytes accessed | tf_op | source)
XLA Modules:
  0.0 145.8 jit_solution(8396716837646164)
XLA Ops:
  0.6 1.4 shard_map.180
  2.0 28.2 %all_to_all.10 = bf16[32,32,256]{2,1,0:T(8,128)(2,1)S(1)} all-to-all(bf16[32,32,256]{2,1,0:T(8,128)(2,1)S(1)} %get-tuple-element.59), channel_id=1, replica_groups=mesh['z'=8,'x'=4,'y'=4,'c'=2] {'z','x'}, dimensions={0} | all-to-all | bytes 1048576 | tf_op jit(solution)/shard_map/all_to_all | solution.py:262
  30.3 1.6 %collective-permute-start.3 = (bf16[512,256]{1,0:T(8,128)(2,1)S(1)}, bf16[512,256]{1,0:T(8,128)(2,1)S(1)}, u32[]{:S(2)}, u32[]{:S(2)}) collective-permute-start(bf16[512,256]{1,0:T(8,128)(2,1)S(1)} %bitcast.30), channel_id=1, source_target_pairs={{0,2},{2,4},{4,6},{6,0},{1,3},{3,5},{5,7},{7,1},{8,10},{10,12},{12... | collective-permute-start | bytes 786440 | tf_op jit(solution)/shard_map/ppermute | solution.py:52
  32.0 1.7 %collective-permute-start.4 = (bf16[512,256]{1,0:T(8,128)(2,1)S(1)}, bf16[512,256]{1,0:T(8,128)(2,1)S(1)}, u32[]{:S(2)}, u32[]{:S(2)}) collective-permute-start(bf16[512,256]{1,0:T(8,128)(2,1)S(1)} %bitcast.26), channel_id=1, source_target_pairs={{0,6},{2,0},{4,2},{6,4},{1,7},{3,1},{5,3},{7,5},{8,14},{10,8},{12,... | collective-permute-start | bytes 786440 | tf_op jit(solution)/shard_map/ppermute | solution.py:52
  33.6 0.4 collective-permute-start.11
  34.0 2.9 %collective-permute-start.2 = (bf16[512,256]{1,0:T(8,128)(2,1)S(1)}, bf16[512,256]{1,0:T(8,128)(2,1)S(1)}, u32[]{:S(2)}, u32[]{:S(2)}) collective-permute-start(bf16[512,256]{1,0:T(8,128)(2,1)S(1)} %bitcast.31), channel_id=1, source_target_pairs={{0,6},{2,0},{4,2},{6,4},{1,7},{3,1},{5,3},{7,5},{8,14},{10,8},{12,... | collective-permute-start | bytes 786440 | tf_op jit(solution)/shard_map/ppermute | solution.py:52
  36.9 0.0 collective-permute-start
  36.9 2.3 %shard_map.181 = (bf16[704,2048]{1,0:T(8,128)(2,1)S(1)}, bf16[352,2048]{1,0:T(8,128)(2,1)S(1)}) custom-call(bf16[352,2048]{1,0:T(8,128)(2,1)} %bitcast.34, bf16[352,2048]{1,0:T(8,128)(2,1)} %bitcast.35, bf16[352,2048]{1,0:T(8,128)(2,1)} %bitcast.36), custom_call_target="tpu_custom_call" | custom-call | tf_op jit(solution)/shard_map/pallas_call | solution.py:28
  39.1 1.6 %collective-permute-done.3.refs_12_ = bf16[512,256]{1,0:T(8,128)(2,1)S(1)} collective-permute-done((bf16[512,256]{1,0:T(8,128)(2,1)S(1)}, bf16[512,256]{1,0:T(8,128)(2,1)S(1)}, u32[]{:S(2)}, u32[]{:S(2)}) %collective-permute-start.3) | collective-permute-done | bytes 262176 | tf_op jit(solution)/shard_map/ppermute | solution.py:52
  40.8 0.0 collective-permute-start.1
  40.8 0.4 collective-permute-done.4.refs_5_
  41.1 2.9 %collective-permute-start.8 = (bf16[512,256]{1,0:T(8,128)(2,1)S(1)}, bf16[512,256]{1,0:T(8,128)(2,1)S(1)}, u32[]{:S(2)}, u32[]{:S(2)}) collective-permute-start(bf16[512,256]{1,0:T(8,128)(2,1)S(1)} %collective-permute-done.4.refs_5_), channel_id=1, source_target_pairs={{0,6},{2,0},{4,2},{6,4},{1,7},{3,1},{5,3},{7,5},{8,14},{10,8},{12,... | collective-permute-start | bytes 786440 | tf_op jit(solution)/shard_map/ppermute | solution.py:52
  44.0 0.0 collective-permute-done.11.refs_13_
  44.0 0.3 collective-permute-start.7
  44.4 0.5 collective-permute-start.6
  44.9 0.1 collective-permute-start.13
  45.0 4.7 %collective-permute-done.8.refs_9_ = bf16[512,256]{1,0:T(8,128)(2,1)S(1)} collective-permute-done((bf16[512,256]{1,0:T(8,128)(2,1)S(1)}, bf16[512,256]{1,0:T(8,128)(2,1)S(1)}, u32[]{:S(2)}, u32[]{:S(2)}) %collective-permute-start.8) | collective-permute-done | bytes 262176 | tf_op jit(solution)/shard_map/ppermute | solution.py:52
  49.7 2.6 %collective-permute-done.7.refs_8_ = bf16[512,256]{1,0:T(8,128)(2,1)S(1)} collective-permute-done((bf16[512,256]{1,0:T(8,128)(2,1)S(1)}, bf16[512,256]{1,0:T(8,128)(2,1)S(1)}, u32[]{:S(2)}, u32[]{:S(2)}) %collective-permute-start.7) | collective-permute-done | bytes 262176 | tf_op jit(solution)/shard_map/ppermute | solution.py:52
  52.3 0.5 collective-permute-start.9
  52.8 1.0 collective-permute-done.10.refs_11_
  53.8 0.4 collective-permute-done.9.refs_10_
  54.2 4.1 %shard_map.182 = (bf16[4,512,256]{2,1,0:T(8,128)(2,1)S(1)}, bf16[512,2048]{1,0:T(8,128)(2,1)S(1)}, bf16[512,2048]{1,0:T(8,128)(2,1)S(1)}, bf16[352,512]{1,0:T(8,...) custom-call(s32[1]{0:T(128)} %bitcast.y_ref, s32[1]{0:T(128)} %bitcast.1.c_ref, ...), custom_call_target="tpu_custom_call" | custom-call | flops 2952790016 | tf_op jit(solution)/shard_map/pallas_call | solution.py:28
  58.3 0.2 collective-permute-start.14
  58.5 0.9 shard_map.185
  59.4 1.7 %collective-permute-start.18 = (bf16[128,256]{1,0:T(8,128)(2,1)S(1)}, bf16[128,256]{1,0:T(8,128)(2,1)S(1)}, u32[]{:S(2)}, u32[]{:S(2)}) collective-permute-start(bf16[128,256]{1,0:T(8,128)(2,1)S(1)} %shard_map.185), channel_id=1, source_target_pairs={{0,128},{32,160},{64,192},{96,224},{128,0},{160,32},{192,64},{224,... | collective-permute-start | bytes 196616 | tf_op jit(solution)/shard_map/ppermute | solution.py:239
  61.1 7.1 %collective-permute-done.18 = bf16[128,256]{1,0:T(8,128)(2,1)S(1)} collective-permute-done((bf16[128,256]{1,0:T(8,128)(2,1)S(1)}, bf16[128,256]{1,0:T(8,128)(2,1)S(1)}, u32[]{:S(2)}, u32[]{:S(2)}) %collective-permute-start.18) | collective-permute-done | bytes 65568 | tf_op jit(solution)/shard_map/ppermute | solution.py:239
  68.1 0.1 collective-permute-start.19
  68.2 8.4 %collective-permute-done.19 = bf16[256,256]{1,0:T(8,128)(2,1)S(1)} collective-permute-done((bf16[256,256]{1,0:T(8,128)(2,1)S(1)}, bf16[256,256]{1,0:T(8,128)(2,1)S(1)}, u32[]{:S(2)}, u32[]{:S(2)}) %collective-permute-start.19) | collective-permute-done | bytes 131104 | tf_op jit(solution)/shard_map/ppermute | solution.py:239
  76.6 0.1 collective-permute-start.20
  76.7 1.0 shard_map.183.mine_ref
  77.8 0.2 shard_map.184
  78.0 0.1 collective-permute-start.15
  78.1 3.2 %collective-permute-start.16 = (bf16[512,256]{1,0:T(8,128)(2,1)S(1)}, bf16[512,256]{1,0:T(8,128)(2,1)S(1)}, u32[]{:S(2)}, u32[]{:S(2)}) collective-permute-start(bf16[512,256]{1,0:T(8,128)(2,1)S(1)} %get-tuple-element.73), channel_id=1, source_target_pairs={{0,6},{2,0},{4,2},{6,4},{1,7},{3,1},{5,3},{7,5},{8,14},{10,8},{12,... | collective-permute-start | bytes 786440 | tf_op jit(solution)/shard_map/ppermute | solution.py:52
  81.3 1.8 %collective-permute-done.20 = bf16[512,256]{1,0:T(8,128)(2,1)S(1)} collective-permute-done((bf16[512,256]{1,0:T(8,128)(2,1)S(1)}, bf16[512,256]{1,0:T(8,128)(2,1)S(1)}, u32[]{:S(2)}, u32[]{:S(2)}) %collective-permute-start.20) | collective-permute-done | bytes 262176 | tf_op jit(solution)/shard_map/ppermute | solution.py:239
  83.1 3.8 %shard_map.186 = (bf16[352,2048]{1,0:T(8,128)(2,1)}, bf16[352,2048]{1,0:T(8,128)(2,1)}, bf16[352,2048]{1,0:T(8,128)(2,1)}) custom-call(bf16[512,2048]{1,0:T(8,128)(2,1)S(1)} %get-tuple-element.77.x_ref, bf16[512,2048]{1,0:T(8,128)(2,1)S(1)} %get-tuple-element.78.dy_ref, bf16[352,512]{1,0:T(8,128)(2,1)S(1)} %get-tuple-element.79.hid_ref, ...), custom_call_target="tpu_custom_call" | custom-call | flops 2214592512 | tf_op jit(solution)/shard_map/pallas_call | solution.py:28
  86.9 4.4 %collective-permute-done.15.refs_1_ = bf16[512,256]{1,0:T(8,128)(2,1)S(1)} collective-permute-done((bf16[512,256]{1,0:T(8,128)(2,1)S(1)}, bf16[512,256]{1,0:T(8,128)(2,1)S(1)}, u32[]{:S(2)}, u32[]{:S(2)}) %collective-permute-start.15) | collective-permute-done | bytes 262176 | tf_op jit(solution)/shard_map/ppermute | solution.py:52
  91.3 0.1 shard_map.187
  91.4 18.3 %all_to_all.11 = bf16[32,16,256]{2,1,0:T(8,128)(2,1)S(1)} all-to-all(bf16[32,16,256]{2,1,0:T(8,128)(2,1)S(1)} %bitcast.24), channel_id=1, replica_groups=mesh['z'=8,'x'=4,'y'=4,'c'=2] {'z','x'}, dimensions={0} | all-to-all | bytes 524288 | tf_op jit(solution)/shard_map/all_to_all | solution.py:315
  109.8 0.0 copy-start.4
  109.8 0.0 copy-start.5
  109.8 0.0 copy-start.6
  109.8 0.2 shard_map.188
  110.0 3.0 %collective-permute-start.31 = (bf16[128,256]{1,0:T(8,128)(2,1)S(1)}, bf16[128,256]{1,0:T(8,128)(2,1)S(1)}, u32[]{:S(2)}, u32[]{:S(2)}) collective-permute-start(bf16[128,256]{1,0:T(8,128)(2,1)S(1)} %get-tuple-element.94), channel_id=1, source_target_pairs={{0,6},{2,0},{4,2},{6,4},{1,7},{3,1},{5,3},{7,5},{8,14},{10,8},{12,... | collective-permute-start | bytes 196616 | tf_op jit(solution)/shard_map/ppermute | solution.py:52
  113.0 0.7 collective-permute-start.21
  113.7 3.3 %collective-permute-start.22 = (bf16[2,256]{1,0:T(2,128)(2,1)S(1)}, bf16[2,256]{1,0:T(2,128)(2,1)S(1)}, u32[]{:S(2)}, u32[]{:S(2)}) collective-permute-start(bf16[2,256]{1,0:T(2,128)(2,1)S(1)} %get-tuple-element.95), channel_id=1, source_target_pairs={{0,8},{8,16},{16,24},{24,32},{32,40},{40,48},{48,56},{56,64},{64,7... | collective-permute-start | bytes 3080 | tf_op jit(solution)/shard_map/ppermute | solution.py:233
  117.0 2.6 %collective-permute-start.23 = (bf16[2,256]{1,0:T(2,128)(2,1)S(1)}, bf16[2,256]{1,0:T(2,128)(2,1)S(1)}, u32[]{:S(2)}, u32[]{:S(2)}) collective-permute-start(bf16[2,256]{1,0:T(2,128)(2,1)S(1)} %get-tuple-element.96), channel_id=1, source_target_pairs={{8,0},{16,8},{24,16},{32,24},{40,32},{48,40},{56,48},{64,56},{72,6... | collective-permute-start | bytes 3080 | tf_op jit(solution)/shard_map/ppermute | solution.py:234
  119.6 6.3 %collective-permute-start.32 = (bf16[128,256]{1,0:T(8,128)(2,1)S(1)}, bf16[128,256]{1,0:T(8,128)(2,1)S(1)}, u32[]{:S(2)}, u32[]{:S(2)}) collective-permute-start(bf16[128,256]{1,0:T(8,128)(2,1)S(1)} %get-tuple-element.94), channel_id=1, source_target_pairs={{0,4},{2,6},{4,0},{6,2},{1,5},{3,7},{5,1},{7,3},{8,12},{10,14},{12... | collective-permute-start | bytes 196616 | tf_op jit(solution)/shard_map/ppermute | solution.py:52
  125.8 0.2 collective-permute-start.33
  126.0 3.1 %collective-permute-start.24 = (bf16[144,256]{1,0:T(8,128)(2,1)S(1)}, bf16[144,256]{1,0:T(8,128)(2,1)S(1)}, u32[]{:S(2)}, u32[]{:S(2)}) collective-permute-start(bf16[144,256]{1,0:T(8,128)(2,1)S(1)} %shard_map.189), channel_id=1, source_target_pairs={{0,6},{2,0},{4,2},{6,4},{1,7},{3,1},{5,3},{7,5},{8,14},{10,8},{12,... | collective-permute-start | bytes 221192 | tf_op jit(solution)/shard_map/ppermute | solution.py:52
  129.2 1.0 collective-permute-start.26
  130.2 1.7 %collective-permute-done.24 = bf16[144,256]{1,0:T(8,128)(2,1)S(1)} collective-permute-done((bf16[144,256]{1,0:T(8,128)(2,1)S(1)}, bf16[144,256]{1,0:T(8,128)(2,1)S(1)}, u32[]{:S(2)}, u32[]{:S(2)}) %collective-permute-start.24) | collective-permute-done | bytes 73760 | tf_op jit(solution)/shard_map/ppermute | solution.py:52
  131.9 3.3 %collective-permute-done.25 = bf16[144,256]{1,0:T(8,128)(2,1)S(1)} collective-permute-done((bf16[144,256]{1,0:T(8,128)(2,1)S(1)}, bf16[144,256]{1,0:T(8,128)(2,1)S(1)}, u32[]{:S(2)}, u32[]{:S(2)}) %collective-permute-start.25) | collective-permute-done | bytes 73760 | tf_op jit(solution)/shard_map/ppermute | solution.py:52
  135.1 0.4 collective-permute-done.26
  135.5 0.1 collective-permute-start.27
  135.7 0.6 collective-permute-start.34
  136.2 1.0 collective-permute-done.27.part_ref.edge_part_ref
  137.2 0.4 shard_map.190
  137.6 1.0 collective-permute-start.28
  138.6 1.1 collective-permute-start.29
  139.7 1.5 %collective-permute-start.30 = (bf16[64,256]{1,0:T(8,128)(2,1)S(1)}, bf16[64,256]{1,0:T(8,128)(2,1)S(1)}, u32[]{:S(2)}, u32[]{:S(2)}) collective-permute-start(bf16[64,256]{1,0:T(8,128)(2,1)S(1)} %get-tuple-element.101), channel_id=1, source_target_pairs={{0,16},{8,24},{16,0},{24,8},{1,17},{9,25},{17,1},{25,9},{2,18},{10... | collective-permute-start | bytes 98312 | tf_op jit(solution)/shard_map/ppermute | solution.py:52
  141.3 1.1 shard_map.192
  142.4 0.2 collective-permute-done.29.refs_2_
  142.5 2.6 %collective-permute-done.30.refs_3_ = bf16[64,256]{1,0:T(8,128)(2,1)S(1)} collective-permute-done((bf16[64,256]{1,0:T(8,128)(2,1)S(1)}, bf16[64,256]{1,0:T(8,128)(2,1)S(1)}, u32[]{:S(2)}, u32[]{:S(2)}) %collective-permute-start.30) | collective-permute-done | bytes 32800 | tf_op jit(solution)/shard_map/ppermute | solution.py:52
  145.2 0.6 shard_map.191
  (44 shorter events, 0.2 us)
Async XLA Ops:
  30.3 10.5 %collective-permute-start.3 = (bf16[512,256]{1,0:T(8,128)(2,1)S(1)}, bf16[512,256]{1,0:T(8,128)(2,1)S(1)}, u32[]{:S(2)}, u32[]{:S(2)}) collective-permute-start(bf16[512,256]{1,0:T(8,128)(2,1)S(1)} %bitcast.30), channel_id=1, source_target_pairs={{0,2},{2,4},{4,6},{6,0},{1,3},{3,5},{5,7},{7,1},{8,10},{10,12},{12... | collective-permute-start | bytes 786440 | tf_op jit(solution)/shard_map/ppermute | solution.py:52
  32.0 9.2 %collective-permute-start.4 = (bf16[512,256]{1,0:T(8,128)(2,1)S(1)}, bf16[512,256]{1,0:T(8,128)(2,1)S(1)}, u32[]{:S(2)}, u32[]{:S(2)}) collective-permute-start(bf16[512,256]{1,0:T(8,128)(2,1)S(1)} %bitcast.26), channel_id=1, source_target_pairs={{0,6},{2,0},{4,2},{6,4},{1,7},{3,1},{5,3},{7,5},{8,14},{10,8},{12,... | collective-permute-start | bytes 786440 | tf_op jit(solution)/shard_map/ppermute | solution.py:52
  33.6 10.4 %collective-permute-start.11 = (bf16[512,256]{1,0:T(8,128)(2,1)S(1)}, bf16[512,256]{1,0:T(8,128)(2,1)S(1)}, u32[]{:S(2)}, u32[]{:S(2)}) collective-permute-start(bf16[512,256]{1,0:T(8,128)(2,1)S(1)} %bitcast.27), channel_id=1, source_target_pairs={{0,2},{2,4},{4,6},{6,0},{1,3},{3,5},{5,7},{7,1},{8,10},{10,12},{12... | collective-permute-start | bytes 786440 | tf_op jit(solution)/shard_map/ppermute | solution.py:52
  34.0 10.4 %collective-permute-start.2 = (bf16[512,256]{1,0:T(8,128)(2,1)S(1)}, bf16[512,256]{1,0:T(8,128)(2,1)S(1)}, u32[]{:S(2)}, u32[]{:S(2)}) collective-permute-start(bf16[512,256]{1,0:T(8,128)(2,1)S(1)} %bitcast.31), channel_id=1, source_target_pairs={{0,6},{2,0},{4,2},{6,4},{1,7},{3,1},{5,3},{7,5},{8,14},{10,8},{12,... | collective-permute-start | bytes 786440 | tf_op jit(solution)/shard_map/ppermute | solution.py:52
  36.9 7.5 %collective-permute-start = (bf16[512,256]{1,0:T(8,128)(2,1)S(1)}, bf16[512,256]{1,0:T(8,128)(2,1)S(1)}, u32[]{:S(2)}, u32[]{:S(2)}) collective-permute-start(bf16[512,256]{1,0:T(8,128)(2,1)S(1)} %bitcast.32), channel_id=1, source_target_pairs={{0,1},{1,0},{2,3},{3,2},{4,5},{5,4},{6,7},{7,6},{8,9},{9,8},{10,11... | collective-permute-start | bytes 786440 | tf_op jit(solution)/shard_map/ppermute | solution.py:52
  40.8 4.1 %collective-permute-start.1 = (bf16[512,256]{1,0:T(8,128)(2,1)S(1)}, bf16[512,256]{1,0:T(8,128)(2,1)S(1)}, u32[]{:S(2)}, u32[]{:S(2)}) collective-permute-start(bf16[512,256]{1,0:T(8,128)(2,1)S(1)} %bitcast.28), channel_id=1, source_target_pairs={{0,1},{1,0},{2,3},{3,2},{4,5},{5,4},{6,7},{7,6},{8,9},{9,8},{10,11... | collective-permute-start | bytes 786440 | tf_op jit(solution)/shard_map/ppermute | solution.py:52
  41.1 8.5 %collective-permute-start.8 = (bf16[512,256]{1,0:T(8,128)(2,1)S(1)}, bf16[512,256]{1,0:T(8,128)(2,1)S(1)}, u32[]{:S(2)}, u32[]{:S(2)}) collective-permute-start(bf16[512,256]{1,0:T(8,128)(2,1)S(1)} %collective-permute-done.4.refs_5_), channel_id=1, source_target_pairs={{0,6},{2,0},{4,2},{6,4},{1,7},{3,1},{5,3},{7,5},{8,14},{10,8},{12,... | collective-permute-start | bytes 786440 | tf_op jit(solution)/shard_map/ppermute | solution.py:52
  44.0 8.2 %collective-permute-start.7 = (bf16[512,256]{1,0:T(8,128)(2,1)S(1)}, bf16[512,256]{1,0:T(8,128)(2,1)S(1)}, u32[]{:S(2)}, u32[]{:S(2)}) collective-permute-start(bf16[512,256]{1,0:T(8,128)(2,1)S(1)} %collective-permute-done.3.refs_12_), channel_id=1, source_target_pairs={{0,2},{2,4},{4,6},{6,0},{1,3},{3,5},{5,7},{7,1},{8,10},{10,12},{12... | collective-permute-start | bytes 786440 | tf_op jit(solution)/shard_map/ppermute | solution.py:52
  44.3 7.9 %collective-permute-start.12 = (bf16[512,256]{1,0:T(8,128)(2,1)S(1)}, bf16[512,256]{1,0:T(8,128)(2,1)S(1)}, u32[]{:S(2)}, u32[]{:S(2)}) collective-permute-start(bf16[512,256]{1,0:T(8,128)(2,1)S(1)} %collective-permute-done.3.refs_12_), channel_id=1, source_target_pairs={{0,1},{1,0},{2,3},{3,2},{4,5},{5,4},{6,7},{7,6},{8,9},{9,8},{10,11... | collective-permute-start | bytes 786440 | tf_op jit(solution)/shard_map/ppermute | solution.py:52
  44.4 8.4 %collective-permute-start.6 = (bf16[512,256]{1,0:T(8,128)(2,1)S(1)}, bf16[512,256]{1,0:T(8,128)(2,1)S(1)}, u32[]{:S(2)}, u32[]{:S(2)}) collective-permute-start(bf16[512,256]{1,0:T(8,128)(2,1)S(1)} %collective-permute-done.4.refs_5_), channel_id=1, source_target_pairs={{0,1},{1,0},{2,3},{3,2},{4,5},{5,4},{6,7},{7,6},{8,9},{9,8},{10,11... | collective-permute-start | bytes 786440 | tf_op jit(solution)/shard_map/ppermute | solution.py:52
  44.9 7.9 %collective-permute-start.13 = (bf16[512,256]{1,0:T(8,128)(2,1)S(1)}, bf16[512,256]{1,0:T(8,128)(2,1)S(1)}, u32[]{:S(2)}, u32[]{:S(2)}) collective-permute-start(bf16[512,256]{1,0:T(8,128)(2,1)S(1)} %collective-permute-done.11.refs_13_), channel_id=1, source_target_pairs={{0,1},{1,0},{2,3},{3,2},{4,5},{5,4},{6,7},{7,6},{8,9},{9,8},{10,11... | collective-permute-start | bytes 786440 | tf_op jit(solution)/shard_map/ppermute | solution.py:52
  49.7 3.1 %collective-permute-start.5 = (bf16[512,256]{1,0:T(8,128)(2,1)S(1)}, bf16[512,256]{1,0:T(8,128)(2,1)S(1)}, u32[]{:S(2)}, u32[]{:S(2)}) collective-permute-start(bf16[512,256]{1,0:T(8,128)(2,1)S(1)} %collective-permute-done.2.refs_4_), channel_id=1, source_target_pairs={{0,1},{1,0},{2,3},{3,2},{4,5},{5,4},{6,7},{7,6},{8,9},{9,8},{10,11... | collective-permute-start | bytes 786440 | tf_op jit(solution)/shard_map/ppermute | solution.py:52
  52.2 1.5 %collective-permute-start.10 = (bf16[512,256]{1,0:T(8,128)(2,1)S(1)}, bf16[512,256]{1,0:T(8,128)(2,1)S(1)}, u32[]{:S(2)}, u32[]{:S(2)}) collective-permute-start(bf16[512,256]{1,0:T(8,128)(2,1)S(1)} %collective-permute-done.8.refs_9_), channel_id=1, source_target_pairs={{0,1},{1,0},{2,3},{3,2},{4,5},{5,4},{6,7},{7,6},{8,9},{9,8},{10,11... | collective-permute-start | bytes 786440 | tf_op jit(solution)/shard_map/ppermute | solution.py:52
  52.3 1.9 %collective-permute-start.9 = (bf16[512,256]{1,0:T(8,128)(2,1)S(1)}, bf16[512,256]{1,0:T(8,128)(2,1)S(1)}, u32[]{:S(2)}, u32[]{:S(2)}) collective-permute-start(bf16[512,256]{1,0:T(8,128)(2,1)S(1)} %collective-permute-done.7.refs_8_), channel_id=1, source_target_pairs={{0,1},{1,0},{2,3},{3,2},{4,5},{5,4},{6,7},{7,6},{8,9},{9,8},{10,11... | collective-permute-start | bytes 786440 | tf_op jit(solution)/shard_map/ppermute | solution.py:52
  58.3 19.5 %collective-permute-start.14 = (bf16[4,512,256]{2,1,0:T(8,128)(2,1)S(1)}, bf16[4,512,256]{2,1,0:T(8,128)(2,1)S(1)}, u32[]{:S(2)}, u32[]{:S(2)}) collective-permute-start(bf16[4,512,256]{2,1,0:T(8,128)(2,1)S(1)} %get-tuple-element.71), channel_id=1, source_target_pairs={{0,1},{1,0},{2,3},{3,2},{4,5},{5,4},{6,7},{7,6},{8,9},{9,8},{10,11... | collective-permute-start | bytes 3145736 | tf_op jit(solution)/shard_map/ppermute | solution.py:52
  59.4 8.7 %collective-permute-start.18 = (bf16[128,256]{1,0:T(8,128)(2,1)S(1)}, bf16[128,256]{1,0:T(8,128)(2,1)S(1)}, u32[]{:S(2)}, u32[]{:S(2)}) collective-permute-start(bf16[128,256]{1,0:T(8,128)(2,1)S(1)} %shard_map.185), channel_id=1, source_target_pairs={{0,128},{32,160},{64,192},{96,224},{128,0},{160,32},{192,64},{224,... | collective-permute-start | bytes 196616 | tf_op jit(solution)/shard_map/ppermute | solution.py:239
  68.1 8.5 %collective-permute-start.19 = (bf16[256,256]{1,0:T(8,128)(2,1)S(1)}, bf16[256,256]{1,0:T(8,128)(2,1)S(1)}, u32[]{:S(2)}, u32[]{:S(2)}) collective-permute-start(bf16[256,256]{1,0:T(8,128)(2,1)S(1)} %pad_maximum_fusion.3), channel_id=1, source_target_pairs={{0,64},{32,96},{64,0},{96,32},{128,192},{160,224},{192,128},{224,1... | collective-permute-start | bytes 393224 | tf_op jit(solution)/shard_map/ppermute | solution.py:239
  76.6 6.5 %collective-permute-start.20 = (bf16[512,256]{1,0:T(8,128)(2,1)S(1)}, bf16[512,256]{1,0:T(8,128)(2,1)S(1)}, u32[]{:S(2)}, u32[]{:S(2)}) collective-permute-start(bf16[512,256]{1,0:T(8,128)(2,1)S(1)} %pad_maximum_fusion.2), channel_id=1, source_target_pairs={{0,32},{32,0},{64,96},{96,64},{128,160},{160,128},{192,224},{224,1... | collective-permute-start | bytes 786440 | tf_op jit(solution)/shard_map/ppermute | solution.py:239
  78.0 13.3 %collective-permute-start.15 = (bf16[512,256]{1,0:T(8,128)(2,1)S(1)}, bf16[512,256]{1,0:T(8,128)(2,1)S(1)}, u32[]{:S(2)}, u32[]{:S(2)}) collective-permute-start(bf16[512,256]{1,0:T(8,128)(2,1)S(1)} %get-tuple-element.72), channel_id=1, source_target_pairs={{0,2},{2,4},{4,6},{6,0},{1,3},{3,5},{5,7},{7,1},{8,10},{10,12},{12... | collective-permute-start | bytes 786440 | tf_op jit(solution)/shard_map/ppermute | solution.py:52
  78.1 13.2 %collective-permute-start.16 = (bf16[512,256]{1,0:T(8,128)(2,1)S(1)}, bf16[512,256]{1,0:T(8,128)(2,1)S(1)}, u32[]{:S(2)}, u32[]{:S(2)}) collective-permute-start(bf16[512,256]{1,0:T(8,128)(2,1)S(1)} %get-tuple-element.73), channel_id=1, source_target_pairs={{0,6},{2,0},{4,2},{6,4},{1,7},{3,1},{5,3},{7,5},{8,14},{10,8},{12,... | collective-permute-start | bytes 786440 | tf_op jit(solution)/shard_map/ppermute | solution.py:52
  81.3 10.0 %collective-permute-start.17 = (bf16[512,256]{1,0:T(8,128)(2,1)S(1)}, bf16[512,256]{1,0:T(8,128)(2,1)S(1)}, u32[]{:S(2)}, u32[]{:S(2)}) collective-permute-start(bf16[512,256]{1,0:T(8,128)(2,1)S(1)} %get-tuple-element.74), channel_id=1, source_target_pairs={{0,4},{2,6},{4,0},{6,2},{1,5},{3,7},{5,1},{7,3},{8,12},{10,14},{12... | collective-permute-start | bytes 786440 | tf_op jit(solution)/shard_map/ppermute | solution.py:52
  86.9 22.8 %copy-start.1 = (bf16[128,256]{1,0:T(8,128)(2,1)S(1)}, bf16[128,256]{1,0:T(8,128)(2,1)}, u32[]{:S(2)}) copy-start(bf16[128,256]{1,0:T(8,128)(2,1)} %b_ref.2) | copy-start | bytes 196612
  86.9 22.8 %copy-start.3 = (bf16[128,256]{1,0:T(8,128)(2,1)S(1)}, bf16[128,256]{1,0:T(8,128)(2,1)}, u32[]{:S(2)}) copy-start(bf16[128,256]{1,0:T(8,128)(2,1)} %og_ref.3) | copy-start | bytes 196612
  109.7 31.5 %copy-start = (bf16[2048,256]{1,0:T(8,128)(2,1)S(1)}, bf16[2048,256]{1,0:T(8,128)(2,1)}, u32[]{:S(2)}) copy-start(bf16[2048,256]{1,0:T(8,128)(2,1)} %w_ref.1) | copy-start | bytes 3145732
  109.8 31.5 %copy-start.2 = (bf16[128,256]{1,0:T(8,128)(2,1)S(1)}, bf16[128,256]{1,0:T(8,128)(2,1)}, u32[]{:S(2)}) copy-start(bf16[128,256]{1,0:T(8,128)(2,1)} %co_ref.1) | copy-start | bytes 196612
  109.8 31.5 %copy-start.4 = (bf16[128,256]{1,0:T(8,128)(2,1)S(1)}, bf16[128,256]{1,0:T(8,128)(2,1)}, u32[]{:S(2)}) copy-start(bf16[128,256]{1,0:T(8,128)(2,1)} %v_ref.1) | copy-start | bytes 196612
  109.8 31.5 %copy-start.5 = (bf16[128,256]{1,0:T(8,128)(2,1)S(1)}, bf16[128,256]{1,0:T(8,128)(2,1)}, u32[]{:S(2)}) copy-start(bf16[128,256]{1,0:T(8,128)(2,1)} %g_ref.1) | copy-start | bytes 196612
  109.8 31.5 %copy-start.6 = (f32[3,256]{1,0:T(4,128)S(1)}, f32[3,256]{1,0:T(4,128)}, u32[]{:S(2)}) copy-start(f32[3,256]{1,0:T(4,128)} %t_ref.1) | copy-start | bytes 9220
  110.0 19.2 %collective-permute-start.31 = (bf16[128,256]{1,0:T(8,128)(2,1)S(1)}, bf16[128,256]{1,0:T(8,128)(2,1)S(1)}, u32[]{:S(2)}, u32[]{:S(2)}) collective-permute-start(bf16[128,256]{1,0:T(8,128)(2,1)S(1)} %get-tuple-element.94), channel_id=1, source_target_pairs={{0,6},{2,0},{4,2},{6,4},{1,7},{3,1},{5,3},{7,5},{8,14},{10,8},{12,... | collective-permute-start | bytes 196616 | tf_op jit(solution)/shard_map/ppermute | solution.py:52
  113.0 13.0 %collective-permute-start.21 = (bf16[128,256]{1,0:T(8,128)(2,1)S(1)}, bf16[128,256]{1,0:T(8,128)(2,1)S(1)}, u32[]{:S(2)}, u32[]{:S(2)}) collective-permute-start(bf16[128,256]{1,0:T(8,128)(2,1)S(1)} %get-tuple-element.94), channel_id=1, source_target_pairs={{0,0},{1,32},{2,64},{3,96},{4,128},{5,160},{6,192},{7,224},{32,1},... | collective-permute-start | bytes 196616 | tf_op jit(solution)/shard_map/ppermute | solution.py:320
  113.7 12.1 %collective-permute-start.22 = (bf16[2,256]{1,0:T(2,128)(2,1)S(1)}, bf16[2,256]{1,0:T(2,128)(2,1)S(1)}, u32[]{:S(2)}, u32[]{:S(2)}) collective-permute-start(bf16[2,256]{1,0:T(2,128)(2,1)S(1)} %get-tuple-element.95), channel_id=1, source_target_pairs={{0,8},{8,16},{16,24},{24,32},{32,40},{40,48},{48,56},{56,64},{64,7... | collective-permute-start | bytes 3080 | tf_op jit(solution)/shard_map/ppermute | solution.py:233
  117.0 9.0 %collective-permute-start.23 = (bf16[2,256]{1,0:T(2,128)(2,1)S(1)}, bf16[2,256]{1,0:T(2,128)(2,1)S(1)}, u32[]{:S(2)}, u32[]{:S(2)}) collective-permute-start(bf16[2,256]{1,0:T(2,128)(2,1)S(1)} %get-tuple-element.96), channel_id=1, source_target_pairs={{8,0},{16,8},{24,16},{32,24},{40,32},{48,40},{56,48},{64,56},{72,6... | collective-permute-start | bytes 3080 | tf_op jit(solution)/shard_map/ppermute | solution.py:234
  119.6 10.6 %collective-permute-start.32 = (bf16[128,256]{1,0:T(8,128)(2,1)S(1)}, bf16[128,256]{1,0:T(8,128)(2,1)S(1)}, u32[]{:S(2)}, u32[]{:S(2)}) collective-permute-start(bf16[128,256]{1,0:T(8,128)(2,1)S(1)} %get-tuple-element.94), channel_id=1, source_target_pairs={{0,4},{2,6},{4,0},{6,2},{1,5},{3,7},{5,1},{7,3},{8,12},{10,14},{12... | collective-permute-start | bytes 196616 | tf_op jit(solution)/shard_map/ppermute | solution.py:52
  125.8 9.8 %collective-permute-start.33 = (bf16[128,256]{1,0:T(8,128)(2,1)S(1)}, bf16[128,256]{1,0:T(8,128)(2,1)S(1)}, u32[]{:S(2)}, u32[]{:S(2)}) collective-permute-start(bf16[128,256]{1,0:T(8,128)(2,1)S(1)} %get-tuple-element.94), channel_id=1, source_target_pairs={{0,2},{2,4},{4,6},{6,0},{1,3},{3,5},{5,7},{7,1},{8,10},{10,12},{12... | collective-permute-start | bytes 196616 | tf_op jit(solution)/shard_map/ppermute | solution.py:52
  126.0 5.8 %collective-permute-start.24 = (bf16[144,256]{1,0:T(8,128)(2,1)S(1)}, bf16[144,256]{1,0:T(8,128)(2,1)S(1)}, u32[]{:S(2)}, u32[]{:S(2)}) collective-permute-start(bf16[144,256]{1,0:T(8,128)(2,1)S(1)} %shard_map.189), channel_id=1, source_target_pairs={{0,6},{2,0},{4,2},{6,4},{1,7},{3,1},{5,3},{7,5},{8,14},{10,8},{12,... | collective-permute-start | bytes 221192 | tf_op jit(solution)/shard_map/ppermute | solution.py:52
  129.2 6.0 %collective-permute-start.25 = (bf16[144,256]{1,0:T(8,128)(2,1)S(1)}, bf16[144,256]{1,0:T(8,128)(2,1)S(1)}, u32[]{:S(2)}, u32[]{:S(2)}) collective-permute-start(bf16[144,256]{1,0:T(8,128)(2,1)S(1)} %shard_map.189), channel_id=1, source_target_pairs={{0,4},{2,6},{4,0},{6,2},{1,5},{3,7},{5,1},{7,3},{8,12},{10,14},{12... | collective-permute-start | bytes 221192 | tf_op jit(solution)/shard_map/ppermute | solution.py:52
  129.2 6.4 %collective-permute-start.26 = (bf16[144,256]{1,0:T(8,128)(2,1)S(1)}, bf16[144,256]{1,0:T(8,128)(2,1)S(1)}, u32[]{:S(2)}, u32[]{:S(2)}) collective-permute-start(bf16[144,256]{1,0:T(8,128)(2,1)S(1)} %shard_map.189), channel_id=1, source_target_pairs={{0,2},{2,4},{4,6},{6,0},{1,3},{3,5},{5,7},{7,1},{8,10},{10,12},{12... | collective-permute-start | bytes 221192 | tf_op jit(solution)/shard_map/ppermute | solution.py:52
  135.5 1.7 %collective-permute-start.27 = (bf16[576,256]{1,0:T(8,128)(2,1)S(1)}, bf16[576,256]{1,0:T(8,128)(2,1)S(1)}, u32[]{:S(2)}, u32[]{:S(2)}) collective-permute-start(bf16[576,256]{1,0:T(8,128)(2,1)S(1)} %pad_maximum_fusion.1.own_ref.edge_own_ref), channel_id=1, source_target_pairs={{0,1},{1,0},{2,3},{3,2},{4,5},{5,4},{6,7},{7,6},{8,9},{9,8},{10,11... | collective-permute-start | bytes 884744 | tf_op jit(solution)/shard_map/ppermute | solution.py:52
  135.7 5.6 %collective-permute-start.34 = (bf16[512,256]{1,0:T(8,128)(2,1)S(1)}, bf16[512,256]{1,0:T(8,128)(2,1)S(1)}, u32[]{:S(2)}, u32[]{:S(2)}) collective-permute-start(bf16[512,256]{1,0:T(8,128)(2,1)S(1)} %constant_dynamic-update-slice_fusion.own_ref), channel_id=1, source_target_pairs={{0,1},{1,0},{2,3},{3,2},{4,5},{5,4},{6,7},{7,6},{8,9},{9,8},{10,11... | collective-permute-start | bytes 786440 | tf_op jit(solution)/shard_map/ppermute | solution.py:52
  137.6 4.7 %collective-permute-start.28 = (bf16[64,256]{1,0:T(8,128)(2,1)S(1)}, bf16[64,256]{1,0:T(8,128)(2,1)S(1)}, u32[]{:S(2)}, u32[]{:S(2)}) collective-permute-start(bf16[64,256]{1,0:T(8,128)(2,1)S(1)} %get-tuple-element.99), channel_id=1, source_target_pairs={{0,8},{8,16},{16,24},{24,0},{1,9},{9,17},{17,25},{25,1},{2,10},{10... | collective-permute-start | bytes 98312 | tf_op jit(solution)/shard_map/ppermute | solution.py:52
  138.6 3.9 %collective-permute-start.29 = (bf16[64,256]{1,0:T(8,128)(2,1)S(1)}, bf16[64,256]{1,0:T(8,128)(2,1)S(1)}, u32[]{:S(2)}, u32[]{:S(2)}) collective-permute-start(bf16[64,256]{1,0:T(8,128)(2,1)S(1)} %get-tuple-element.100), channel_id=1, source_target_pairs={{0,24},{8,0},{16,8},{24,16},{1,25},{9,1},{17,9},{25,17},{2,26},{10... | collective-permute-start | bytes 98312 | tf_op jit(solution)/shard_map/ppermute | solution.py:52
  139.7 5.4 %collective-permute-start.30 = (bf16[64,256]{1,0:T(8,128)(2,1)S(1)}, bf16[64,256]{1,0:T(8,128)(2,1)S(1)}, u32[]{:S(2)}, u32[]{:S(2)}) collective-permute-start(bf16[64,256]{1,0:T(8,128)(2,1)S(1)} %get-tuple-element.101), channel_id=1, source_target_pairs={{0,16},{8,24},{16,0},{24,8},{1,17},{9,25},{17,1},{25,9},{2,18},{10... | collective-permute-start | bytes 98312 | tf_op jit(solution)/shard_map/ppermute | solution.py:52
where the time goes:
time: 147 us; the launch traced here: 146 us
  blocking collectives  46.6 us (32%)
  waiting for transfers between devices  41.5 us (28%)
  starting transfers between devices  40.5 us (28%)
  Pallas kernels  16.2 us (11%)
    ppermute x29, starting transfers between devices, shift(): return lax.ppermute(x, axis, [(i, (i + k) % n) for i in range(n)])  32.2 us
    all_to_all x1, blocking collectives, local(): recv = lax.all_to_all(send, SP, 0, 0, tiled=True)  28.2 us
    ppermute x29, waiting for transfers between devices, shift(): return lax.ppermute(x, axis, [(i, (i + k) % n) for i in range(n)])  24.2 us
    all_to_all x1, blocking collectives, local(): back = lax.all_to_all(summed.reshape(n_exp, cap, ch), SP, 0, 0, tiled=True)  18.3 us
    ppermute x3, waiting for transfers between devices, widen(): lax.ppermute(x, 'z', [(i, i ^ bit) for i in range(8)])  17.2 us
    pallas_call x13, Pallas kernels, call(): pl.pallas_call(body, out_shape=outs, in_specs=[SMEM if i < n_smem else AN...  16.2 us
    ppermute x1, starting transfers between devices, edges(): low = lax.ppermute(last, SP, [(i, i + 1) for i in range(n - 1)])  3.28 us
  transfers between devices with their start and end apart: 35, of which 16 were waited for; matrix products, arithmetic and copies ran while one was open for 0% of the time, Pallas kernels for 7%

commit v1 on v0

--- a/solution.py
+++ b/solution.py
@@ -49,7 +49,7 @@
 
 
 def shift(x, axis, n, k):
-    return lax.ppermute(x, axis, [(i, (i + k) % n) for i in range(n)])
+    return lax.ppermute(x, axis, [(i, i ^ k) for i in range(n)])
 
 
 def dispatch_kernel(x_ref, og_ref, w_ref, ids_ref, send_ref, sel_ref):
@@ -133,7 +133,7 @@
 
 
 def channels(y, d, core, ch):
-    return pl.multiple_of(ch * (2 * lax.rem(y + d, 4) + core), ch)
+    return pl.multiple_of(ch * (2 * (y ^ d) + core), ch)
 
 
 def own_half_kernel(y_ref, c_ref, d_ref, w_ref, mine_ref):
@@ -163,40 +163,43 @@
     gd_ref[...] = nn(hid_ref[...], dy_ref[...]).astype(BF)
 
 
-def combine_kernel(sel_ref, back_ref, og_ref, b_ref, dh_ref, first_ref, last_ref):
+def combine_kernel(xi_ref, sel_ref, back_ref, og_ref, b_ref, dh_ref, one_ref, two_ref):
     dh = (og_ref[...].astype(F32) + nn(sel_ref[...], back_ref[...])).astype(BF)
     dh_ref[...] = dh
     tok = dh.shape[0]
-    first_ref[0:1] = dh[:1]
-    first_ref[1:2] = b_ref[0:1]
-    last_ref[0:1] = dh[tok - 1 :]
-    last_ref[1:2] = b_ref[tok - 1 :]
-
-
-def stack_kernel(turned_ref, low_ref, high_ref, out_ref):
+    even = xi_ref[0] % 2 == 0
+    for k, source in enumerate((dh_ref, b_ref)):
+        first, last = source[0:1].astype(F32), source[tok - 1 :].astype(F32)
+        one_ref[k : k + 1] = jnp.where(even, last, first).astype(BF)
+        two_ref[k : k + 1] = jnp.where(even, first, last).astype(BF)
+
+
+def stack_kernel(turned_ref, dh_ref, low_ref, high_ref, out_ref):
     tok, ch = turned_ref.shape
     out_ref[:tok] = turned_ref[...]
+    out_ref[tok : 2 * tok] = dh_ref[...]
     row = lax.broadcasted_iota(jnp.int32, (16, ch), 0)
     low, high = low_ref[0:1].astype(F32), high_ref[0:1].astype(F32)
-    out_ref[tok:] = jnp.where(row == 0, low, jnp.where(row == 1, high, 0.0)).astype(BF)
+    out_ref[2 * tok :] = jnp.where(row == 0, low, jnp.where(row == 1, high, 0.0)).astype(BF)
 
 
 def mixer_kernel(
-    y_ref, c_ref, own_ref, part_ref, edge_own_ref, edge_part_ref, w_ref, b_ref, co_ref, bl_ref, bh_ref, t_ref, v_ref, g_ref,
+    y_ref, c_ref, xi_ref, own_ref, part_ref, w_ref, b_ref, co_ref, bl_ref, bh_ref, t_ref, v_ref, g_ref,
     gb_ref, gc_ref, gv_ref,
 ):
     y, c = y_ref[0], c_ref[0]
     tok, ch = b_ref.shape
-    size = edge_own_ref.shape[0] // 4
-    acc = jnp.zeros((size, ch), F32)
-    for d in range(4):
-        for ref, edge, core in ((own_ref, edge_own_ref, c), (part_ref, edge_part_ref, 1 - c)):
-            rows = jnp.concatenate([ref[d * tok : (d + 1) * tok], edge[d * size + tok : (d + 1) * size]], axis=0)
-            acc = acc + nn(rows, w_ref[pl.ds(channels(y, d, core, ch), ch), :])
+    size = own_ref.shape[0] // 4
+    acc = jnp.zeros((size - tok, ch), F32)
+    for d in range(4):
+        for ref, core in ((own_ref, c), (part_ref, 1 - c)):
+            acc = acc + nn(ref[d * size + tok : (d + 1) * size, :], w_ref[pl.ds(channels(y, d, core, ch), ch), :])
     gb_ref[...] = (acc[:tok] * co_ref[...].astype(F32)).astype(BF)
     dc = (acc[:tok] * b_ref[...].astype(F32)).astype(BF).astype(F32)
-    low = (acc[tok : tok + 1] * bl_ref[1:2].astype(F32)).astype(BF).astype(F32)
-    high = (acc[tok + 1 : tok + 2] * bh_ref[1:2].astype(F32)).astype(BF).astype(F32)
+    one = (acc[tok : tok + 1] * bl_ref[1:2].astype(F32)).astype(BF).astype(F32)
+    two = (acc[tok + 1 : tok + 2] * bh_ref[1:2].astype(F32)).astype(BF).astype(F32)
+    even = xi_ref[0] % 2 == 0
+    low, high = jnp.where(even, two, one), jnp.where(even, one, two)
     row = lax.broadcasted_iota(jnp.int32, dc.shape, 0)
     nxt = jnp.where(row == tok - 1, high, pltpu.roll(dc, tok - 1, 0))
     prv = jnp.where(row == 0, low, pltpu.roll(dc, 1, 0))
@@ -219,20 +222,20 @@
     o_s[...] = tn(a_s[...], b_s[...])
     rows = out_refs[0].shape[0]
     for k, ref in enumerate(out_refs):
-        ref[...] = o_s[pl.ds(pl.multiple_of(rows * lax.rem(xi_ref[0] + k, 4), rows), rows), :].astype(BF)
+        ref[...] = o_s[pl.ds(pl.multiple_of(rows * (xi_ref[0] ^ k), rows), rows), :].astype(BF)
 
 
 def over_tp(x):
-    parts = [x] + [shift(x, "y", 4, 4 - k) for k in (1, 2, 3)]
+    parts = [x] + [shift(x, "y", 4, k) for k in (1, 2, 3)]
     own = jnp.concatenate(parts, axis=0)
     return own, shift(own, "c", 2, 1)
 
 
-def edges(first, last):
+def edges(one, two):
     n = lax.axis_size(SP)
-    low = lax.ppermute(last, SP, [(i, i + 1) for i in range(n - 1)])
-    high = lax.ppermute(first, SP, [(i + 1, i) for i in range(n - 1)])
-    return low, high
+    one = lax.ppermute(one, SP, [(i, i ^ 1) for i in range(n)])
+    two = lax.ppermute(two, SP, [(i, i + 1 if i % 2 else i - 1) for i in range(1, n - 1)])
+    return one, two
 
 
 def widen(x, bit):
@@ -280,12 +283,12 @@
         scratch=[pltpu.SemaphoreType.DMA((3,))],
         any_args=(0, 1, 2),
     )
-    ax, by, w_pair, w_down = lax.optimization_barrier((ax, by, w_pair, w_down))
-    fx = shift(ax, "y", 4, 1)
-    fy = shift(by, "y", 4, 3)
+    bx, ay, w_pair, w_down = lax.optimization_barrier((bx, ay, w_pair, w_down))
+    fx = shift(bx, "y", 4, 1)
+    fy = shift(ay, "y", 4, 3)
     mix = widen(mix, 2)
     pieces = []
-    for px, py in ((hx, hy), (bx, by), (fx, fy), (ax, ay)):
+    for px, py in ((hx, hy), (ax, ay), (fx, fy), (bx, by)):
         pieces += [px, py, shift(px, "c", 2, 1), shift(py, "c", 2, 1)]
     mix = widen(mix, 1)
     theirs, xin, dyin, hidden, dgu, dgu_rows = call(
@@ -313,20 +316,19 @@
     parts, mix, gate_t, up_t, grad_down = lax.optimization_barrier((parts, mix, gate_t, up_t, grad_down))
     (summed,) = call(sum_kernel, [(total, ch)], 0, (pair[0], *parts))
     back = lax.all_to_all(summed.reshape(n_exp, cap, ch), SP, 0, 0, tiled=True)
-    dh, first, last = call(
-        combine_kernel, [(tok, ch), (2, ch), (2, ch)], 0, (sel, back.reshape(total, ch), out_grad, gate_b)
+    dh, one, two = call(
+        combine_kernel, [(tok, ch), (2, ch), (2, ch)], 1, (xi, sel, back.reshape(total, ch), out_grad, gate_b)
     )
     swap = [(z * 8 + y * 2 + c, (y * 2 + c) * 8 + z) for z in range(8) for y in range(4) for c in range(2)]
     turned = lax.ppermute(dh, ("z", "y", "c"), swap)
-    low, high = edges(first, last)
-    h_own, h_part = over_tp(dh)
-    (stack,) = call(stack_kernel, [(tok + 16, ch)], 0, (turned, low, high))
-    t_own, t_part = over_tp(stack)
+    one, two = edges(one, two)
+    (stack,) = call(stack_kernel, [(2 * tok + 16, ch)], 0, (turned, dh, one, two))
+    own, part = over_tp(stack)
     terms = call(
         outer_kernel,
         [(ch // 4, ch)] * 4,
         4,
-        (yi, ci, zi, xi, t_own, t_part, mix),
+        (yi, ci, zi, xi, own, part, mix),
         scratch=[pltpu.VMEM((8 * tok, ch), BF)] * 2 + [pltpu.VMEM((ch, ch), F32)],
         flops=16 * tok * ch * ch,
     )
@@ -334,8 +336,8 @@
     grad_b, grad_c, grad_v = call(
         mixer_kernel,
         [(tok, ch)] * 3,
-        2,
-        (yi, ci, h_own, h_part, t_own, t_part, out_proj, gate_b, conv_out, low, high, conv_taps, value_v, gate_c),
+        3,
+        (yi, ci, xi, own, part, out_proj, gate_b, conv_out, one, two, conv_taps, value_v, gate_c),
         flops=2 * tok * d * ch,
         hbm_outs=(0, 1, 2),
     )

time: 147 us -> 145 us (0.986)
  waiting for transfers between devices: 41.5 us -> 52.1 us
  starting transfers between devices: 40.5 us -> 30.3 us
  blocking collectives: 46.6 us -> 44.6 us
    ppermute x31 -> x27, starting transfers between devices: 38 us -> 27.8 us  [the longest x25 23.1 us: shift(): return lax.ppermute(x, axis, [(i, i ^ k) for i in range(n)])]
    ppermute x31 -> x27, waiting for transfers between devices: 24.2 us -> 33.3 us  [the longest x25 30.3 us: shift(): return lax.ppermute(x, axis, [(i, i ^ k) for i in range(n)])]
    all_to_all x1, blocking collectives: 18.3 us -> 16.3 us  [local(): back = lax.all_to_all(summed.reshape(n_exp, cap, ch), SP, 0, 0, tiled=True)]
    ppermute x3, waiting for transfers between devices: 17.2 us -> 18.8 us  [widen(): lax.ppermute(x, 'z', [(i, i ^ bit) for i in range(8)])]
  transfers between devices with their start and end apart: 35 -> 31, of which waited for: 16 -> 19; matrix products, arithmetic and copies ran while one was open for 0% -> 0% of each run, Pallas kernels for 7% -> 6%
where the time goes in v1:
time: 145 us; the launch traced here: 144 us
  waiting for transfers between devices  52.1 us (36%)
  blocking collectives  44.6 us (31%)
  starting transfers between devices  30.3 us (21%)
  Pallas kernels  16.2 us (11%)
    ppermute x25, waiting for transfers between devices, shift(): return lax.ppermute(x, axis, [(i, i ^ k) for i in range(n)])  30.3 us
    all_to_all x1, blocking collectives, local(): recv = lax.all_to_all(send, SP, 0, 0, tiled=True)  28.3 us
    ppermute x25, starting transfers between devices, shift(): return lax.ppermute(x, axis, [(i, i ^ k) for i in range(n)])  23.1 us
    ppermute x3, waiting for transfers between devices, widen(): lax.ppermute(x, 'z', [(i, i ^ bit) for i in range(8)])  18.8 us
    all_to_all x1, blocking collectives, local(): back = lax.all_to_all(summed.reshape(n_exp, cap, ch), SP, 0, 0, tiled=True)  16.3 us
    pallas_call x13, Pallas kernels, call(): pl.pallas_call(body, out_shape=outs, in_specs=[SMEM if i < n_smem else AN...  16.2 us
    ppermute x1, waiting for transfers between devices, edges(): lax.ppermute(two, SP, [(i, i + 1 if i % 2 else i - 1) for i in range(1, n...  3.06 us
  transfers between devices with their start and end apart: 31, of which 19 were waited for; matrix products, arithmetic and copies ran while one was open for 0% of the time, Pallas kernels for 6%

profile of v1, /device:TPU:2, one launch (start us, length us, event | category | flops | bytes accessed | tf_op | source)
XLA Modules:
  0.0 144.2 jit_solution(11357983240973326895)
XLA Ops:
  0.6 1.4 shard_map.180
  2.0 28.3 %all_to_all.10 = bf16[32,32,256]{2,1,0:T(8,128)(2,1)S(1)} all-to-all(bf16[32,32,256]{2,1,0:T(8,128)(2,1)S(1)} %get-tuple-element.59), channel_id=1, replica_groups=mesh['z'=8,'x'=4,'y'=4,'c'=2] {'z','x'}, dimensions={0} | all-to-all | bytes 1048576 | tf_op jit(solution)/shard_map/all_to_all | solution.py:265
  30.3 3.1 %collective-permute-start.3 = (bf16[512,256]{1,0:T(8,128)(2,1)S(1)}, bf16[512,256]{1,0:T(8,128)(2,1)S(1)}, u32[]{:S(2)}, u32[]{:S(2)}) collective-permute-start(bf16[512,256]{1,0:T(8,128)(2,1)S(1)} %bitcast.30), channel_id=1, source_target_pairs={{0,6},{2,4},{4,2},{6,0},{1,7},{3,5},{5,3},{7,1},{8,14},{10,12},{12... | collective-permute-start | bytes 786440 | tf_op jit(solution)/shard_map/ppermute | solution.py:52
  33.4 0.1 collective-permute-start.4
  33.6 1.1 collective-permute-start.11
  34.6 0.8 collective-permute-start.2
  35.5 2.3 %shard_map.181 = (bf16[704,2048]{1,0:T(8,128)(2,1)S(1)}, bf16[352,2048]{1,0:T(8,128)(2,1)S(1)}) custom-call(bf16[352,2048]{1,0:T(8,128)(2,1)} %bitcast.34, bf16[352,2048]{1,0:T(8,128)(2,1)} %bitcast.35, bf16[352,2048]{1,0:T(8,128)(2,1)} %bitcast.36), custom_call_target="tpu_custom_call" | custom-call | tf_op jit(solution)/shard_map/pallas_call | solution.py:28
  37.7 3.1 %collective-permute-done.3.refs_12_ = bf16[512,256]{1,0:T(8,128)(2,1)S(1)} collective-permute-done((bf16[512,256]{1,0:T(8,128)(2,1)S(1)}, bf16[512,256]{1,0:T(8,128)(2,1)S(1)}, u32[]{:S(2)}, u32[]{:S(2)}) %collective-permute-start.3) | collective-permute-done | bytes 262176 | tf_op jit(solution)/shard_map/ppermute | solution.py:52
  40.8 1.8 %collective-permute-done.4.refs_5_ = bf16[512,256]{1,0:T(8,128)(2,1)S(1)} collective-permute-done((bf16[512,256]{1,0:T(8,128)(2,1)S(1)}, bf16[512,256]{1,0:T(8,128)(2,1)S(1)}, u32[]{:S(2)}, u32[]{:S(2)}) %collective-permute-start.4) | collective-permute-done | bytes 262176 | tf_op jit(solution)/shard_map/ppermute | solution.py:52
  42.6 1.2 collective-permute-start.8
  43.8 0.2 collective-permute-done.11.refs_13_
  44.1 0.4 collective-permute-start.7
  44.4 1.1 collective-permute-done.2.refs_4_
  45.5 0.5 collective-permute-start.6
  46.0 0.1 collective-permute-start.13
  46.1 4.7 %collective-permute-done.8.refs_9_ = bf16[512,256]{1,0:T(8,128)(2,1)S(1)} collective-permute-done((bf16[512,256]{1,0:T(8,128)(2,1)S(1)}, bf16[512,256]{1,0:T(8,128)(2,1)S(1)}, u32[]{:S(2)}, u32[]{:S(2)}) %collective-permute-start.8) | collective-permute-done | bytes 262176 | tf_op jit(solution)/shard_map/ppermute | solution.py:52
  50.8 1.5 %collective-permute-done.7.refs_8_ = bf16[512,256]{1,0:T(8,128)(2,1)S(1)} collective-permute-done((bf16[512,256]{1,0:T(8,128)(2,1)S(1)}, bf16[512,256]{1,0:T(8,128)(2,1)S(1)}, u32[]{:S(2)}, u32[]{:S(2)}) %collective-permute-start.7) | collective-permute-done | bytes 262176 | tf_op jit(solution)/shard_map/ppermute | solution.py:52
  52.3 0.5 collective-permute-start.9
  52.8 1.0 collective-permute-done.10.refs_11_
  53.8 0.4 collective-permute-done.9.refs_10_
  54.2 4.1 %shard_map.182 = (bf16[4,512,256]{2,1,0:T(8,128)(2,1)S(1)}, bf16[512,2048]{1,0:T(8,128)(2,1)S(1)}, bf16[512,2048]{1,0:T(8,128)(2,1)S(1)}, bf16[352,512]{1,0:T(8,...) custom-call(s32[1]{0:T(128)} %bitcast.y_ref, s32[1]{0:T(128)} %bitcast.1.c_ref, ...), custom_call_target="tpu_custom_call" | custom-call | flops 2952790016 | tf_op jit(solution)/shard_map/pallas_call | solution.py:28
  58.3 0.4 collective-permute-start.14
  58.7 0.9 shard_map.185
  59.6 1.7 %collective-permute-start.18 = (bf16[128,256]{1,0:T(8,128)(2,1)S(1)}, bf16[128,256]{1,0:T(8,128)(2,1)S(1)}, u32[]{:S(2)}, u32[]{:S(2)}) collective-permute-start(bf16[128,256]{1,0:T(8,128)(2,1)S(1)} %shard_map.185), channel_id=1, source_target_pairs={{0,128},{32,160},{64,192},{96,224},{128,0},{160,32},{192,64},{224,... | collective-permute-start | bytes 196616 | tf_op jit(solution)/shard_map/ppermute | solution.py:242
  61.3 7.6 %collective-permute-done.18 = bf16[128,256]{1,0:T(8,128)(2,1)S(1)} collective-permute-done((bf16[128,256]{1,0:T(8,128)(2,1)S(1)}, bf16[128,256]{1,0:T(8,128)(2,1)S(1)}, u32[]{:S(2)}, u32[]{:S(2)}) %collective-permute-start.18) | collective-permute-done | bytes 65568 | tf_op jit(solution)/shard_map/ppermute | solution.py:242
  68.8 0.1 collective-permute-start.19
  68.9 8.8 %collective-permute-done.19 = bf16[256,256]{1,0:T(8,128)(2,1)S(1)} collective-permute-done((bf16[256,256]{1,0:T(8,128)(2,1)S(1)}, bf16[256,256]{1,0:T(8,128)(2,1)S(1)}, u32[]{:S(2)}, u32[]{:S(2)}) %collective-permute-start.19) | collective-permute-done | bytes 131104 | tf_op jit(solution)/shard_map/ppermute | solution.py:242
  77.8 0.1 collective-permute-start.20
  77.9 1.0 shard_map.183.mine_ref
  78.9 0.2 shard_map.184
  79.2 0.4 collective-permute-start.15
  79.6 1.1 collective-permute-start.16
  80.7 2.7 %collective-permute-start.17 = (bf16[512,256]{1,0:T(8,128)(2,1)S(1)}, bf16[512,256]{1,0:T(8,128)(2,1)S(1)}, u32[]{:S(2)}, u32[]{:S(2)}) collective-permute-start(bf16[512,256]{1,0:T(8,128)(2,1)S(1)} %get-tuple-element.74), channel_id=1, source_target_pairs={{0,4},{2,6},{4,0},{6,2},{1,5},{3,7},{5,1},{7,3},{8,12},{10,14},{12... | collective-permute-start | bytes 786440 | tf_op jit(solution)/shard_map/ppermute | solution.py:52
  83.3 2.4 %collective-permute-done.20 = bf16[512,256]{1,0:T(8,128)(2,1)S(1)} collective-permute-done((bf16[512,256]{1,0:T(8,128)(2,1)S(1)}, bf16[512,256]{1,0:T(8,128)(2,1)S(1)}, u32[]{:S(2)}, u32[]{:S(2)}) %collective-permute-start.20) | collective-permute-done | bytes 262176 | tf_op jit(solution)/shard_map/ppermute | solution.py:242
  85.8 3.8 %shard_map.186 = (bf16[352,2048]{1,0:T(8,128)(2,1)}, bf16[352,2048]{1,0:T(8,128)(2,1)}, bf16[352,2048]{1,0:T(8,128)(2,1)}) custom-call(bf16[512,2048]{1,0:T(8,128)(2,1)S(1)} %get-tuple-element.77.x_ref, bf16[512,2048]{1,0:T(8,128)(2,1)S(1)} %get-tuple-element.78.dy_ref, bf16[352,512]{1,0:T(8,128)(2,1)S(1)} %get-tuple-element.79.hid_ref, ...), custom_call_target="tpu_custom_call" | custom-call | flops 2214592512 | tf_op jit(solution)/shard_map/pallas_call | solution.py:28
  89.6 4.5 %collective-permute-done.16.refs_2_ = bf16[512,256]{1,0:T(8,128)(2,1)S(1)} collective-permute-done((bf16[512,256]{1,0:T(8,128)(2,1)S(1)}, bf16[512,256]{1,0:T(8,128)(2,1)S(1)}, u32[]{:S(2)}, u32[]{:S(2)}) %collective-permute-start.16) | collective-permute-done | bytes 262176 | tf_op jit(solution)/shard_map/ppermute | solution.py:52
  94.0 0.1 shard_map.187
  94.2 16.3 %all_to_all.11 = bf16[32,16,256]{2,1,0:T(8,128)(2,1)S(1)} all-to-all(bf16[32,16,256]{2,1,0:T(8,128)(2,1)S(1)} %bitcast.24), channel_id=1, replica_groups=mesh['z'=8,'x'=4,'y'=4,'c'=2] {'z','x'}, dimensions={0} | all-to-all | bytes 524288 | tf_op jit(solution)/shard_map/all_to_all | solution.py:318
  110.5 0.2 shard_map.188
  110.7 0.7 collective-permute-start.21
  111.4 2.3 %collective-permute-start.22 = (bf16[2,256]{1,0:T(2,128)(2,1)S(1)}, bf16[2,256]{1,0:T(2,128)(2,1)S(1)}, u32[]{:S(2)}, u32[]{:S(2)}) collective-permute-start(bf16[2,256]{1,0:T(2,128)(2,1)S(1)} %get-tuple-element.95), channel_id=1, source_target_pairs={{0,8},{8,0},{16,24},{24,16},{32,40},{40,32},{48,56},{56,48},{64,72... | collective-permute-start | bytes 3080 | tf_op jit(solution)/shard_map/ppermute | solution.py:236
  113.7 2.4 %collective-permute-start.23 = (bf16[2,256]{1,0:T(2,128)(2,1)S(1)}, bf16[2,256]{1,0:T(2,128)(2,1)S(1)}, u32[]{:S(2)}, u32[]{:S(2)}) collective-permute-start(bf16[2,256]{1,0:T(2,128)(2,1)S(1)} %get-tuple-element.96), channel_id=1, source_target_pairs={{8,16},{16,8},{24,32},{32,24},{40,48},{48,40},{56,64},{64,56},{72,... | collective-permute-start | bytes 3080 | tf_op jit(solution)/shard_map/ppermute | solution.py:237
  116.1 3.1 %collective-permute-done.23.high_ref.bh_ref = bf16[2,256]{1,0:T(2,128)(2,1)S(1)} collective-permute-done((bf16[2,256]{1,0:T(2,128)(2,1)S(1)}, bf16[2,256]{1,0:T(2,128)(2,1)S(1)}, u32[]{:S(2)}, u32[]{:S(2)}) %collective-permute-start.23) | collective-permute-done | bytes 1056 | tf_op jit(solution)/shard_map/ppermute | solution.py:237
  119.2 0.0 copy-start
  119.2 0.0 copy-start.2
  119.2 0.0 copy-start.4
  119.2 0.0 copy-start.5
  119.2 0.0 copy-start.6
  119.2 3.7 %collective-permute-start.24 = (bf16[272,256]{1,0:T(8,128)(2,1)S(1)}, bf16[272,256]{1,0:T(8,128)(2,1)S(1)}, u32[]{:S(2)}, u32[]{:S(2)}) collective-permute-start(bf16[272,256]{1,0:T(8,128)(2,1)S(1)} %shard_map.189), channel_id=1, source_target_pairs={{0,2},{2,0},{4,6},{6,4},{1,3},{3,1},{5,7},{7,5},{8,10},{10,8},{12,... | collective-permute-start | bytes 417800 | tf_op jit(solution)/shard_map/ppermute | solution.py:52
  122.9 2.5 %collective-permute-start.25 = (bf16[272,256]{1,0:T(8,128)(2,1)S(1)}, bf16[272,256]{1,0:T(8,128)(2,1)S(1)}, u32[]{:S(2)}, u32[]{:S(2)}) collective-permute-start(bf16[272,256]{1,0:T(8,128)(2,1)S(1)} %shard_map.189), channel_id=1, source_target_pairs={{0,4},{2,6},{4,0},{6,2},{1,5},{3,7},{5,1},{7,3},{8,12},{10,14},{12... | collective-permute-start | bytes 417800 | tf_op jit(solution)/shard_map/ppermute | solution.py:52
  125.4 0.3 collective-permute-start.26
  125.7 1.2 collective-permute-done.24
  126.8 3.8 %collective-permute-done.25 = bf16[272,256]{1,0:T(8,128)(2,1)S(1)} collective-permute-done((bf16[272,256]{1,0:T(8,128)(2,1)S(1)}, bf16[272,256]{1,0:T(8,128)(2,1)S(1)}, u32[]{:S(2)}, u32[]{:S(2)}) %collective-permute-start.25) | collective-permute-done | bytes 139296 | tf_op jit(solution)/shard_map/ppermute | solution.py:52
  130.6 1.6 %collective-permute-done.26 = bf16[272,256]{1,0:T(8,128)(2,1)S(1)} collective-permute-done((bf16[272,256]{1,0:T(8,128)(2,1)S(1)}, bf16[272,256]{1,0:T(8,128)(2,1)S(1)}, u32[]{:S(2)}, u32[]{:S(2)}) %collective-permute-start.26) | collective-permute-done | bytes 139296 | tf_op jit(solution)/shard_map/ppermute | solution.py:52
  132.3 0.1 collective-permute-start.27
  132.4 1.9 %collective-permute-done.27.part_ref = bf16[1088,256]{1,0:T(8,128)(2,1)S(1)} collective-permute-done((bf16[1088,256]{1,0:T(8,128)(2,1)S(1)}, bf16[1088,256]{1,0:T(8,128)(2,1)S(1)}, u32[]{:S(2)}, u32[]{:S(2)}) %collective-permute-start.27) | collective-permute-done | bytes 557088 | tf_op jit(solution)/shard_map/ppermute | solution.py:52
  134.3 0.4 shard_map.190
  134.7 1.2 collective-permute-start.28
  136.0 2.2 %collective-permute-start.29 = (bf16[64,256]{1,0:T(8,128)(2,1)S(1)}, bf16[64,256]{1,0:T(8,128)(2,1)S(1)}, u32[]{:S(2)}, u32[]{:S(2)}) collective-permute-start(bf16[64,256]{1,0:T(8,128)(2,1)S(1)} %get-tuple-element.100), channel_id=1, source_target_pairs={{0,24},{8,16},{16,8},{24,0},{1,25},{9,17},{17,9},{25,1},{2,26},{10... | collective-permute-start | bytes 98312 | tf_op jit(solution)/shard_map/ppermute | solution.py:52
  138.1 0.8 collective-permute-start.30
  138.9 1.1 shard_map.192
  140.0 0.1 collective-permute-done.29.refs_2_
  140.0 3.5 %collective-permute-done.30.refs_3_ = bf16[64,256]{1,0:T(8,128)(2,1)S(1)} collective-permute-done((bf16[64,256]{1,0:T(8,128)(2,1)S(1)}, bf16[64,256]{1,0:T(8,128)(2,1)S(1)}, u32[]{:S(2)}, u32[]{:S(2)}) %collective-permute-start.30) | collective-permute-done | bytes 32800 | tf_op jit(solution)/shard_map/ppermute | solution.py:52
  143.6 0.6 shard_map.191
  (32 shorter events, 0.2 us)
Async XLA Ops:
  30.3 10.5 %collective-permute-start.3 = (bf16[512,256]{1,0:T(8,128)(2,1)S(1)}, bf16[512,256]{1,0:T(8,128)(2,1)S(1)}, u32[]{:S(2)}, u32[]{:S(2)}) collective-permute-start(bf16[512,256]{1,0:T(8,128)(2,1)S(1)} %bitcast.30), channel_id=1, source_target_pairs={{0,6},{2,4},{4,2},{6,0},{1,7},{3,5},{5,3},{7,1},{8,14},{10,12},{12... | collective-permute-start | bytes 786440 | tf_op jit(solution)/shard_map/ppermute | solution.py:52
  33.4 9.2 %collective-permute-start.4 = (bf16[512,256]{1,0:T(8,128)(2,1)S(1)}, bf16[512,256]{1,0:T(8,128)(2,1)S(1)}, u32[]{:S(2)}, u32[]{:S(2)}) collective-permute-start(bf16[512,256]{1,0:T(8,128)(2,1)S(1)} %bitcast.26), channel_id=1, source_target_pairs={{0,2},{2,0},{4,6},{6,4},{1,3},{3,1},{5,7},{7,5},{8,10},{10,8},{12,... | collective-permute-start | bytes 786440 | tf_op jit(solution)/shard_map/ppermute | solution.py:52
  33.6 10.5 %collective-permute-start.11 = (bf16[512,256]{1,0:T(8,128)(2,1)S(1)}, bf16[512,256]{1,0:T(8,128)(2,1)S(1)}, u32[]{:S(2)}, u32[]{:S(2)}) collective-permute-start(bf16[512,256]{1,0:T(8,128)(2,1)S(1)} %bitcast.27), channel_id=1, source_target_pairs={{0,6},{2,4},{4,2},{6,0},{1,7},{3,5},{5,3},{7,1},{8,14},{10,12},{12... | collective-permute-start | bytes 786440 | tf_op jit(solution)/shard_map/ppermute | solution.py:52
  34.6 10.9 %collective-permute-start.2 = (bf16[512,256]{1,0:T(8,128)(2,1)S(1)}, bf16[512,256]{1,0:T(8,128)(2,1)S(1)}, u32[]{:S(2)}, u32[]{:S(2)}) collective-permute-start(bf16[512,256]{1,0:T(8,128)(2,1)S(1)} %bitcast.31), channel_id=1, source_target_pairs={{0,2},{2,0},{4,6},{6,4},{1,3},{3,1},{5,7},{7,5},{8,10},{10,8},{12,... | collective-permute-start | bytes 786440 | tf_op jit(solution)/shard_map/ppermute | solution.py:52
  35.4 10.1 %collective-permute-start = (bf16[512,256]{1,0:T(8,128)(2,1)S(1)}, bf16[512,256]{1,0:T(8,128)(2,1)S(1)}, u32[]{:S(2)}, u32[]{:S(2)}) collective-permute-start(bf16[512,256]{1,0:T(8,128)(2,1)S(1)} %bitcast.32), channel_id=1, source_target_pairs={{0,1},{1,0},{2,3},{3,2},{4,5},{5,4},{6,7},{7,6},{8,9},{9,8},{10,11... | collective-permute-start | bytes 786440 | tf_op jit(solution)/shard_map/ppermute | solution.py:52
  40.8 5.2 %collective-permute-start.1 = (bf16[512,256]{1,0:T(8,128)(2,1)S(1)}, bf16[512,256]{1,0:T(8,128)(2,1)S(1)}, u32[]{:S(2)}, u32[]{:S(2)}) collective-permute-start(bf16[512,256]{1,0:T(8,128)(2,1)S(1)} %bitcast.28), channel_id=1, source_target_pairs={{0,1},{1,0},{2,3},{3,2},{4,5},{5,4},{6,7},{7,6},{8,9},{9,8},{10,11... | collective-permute-start | bytes 786440 | tf_op jit(solution)/shard_map/ppermute | solution.py:52
  42.6 8.2 %collective-permute-start.8 = (bf16[512,256]{1,0:T(8,128)(2,1)S(1)}, bf16[512,256]{1,0:T(8,128)(2,1)S(1)}, u32[]{:S(2)}, u32[]{:S(2)}) collective-permute-start(bf16[512,256]{1,0:T(8,128)(2,1)S(1)} %collective-permute-done.4.refs_5_), channel_id=1, source_target_pairs={{0,6},{2,4},{4,2},{6,0},{1,7},{3,5},{5,3},{7,1},{8,14},{10,12},{12... | collective-permute-start | bytes 786440 | tf_op jit(solution)/shard_map/ppermute | solution.py:52
  44.1 8.2 %collective-permute-start.7 = (bf16[512,256]{1,0:T(8,128)(2,1)S(1)}, bf16[512,256]{1,0:T(8,128)(2,1)S(1)}, u32[]{:S(2)}, u32[]{:S(2)}) collective-permute-start(bf16[512,256]{1,0:T(8,128)(2,1)S(1)} %collective-permute-done.3.refs_12_), channel_id=1, source_target_pairs={{0,2},{2,0},{4,6},{6,4},{1,3},{3,1},{5,7},{7,5},{8,10},{10,8},{12,... | collective-permute-start | bytes 786440 | tf_op jit(solution)/shard_map/ppermute | solution.py:52
  45.5 6.7 %collective-permute-start.12 = (bf16[512,256]{1,0:T(8,128)(2,1)S(1)}, bf16[512,256]{1,0:T(8,128)(2,1)S(1)}, u32[]{:S(2)}, u32[]{:S(2)}) collective-permute-start(bf16[512,256]{1,0:T(8,128)(2,1)S(1)} %collective-permute-done.3.refs_12_), channel_id=1, source_target_pairs={{0,1},{1,0},{2,3},{3,2},{4,5},{5,4},{6,7},{7,6},{8,9},{9,8},{10,11... | collective-permute-start | bytes 786440 | tf_op jit(solution)/shard_map/ppermute | solution.py:52
  45.5 7.3 %collective-permute-start.6 = (bf16[512,256]{1,0:T(8,128)(2,1)S(1)}, bf16[512,256]{1,0:T(8,128)(2,1)S(1)}, u32[]{:S(2)}, u32[]{:S(2)}) collective-permute-start(bf16[512,256]{1,0:T(8,128)(2,1)S(1)} %collective-permute-done.4.refs_5_), channel_id=1, source_target_pairs={{0,1},{1,0},{2,3},{3,2},{4,5},{5,4},{6,7},{7,6},{8,9},{9,8},{10,11... | collective-permute-start | bytes 786440 | tf_op jit(solution)/shard_map/ppermute | solution.py:52
  46.0 6.7 %collective-permute-start.13 = (bf16[512,256]{1,0:T(8,128)(2,1)S(1)}, bf16[512,256]{1,0:T(8,128)(2,1)S(1)}, u32[]{:S(2)}, u32[]{:S(2)}) collective-permute-start(bf16[512,256]{1,0:T(8,128)(2,1)S(1)} %collective-permute-done.11.refs_13_), channel_id=1, source_target_pairs={{0,1},{1,0},{2,3},{3,2},{4,5},{5,4},{6,7},{7,6},{8,9},{9,8},{10,11... | collective-permute-start | bytes 786440 | tf_op jit(solution)/shard_map/ppermute | solution.py:52
  50.8 2.0 %collective-permute-start.5 = (bf16[512,256]{1,0:T(8,128)(2,1)S(1)}, bf16[512,256]{1,0:T(8,128)(2,1)S(1)}, u32[]{:S(2)}, u32[]{:S(2)}) collective-permute-start(bf16[512,256]{1,0:T(8,128)(2,1)S(1)} %collective-permute-done.2.refs_4_), channel_id=1, source_target_pairs={{0,1},{1,0},{2,3},{3,2},{4,5},{5,4},{6,7},{7,6},{8,9},{9,8},{10,11... | collective-permute-start | bytes 786440 | tf_op jit(solution)/shard_map/ppermute | solution.py:52
  52.3 1.5 %collective-permute-start.10 = (bf16[512,256]{1,0:T(8,128)(2,1)S(1)}, bf16[512,256]{1,0:T(8,128)(2,1)S(1)}, u32[]{:S(2)}, u32[]{:S(2)}) collective-permute-start(bf16[512,256]{1,0:T(8,128)(2,1)S(1)} %collective-permute-done.8.refs_9_), channel_id=1, source_target_pairs={{0,1},{1,0},{2,3},{3,2},{4,5},{5,4},{6,7},{7,6},{8,9},{9,8},{10,11... | collective-permute-start | bytes 786440 | tf_op jit(solution)/shard_map/ppermute | solution.py:52
  52.3 1.9 %collective-permute-start.9 = (bf16[512,256]{1,0:T(8,128)(2,1)S(1)}, bf16[512,256]{1,0:T(8,128)(2,1)S(1)}, u32[]{:S(2)}, u32[]{:S(2)}) collective-permute-start(bf16[512,256]{1,0:T(8,128)(2,1)S(1)} %collective-permute-done.7.refs_8_), channel_id=1, source_target_pairs={{0,1},{1,0},{2,3},{3,2},{4,5},{5,4},{6,7},{7,6},{8,9},{9,8},{10,11... | collective-permute-start | bytes 786440 | tf_op jit(solution)/shard_map/ppermute | solution.py:52
  58.3 20.6 %collective-permute-start.14 = (bf16[4,512,256]{2,1,0:T(8,128)(2,1)S(1)}, bf16[4,512,256]{2,1,0:T(8,128)(2,1)S(1)}, u32[]{:S(2)}, u32[]{:S(2)}) collective-permute-start(bf16[4,512,256]{2,1,0:T(8,128)(2,1)S(1)} %get-tuple-element.71), channel_id=1, source_target_pairs={{0,1},{1,0},{2,3},{3,2},{4,5},{5,4},{6,7},{7,6},{8,9},{9,8},{10,11... | collective-permute-start | bytes 3145736 | tf_op jit(solution)/shard_map/ppermute | solution.py:52
  59.6 9.2 %collective-permute-start.18 = (bf16[128,256]{1,0:T(8,128)(2,1)S(1)}, bf16[128,256]{1,0:T(8,128)(2,1)S(1)}, u32[]{:S(2)}, u32[]{:S(2)}) collective-permute-start(bf16[128,256]{1,0:T(8,128)(2,1)S(1)} %shard_map.185), channel_id=1, source_target_pairs={{0,128},{32,160},{64,192},{96,224},{128,0},{160,32},{192,64},{224,... | collective-permute-start | bytes 196616 | tf_op jit(solution)/shard_map/ppermute | solution.py:242
  68.8 8.9 %collective-permute-start.19 = (bf16[256,256]{1,0:T(8,128)(2,1)S(1)}, bf16[256,256]{1,0:T(8,128)(2,1)S(1)}, u32[]{:S(2)}, u32[]{:S(2)}) collective-permute-start(bf16[256,256]{1,0:T(8,128)(2,1)S(1)} %pad_maximum_fusion.3), channel_id=1, source_target_pairs={{0,64},{32,96},{64,0},{96,32},{128,192},{160,224},{192,128},{224,1... | collective-permute-start | bytes 393224 | tf_op jit(solution)/shard_map/ppermute | solution.py:242
  77.8 7.9 %collective-permute-start.20 = (bf16[512,256]{1,0:T(8,128)(2,1)S(1)}, bf16[512,256]{1,0:T(8,128)(2,1)S(1)}, u32[]{:S(2)}, u32[]{:S(2)}) collective-permute-start(bf16[512,256]{1,0:T(8,128)(2,1)S(1)} %pad_maximum_fusion.2), channel_id=1, source_target_pairs={{0,32},{32,0},{64,96},{96,64},{128,160},{160,128},{192,224},{224,1... | collective-permute-start | bytes 786440 | tf_op jit(solution)/shard_map/ppermute | solution.py:242
  79.2 10.4 %collective-permute-start.15 = (bf16[512,256]{1,0:T(8,128)(2,1)S(1)}, bf16[512,256]{1,0:T(8,128)(2,1)S(1)}, u32[]{:S(2)}, u32[]{:S(2)}) collective-permute-start(bf16[512,256]{1,0:T(8,128)(2,1)S(1)} %get-tuple-element.72), channel_id=1, source_target_pairs={{0,2},{2,0},{4,6},{6,4},{1,3},{3,1},{5,7},{7,5},{8,10},{10,8},{12,... | collective-permute-start | bytes 786440 | tf_op jit(solution)/shard_map/ppermute | solution.py:52
  79.6 14.5 %collective-permute-start.16 = (bf16[512,256]{1,0:T(8,128)(2,1)S(1)}, bf16[512,256]{1,0:T(8,128)(2,1)S(1)}, u32[]{:S(2)}, u32[]{:S(2)}) collective-permute-start(bf16[512,256]{1,0:T(8,128)(2,1)S(1)} %get-tuple-element.73), channel_id=1, source_target_pairs={{0,6},{2,4},{4,2},{6,0},{1,7},{3,5},{5,3},{7,1},{8,14},{10,12},{12... | collective-permute-start | bytes 786440 | tf_op jit(solution)/shard_map/ppermute | solution.py:52
  80.7 13.4 %collective-permute-start.17 = (bf16[512,256]{1,0:T(8,128)(2,1)S(1)}, bf16[512,256]{1,0:T(8,128)(2,1)S(1)}, u32[]{:S(2)}, u32[]{:S(2)}) collective-permute-start(bf16[512,256]{1,0:T(8,128)(2,1)S(1)} %get-tuple-element.74), channel_id=1, source_target_pairs={{0,4},{2,6},{4,0},{6,2},{1,5},{3,7},{5,1},{7,3},{8,12},{10,14},{12... | collective-permute-start | bytes 786440 | tf_op jit(solution)/shard_map/ppermute | solution.py:52
  89.6 20.9 %copy-start.1 = (bf16[128,256]{1,0:T(8,128)(2,1)S(1)}, bf16[128,256]{1,0:T(8,128)(2,1)}, u32[]{:S(2)}) copy-start(bf16[128,256]{1,0:T(8,128)(2,1)} %b_ref.2) | copy-start | bytes 196612
  89.6 20.9 %copy-start.3 = (bf16[128,256]{1,0:T(8,128)(2,1)S(1)}, bf16[128,256]{1,0:T(8,128)(2,1)}, u32[]{:S(2)}) copy-start(bf16[128,256]{1,0:T(8,128)(2,1)} %og_ref.3) | copy-start | bytes 196612
  110.7 8.4 %collective-permute-start.21 = (bf16[128,256]{1,0:T(8,128)(2,1)S(1)}, bf16[128,256]{1,0:T(8,128)(2,1)S(1)}, u32[]{:S(2)}, u32[]{:S(2)}) collective-permute-start(bf16[128,256]{1,0:T(8,128)(2,1)S(1)} %get-tuple-element.94.dh_ref), channel_id=1, source_target_pairs={{0,0},{1,32},{2,64},{3,96},{4,128},{5,160},{6,192},{7,224},{32,1},... | collective-permute-start | bytes 196616 | tf_op jit(solution)/shard_map/ppermute | solution.py:323
  111.4 4.7 %collective-permute-start.22 = (bf16[2,256]{1,0:T(2,128)(2,1)S(1)}, bf16[2,256]{1,0:T(2,128)(2,1)S(1)}, u32[]{:S(2)}, u32[]{:S(2)}) collective-permute-start(bf16[2,256]{1,0:T(2,128)(2,1)S(1)} %get-tuple-element.95), channel_id=1, source_target_pairs={{0,8},{8,0},{16,24},{24,16},{32,40},{40,32},{48,56},{56,48},{64,72... | collective-permute-start | bytes 3080 | tf_op jit(solution)/shard_map/ppermute | solution.py:236
  113.7 5.5 %collective-permute-start.23 = (bf16[2,256]{1,0:T(2,128)(2,1)S(1)}, bf16[2,256]{1,0:T(2,128)(2,1)S(1)}, u32[]{:S(2)}, u32[]{:S(2)}) collective-permute-start(bf16[2,256]{1,0:T(2,128)(2,1)S(1)} %get-tuple-element.96), channel_id=1, source_target_pairs={{8,16},{16,8},{24,32},{32,24},{40,48},{48,40},{56,64},{64,56},{72,... | collective-permute-start | bytes 3080 | tf_op jit(solution)/shard_map/ppermute | solution.py:237
  119.2 19.7 %copy-start = (bf16[2048,256]{1,0:T(8,128)(2,1)S(1)}, bf16[2048,256]{1,0:T(8,128)(2,1)}, u32[]{:S(2)}) copy-start(bf16[2048,256]{1,0:T(8,128)(2,1)} %w_ref.1) | copy-start | bytes 3145732
  119.2 19.7 %copy-start.2 = (bf16[128,256]{1,0:T(8,128)(2,1)S(1)}, bf16[128,256]{1,0:T(8,128)(2,1)}, u32[]{:S(2)}) copy-start(bf16[128,256]{1,0:T(8,128)(2,1)} %co_ref.1) | copy-start | bytes 196612
  119.2 19.7 %copy-start.4 = (bf16[128,256]{1,0:T(8,128)(2,1)S(1)}, bf16[128,256]{1,0:T(8,128)(2,1)}, u32[]{:S(2)}) copy-start(bf16[128,256]{1,0:T(8,128)(2,1)} %v_ref.1) | copy-start | bytes 196612
  119.2 19.7 %copy-start.5 = (bf16[128,256]{1,0:T(8,128)(2,1)S(1)}, bf16[128,256]{1,0:T(8,128)(2,1)}, u32[]{:S(2)}) copy-start(bf16[128,256]{1,0:T(8,128)(2,1)} %g_ref.1) | copy-start | bytes 196612
  119.2 19.7 %copy-start.6 = (f32[3,256]{1,0:T(4,128)S(1)}, f32[3,256]{1,0:T(4,128)}, u32[]{:S(2)}) copy-start(f32[3,256]{1,0:T(4,128)} %t_ref.1) | copy-start | bytes 9220
  119.2 7.6 %collective-permute-start.24 = (bf16[272,256]{1,0:T(8,128)(2,1)S(1)}, bf16[272,256]{1,0:T(8,128)(2,1)S(1)}, u32[]{:S(2)}, u32[]{:S(2)}) collective-permute-start(bf16[272,256]{1,0:T(8,128)(2,1)S(1)} %shard_map.189), channel_id=1, source_target_pairs={{0,2},{2,0},{4,6},{6,4},{1,3},{3,1},{5,7},{7,5},{8,10},{10,8},{12,... | collective-permute-start | bytes 417800 | tf_op jit(solution)/shard_map/ppermute | solution.py:52
  122.9 7.8 %collective-permute-start.25 = (bf16[272,256]{1,0:T(8,128)(2,1)S(1)}, bf16[272,256]{1,0:T(8,128)(2,1)S(1)}, u32[]{:S(2)}, u32[]{:S(2)}) collective-permute-start(bf16[272,256]{1,0:T(8,128)(2,1)S(1)} %shard_map.189), channel_id=1, source_target_pairs={{0,4},{2,6},{4,0},{6,2},{1,5},{3,7},{5,1},{7,3},{8,12},{10,14},{12... | collective-permute-start | bytes 417800 | tf_op jit(solution)/shard_map/ppermute | solution.py:52
  125.4 6.9 %collective-permute-start.26 = (bf16[272,256]{1,0:T(8,128)(2,1)S(1)}, bf16[272,256]{1,0:T(8,128)(2,1)S(1)}, u32[]{:S(2)}, u32[]{:S(2)}) collective-permute-start(bf16[272,256]{1,0:T(8,128)(2,1)S(1)} %shard_map.189), channel_id=1, source_target_pairs={{0,6},{2,4},{4,2},{6,0},{1,7},{3,5},{5,3},{7,1},{8,14},{10,12},{12... | collective-permute-start | bytes 417800 | tf_op jit(solution)/shard_map/ppermute | solution.py:52
  132.3 2.0 %collective-permute-start.27 = (bf16[1088,256]{1,0:T(8,128)(2,1)S(1)}, bf16[1088,256]{1,0:T(8,128)(2,1)S(1)}, u32[]{:S(2)}, u32[]{:S(2)}) collective-permute-start(bf16[1088,256]{1,0:T(8,128)(2,1)S(1)} %pad_maximum_fusion.own_ref), channel_id=1, source_target_pairs={{0,1},{1,0},{2,3},{3,2},{4,5},{5,4},{6,7},{7,6},{8,9},{9,8},{10,11... | collective-permute-start | bytes 1671176 | tf_op jit(solution)/shard_map/ppermute | solution.py:52
  134.7 5.3 %collective-permute-start.28 = (bf16[64,256]{1,0:T(8,128)(2,1)S(1)}, bf16[64,256]{1,0:T(8,128)(2,1)S(1)}, u32[]{:S(2)}, u32[]{:S(2)}) collective-permute-start(bf16[64,256]{1,0:T(8,128)(2,1)S(1)} %get-tuple-element.99), channel_id=1, source_target_pairs={{0,8},{8,0},{16,24},{24,16},{1,9},{9,1},{17,25},{25,17},{2,10},{10... | collective-permute-start | bytes 98312 | tf_op jit(solution)/shard_map/ppermute | solution.py:52
  136.0 4.1 %collective-permute-start.29 = (bf16[64,256]{1,0:T(8,128)(2,1)S(1)}, bf16[64,256]{1,0:T(8,128)(2,1)S(1)}, u32[]{:S(2)}, u32[]{:S(2)}) collective-permute-start(bf16[64,256]{1,0:T(8,128)(2,1)S(1)} %get-tuple-element.100), channel_id=1, source_target_pairs={{0,24},{8,16},{16,8},{24,0},{1,25},{9,17},{17,9},{25,1},{2,26},{10... | collective-permute-start | bytes 98312 | tf_op jit(solution)/shard_map/ppermute | solution.py:52
  138.1 5.4 %collective-permute-start.30 = (bf16[64,256]{1,0:T(8,128)(2,1)S(1)}, bf16[64,256]{1,0:T(8,128)(2,1)S(1)}, u32[]{:S(2)}, u32[]{:S(2)}) collective-permute-start(bf16[64,256]{1,0:T(8,128)(2,1)S(1)} %get-tuple-element.101), channel_id=1, source_target_pairs={{0,16},{8,24},{16,0},{24,8},{1,17},{9,25},{17,1},{25,9},{2,18},{10... | collective-permute-start | bytes 98312 | tf_op jit(solution)/shard_map/ppermute | solution.py:52

commit v2 on v1

--- a/solution.py
+++ b/solution.py
@@ -144,9 +144,20 @@
         mine_ref[d] = nn(d_ref[...], w_ref[:, pl.ds(o, ch)]).astype(BF)
 
 
-def pair_kernel(mine_ref, got_ref, *out_refs):
-    for d in range(4):
-        out_refs[d][...] = (mine_ref[d].astype(F32) + got_ref[d].astype(F32)).astype(BF)
+def pair_kernel(mine_ref, got_ref, keep_ref, *out_refs):
+    half = keep_ref.shape[0] // 2
+    keep_ref[...] = (mine_ref[0].astype(F32) + got_ref[0].astype(F32)).astype(BF)
+    for d in range(1, 4):
+        for k in range(2):
+            rows = slice(k * half, (k + 1) * half)
+            out_refs[2 * d - 2 + k][...] = (mine_ref[d, rows].astype(F32) + got_ref[d, rows].astype(F32)).astype(BF)
+
+
+def halves_kernel(keep_ref, in1_ref, in3_ref, out1_ref, out3_ref, sum_ref):
+    half = keep_ref.shape[0] // 2
+    for at, one, three in ((0, in1_ref, out3_ref), (half, out1_ref, in3_ref)):
+        total = keep_ref[at : at + half].astype(F32) + one[...].astype(F32) + three[...].astype(F32)
+        sum_ref[at : at + half] = total.astype(BF)
 
 
 def sum_kernel(*refs):
@@ -302,8 +313,17 @@
     )
     got = shift(theirs, "c", 2, 1)
     (mine,) = call(own_half_kernel, [(4, total, ch)], 2, (yi, ci, dgu_rows, w_pair), flops=2 * total * d * f)
-    pair = call(pair_kernel, [(total, ch)] * 4, 0, (mine, got))
-    parts = [shift(pair[k], "y", 4, k) for k in (1, 3, 2)]
+    half = total // 2
+    keep, lo1, hi1, lo2, hi2, lo3, hi3 = call(pair_kernel, [(total, ch)] + [(half, ch)] * 6, 0, (mine, got))
+    via1 = shift(lo2, "y", 4, 1)
+    via3 = shift(hi2, "y", 4, 3)
+    in1 = shift(lo1, "y", 4, 1)
+    in3 = shift(hi3, "y", 4, 3)
+    (lo3,) = call(sum_kernel, [(half, ch)], 0, (lo3, via1))
+    out3 = shift(lo3, "y", 4, 3)
+    (hi1,) = call(sum_kernel, [(half, ch)], 0, (hi1, via3))
+    out1 = shift(hi1, "y", 4, 1)
+    parts = (in1, in3, out1, out3)
     gate_t, up_t, grad_down = call(
         weights_kernel,
         [(f, d)] * 3,
@@ -314,7 +334,7 @@
         limit=24,
     )
     parts, mix, gate_t, up_t, grad_down = lax.optimization_barrier((parts, mix, gate_t, up_t, grad_down))
-    (summed,) = call(sum_kernel, [(total, ch)], 0, (pair[0], *parts))
+    (summed,) = call(halves_kernel, [(total, ch)], 0, (keep, *parts))
     back = lax.all_to_all(summed.reshape(n_exp, cap, ch), SP, 0, 0, tiled=True)
     dh, one, two = call(
         combine_kernel, [(tok, ch), (2, ch), (2, ch)], 1, (xi, sel, back.reshape(total, ch), out_grad, gate_b)

time: 145 us -> 144 us (level)
  starting transfers between devices: 30.3 us -> 32.4 us
    ppermute x25 -> x28, waiting for transfers between devices: 30.3 us -> 26.1 us  [shift(): return lax.ppermute(x, axis, [(i, i ^ k) for i in range(n)])]
    ppermute x3, waiting for transfers between devices: 18.8 us -> 21.5 us  [widen(): lax.ppermute(x, 'z', [(i, i ^ bit) for i in range(8)])]
    ppermute x25 -> x28, starting transfers between devices: 23.1 us -> 25.2 us  [shift(): return lax.ppermute(x, axis, [(i, i ^ k) for i in range(n)])]
    pallas_call x13 -> x15, Pallas kernels: 16.2 us -> 16.2 us  [call(): pl.pallas_call(body, out_shape=outs, in_specs=[SMEM if i < n_smem else AN...]
  transfers between devices with their start and end apart: 31 -> 34, of which waited for: 19 -> 20; matrix products, arithmetic and copies ran while one was open for 0% -> 0% of each run, Pallas kernels for 6% -> 6%
where the time goes in v2:
time: 144 us
  waiting for transfers between devices  50.7 us (35%)
  blocking collectives  43.7 us (30%)
  starting transfers between devices  32.4 us (22%)
  Pallas kernels  16.2 us (11%)
    all_to_all x1, blocking collectives, local(): recv = lax.all_to_all(send, SP, 0, 0, tiled=True)  28.3 us
    ppermute x28, waiting for transfers between devices, shift(): return lax.ppermute(x, axis, [(i, i ^ k) for i in range(n)])  26.1 us
    ppermute x28, starting transfers between devices, shift(): return lax.ppermute(x, axis, [(i, i ^ k) for i in range(n)])  25.2 us
    ppermute x3, waiting for transfers between devices, widen(): lax.ppermute(x, 'z', [(i, i ^ bit) for i in range(8)])  21.5 us
    pallas_call x15, Pallas kernels, call(): pl.pallas_call(body, out_shape=outs, in_specs=[SMEM if i < n_smem else AN...  16.2 us
    all_to_all x1, blocking collectives, local(): back = lax.all_to_all(summed.reshape(n_exp, cap, ch), SP, 0, 0, tiled=True)  15.4 us
    ppermute x1, waiting for transfers between devices, edges(): lax.ppermute(two, SP, [(i, i + 1 if i % 2 else i - 1) for i in range(1, n...  3.03 us
  transfers between devices with their start and end apart: 34, of which 20 were waited for; matrix products, arithmetic and copies ran while one was open for 0% of the time, Pallas kernels for 6%

profile of v2, /device:TPU:2, one launch (start us, length us, event | category | flops | bytes accessed | tf_op | source)
XLA Modules:
  0.0 144.0 jit_solution(15569824943935788130)
XLA Ops:
  0.6 1.4 shard_map.180
  2.0 28.3 %all_to_all.10 = bf16[32,32,256]{2,1,0:T(8,128)(2,1)S(1)} all-to-all(bf16[32,32,256]{2,1,0:T(8,128)(2,1)S(1)} %get-tuple-element.63), channel_id=1, replica_groups=mesh['z'=8,'x'=4,'y'=4,'c'=2] {'z','x'}, dimensions={0} | all-to-all | bytes 1048576 | tf_op jit(solution)/shard_map/all_to_all | solution.py:276
  30.3 3.1 %collective-permute-start.3 = (bf16[512,256]{1,0:T(8,128)(2,1)S(1)}, bf16[512,256]{1,0:T(8,128)(2,1)S(1)}, u32[]{:S(2)}, u32[]{:S(2)}) collective-permute-start(bf16[512,256]{1,0:T(8,128)(2,1)S(1)} %bitcast.30), channel_id=1, source_target_pairs={{0,6},{2,4},{4,2},{6,0},{1,7},{3,5},{5,3},{7,1},{8,14},{10,12},{12... | collective-permute-start | bytes 786440 | tf_op jit(solution)/shard_map/ppermute | solution.py:52
  33.4 0.1 collective-permute-start.4
  33.6 1.1 collective-permute-start.11
  34.6 0.8 collective-permute-start.2
  35.5 2.3 %shard_map.181 = (bf16[704,2048]{1,0:T(8,128)(2,1)S(1)}, bf16[352,2048]{1,0:T(8,128)(2,1)S(1)}) custom-call(bf16[352,2048]{1,0:T(8,128)(2,1)} %bitcast.34, bf16[352,2048]{1,0:T(8,128)(2,1)} %bitcast.35, bf16[352,2048]{1,0:T(8,128)(2,1)} %bitcast.36), custom_call_target="tpu_custom_call" | custom-call | tf_op jit(solution)/shard_map/pallas_call | solution.py:28
  37.7 3.1 %collective-permute-done.3.refs_12_ = bf16[512,256]{1,0:T(8,128)(2,1)S(1)} collective-permute-done((bf16[512,256]{1,0:T(8,128)(2,1)S(1)}, bf16[512,256]{1,0:T(8,128)(2,1)S(1)}, u32[]{:S(2)}, u32[]{:S(2)}) %collective-permute-start.3) | collective-permute-done | bytes 262176 | tf_op jit(solution)/shard_map/ppermute | solution.py:52
  40.8 1.8 %collective-permute-done.4.refs_5_ = bf16[512,256]{1,0:T(8,128)(2,1)S(1)} collective-permute-done((bf16[512,256]{1,0:T(8,128)(2,1)S(1)}, bf16[512,256]{1,0:T(8,128)(2,1)S(1)}, u32[]{:S(2)}, u32[]{:S(2)}) %collective-permute-start.4) | collective-permute-done | bytes 262176 | tf_op jit(solution)/shard_map/ppermute | solution.py:52
  42.6 1.2 collective-permute-start.8
  43.8 0.2 collective-permute-done.11.refs_13_
  44.1 0.4 collective-permute-start.7
  44.4 1.1 collective-permute-done.2.refs_4_
  45.5 0.5 collective-permute-start.6
  46.0 0.1 collective-permute-start.13
  46.1 4.7 %collective-permute-done.8.refs_9_ = bf16[512,256]{1,0:T(8,128)(2,1)S(1)} collective-permute-done((bf16[512,256]{1,0:T(8,128)(2,1)S(1)}, bf16[512,256]{1,0:T(8,128)(2,1)S(1)}, u32[]{:S(2)}, u32[]{:S(2)}) %collective-permute-start.8) | collective-permute-done | bytes 262176 | tf_op jit(solution)/shard_map/ppermute | solution.py:52
  50.8 1.5 %collective-permute-done.7.refs_8_ = bf16[512,256]{1,0:T(8,128)(2,1)S(1)} collective-permute-done((bf16[512,256]{1,0:T(8,128)(2,1)S(1)}, bf16[512,256]{1,0:T(8,128)(2,1)S(1)}, u32[]{:S(2)}, u32[]{:S(2)}) %collective-permute-start.7) | collective-permute-done | bytes 262176 | tf_op jit(solution)/shard_map/ppermute | solution.py:52
  52.3 0.5 collective-permute-start.9
  52.8 1.0 collective-permute-done.10.refs_11_
  53.8 0.4 collective-permute-done.9.refs_10_
  54.2 4.1 %shard_map.182 = (bf16[4,512,256]{2,1,0:T(8,128)(2,1)S(1)}, bf16[512,2048]{1,0:T(8,128)(2,1)S(1)}, bf16[512,2048]{1,0:T(8,128)(2,1)S(1)}, bf16[352,512]{1,0:T(8,...) custom-call(s32[1]{0:T(128)} %bitcast.y_ref, s32[1]{0:T(128)} %bitcast.1.c_ref, ...), custom_call_target="tpu_custom_call" | custom-call | flops 2952790016 | tf_op jit(solution)/shard_map/pallas_call | solution.py:28
  58.3 0.4 collective-permute-start.14
  58.7 0.9 shard_map.187
  59.6 1.7 %collective-permute-start.21 = (bf16[128,256]{1,0:T(8,128)(2,1)S(1)}, bf16[128,256]{1,0:T(8,128)(2,1)S(1)}, u32[]{:S(2)}, u32[]{:S(2)}) collective-permute-start(bf16[128,256]{1,0:T(8,128)(2,1)S(1)} %shard_map.187), channel_id=1, source_target_pairs={{0,128},{32,160},{64,192},{96,224},{128,0},{160,32},{192,64},{224,... | collective-permute-start | bytes 196616 | tf_op jit(solution)/shard_map/ppermute | solution.py:253
  61.3 7.6 %collective-permute-done.21 = bf16[128,256]{1,0:T(8,128)(2,1)S(1)} collective-permute-done((bf16[128,256]{1,0:T(8,128)(2,1)S(1)}, bf16[128,256]{1,0:T(8,128)(2,1)S(1)}, u32[]{:S(2)}, u32[]{:S(2)}) %collective-permute-start.21) | collective-permute-done | bytes 65568 | tf_op jit(solution)/shard_map/ppermute | solution.py:253
  68.8 0.1 collective-permute-start.22
  68.9 8.8 %collective-permute-done.22 = bf16[256,256]{1,0:T(8,128)(2,1)S(1)} collective-permute-done((bf16[256,256]{1,0:T(8,128)(2,1)S(1)}, bf16[256,256]{1,0:T(8,128)(2,1)S(1)}, u32[]{:S(2)}, u32[]{:S(2)}) %collective-permute-start.22) | collective-permute-done | bytes 131104 | tf_op jit(solution)/shard_map/ppermute | solution.py:253
  77.8 0.1 collective-permute-start.23
  77.9 1.0 shard_map.183.mine_ref
  78.9 0.2 shard_map.184
  79.2 0.4 collective-permute-start.19
  79.6 1.1 collective-permute-start.17
  80.7 5.1 %collective-permute-done.23 = bf16[512,256]{1,0:T(8,128)(2,1)S(1)} collective-permute-done((bf16[512,256]{1,0:T(8,128)(2,1)S(1)}, bf16[512,256]{1,0:T(8,128)(2,1)S(1)}, u32[]{:S(2)}, u32[]{:S(2)}) %collective-permute-start.23) | collective-permute-done | bytes 262176 | tf_op jit(solution)/shard_map/ppermute | solution.py:253
  85.8 0.4 collective-permute-start.15
  86.2 0.5 collective-permute-start.16
  86.8 2.8 %collective-permute-start.20 = (bf16[256,256]{1,0:T(8,128)(2,1)S(1)}, bf16[256,256]{1,0:T(8,128)(2,1)S(1)}, u32[]{:S(2)}, u32[]{:S(2)}) collective-permute-start(bf16[256,256]{1,0:T(8,128)(2,1)S(1)} %shard_map.186), channel_id=1, source_target_pairs={{0,6},{2,4},{4,2},{6,0},{1,7},{3,5},{5,3},{7,1},{8,14},{10,12},{12... | collective-permute-start | bytes 393224 | tf_op jit(solution)/shard_map/ppermute | solution.py:52
  89.6 0.6 collective-permute-start.18
  90.2 3.8 %shard_map.188 = (bf16[352,2048]{1,0:T(8,128)(2,1)}, bf16[352,2048]{1,0:T(8,128)(2,1)}, bf16[352,2048]{1,0:T(8,128)(2,1)}) custom-call(bf16[512,2048]{1,0:T(8,128)(2,1)S(1)} %get-tuple-element.84.x_ref, bf16[512,2048]{1,0:T(8,128)(2,1)S(1)} %get-tuple-element.85.dy_ref, bf16[352,512]{1,0:T(8,128)(2,1)S(1)} %get-tuple-element.86.hid_ref, ...), custom_call_target="tpu_custom_call" | custom-call | flops 2214592512 | tf_op jit(solution)/shard_map/pallas_call | solution.py:28
  94.0 0.2 collective-permute-done.20.out3_ref
  94.2 0.5 collective-permute-done.18.out1_ref
  94.7 0.1 shard_map.189
  94.8 15.4 %all_to_all.11 = bf16[32,16,256]{2,1,0:T(8,128)(2,1)S(1)} all-to-all(bf16[32,16,256]{2,1,0:T(8,128)(2,1)S(1)} %bitcast.25), channel_id=1, replica_groups=mesh['z'=8,'x'=4,'y'=4,'c'=2] {'z','x'}, dimensions={0} | all-to-all | bytes 524288 | tf_op jit(solution)/shard_map/all_to_all | solution.py:338
  110.2 0.2 shard_map.190
  110.4 0.7 collective-permute-start.24
  111.1 2.3 %collective-permute-start.25 = (bf16[2,256]{1,0:T(2,128)(2,1)S(1)}, bf16[2,256]{1,0:T(2,128)(2,1)S(1)}, u32[]{:S(2)}, u32[]{:S(2)}) collective-permute-start(bf16[2,256]{1,0:T(2,128)(2,1)S(1)} %get-tuple-element.103), channel_id=1, source_target_pairs={{0,8},{8,0},{16,24},{24,16},{32,40},{40,32},{48,56},{56,48},{64,72... | collective-permute-start | bytes 3080 | tf_op jit(solution)/shard_map/ppermute | solution.py:247
  113.4 2.4 %collective-permute-start.26 = (bf16[2,256]{1,0:T(2,128)(2,1)S(1)}, bf16[2,256]{1,0:T(2,128)(2,1)S(1)}, u32[]{:S(2)}, u32[]{:S(2)}) collective-permute-start(bf16[2,256]{1,0:T(2,128)(2,1)S(1)} %get-tuple-element.104), channel_id=1, source_target_pairs={{8,16},{16,8},{24,32},{32,24},{40,48},{48,40},{56,64},{64,56},{72,... | collective-permute-start | bytes 3080 | tf_op jit(solution)/shard_map/ppermute | solution.py:248
  115.8 3.0 %collective-permute-done.26.high_ref.bh_ref = bf16[2,256]{1,0:T(2,128)(2,1)S(1)} collective-permute-done((bf16[2,256]{1,0:T(2,128)(2,1)S(1)}, bf16[2,256]{1,0:T(2,128)(2,1)S(1)}, u32[]{:S(2)}, u32[]{:S(2)}) %collective-permute-start.26) | collective-permute-done | bytes 1056 | tf_op jit(solution)/shard_map/ppermute | solution.py:248
  118.9 0.0 copy-start.2
  118.9 3.7 %collective-permute-start.27 = (bf16[272,256]{1,0:T(8,128)(2,1)S(1)}, bf16[272,256]{1,0:T(8,128)(2,1)S(1)}, u32[]{:S(2)}, u32[]{:S(2)}) collective-permute-start(bf16[272,256]{1,0:T(8,128)(2,1)S(1)} %shard_map.191), channel_id=1, source_target_pairs={{0,2},{2,0},{4,6},{6,4},{1,3},{3,1},{5,7},{7,5},{8,10},{10,8},{12,... | collective-permute-start | bytes 417800 | tf_op jit(solution)/shard_map/ppermute | solution.py:52
  122.7 2.6 %collective-permute-start.28 = (bf16[272,256]{1,0:T(8,128)(2,1)S(1)}, bf16[272,256]{1,0:T(8,128)(2,1)S(1)}, u32[]{:S(2)}, u32[]{:S(2)}) collective-permute-start(bf16[272,256]{1,0:T(8,128)(2,1)S(1)} %shard_map.191), channel_id=1, source_target_pairs={{0,4},{2,6},{4,0},{6,2},{1,5},{3,7},{5,1},{7,3},{8,12},{10,14},{12... | collective-permute-start | bytes 417800 | tf_op jit(solution)/shard_map/ppermute | solution.py:52
  125.3 0.5 collective-permute-start.29
  125.7 1.2 collective-permute-done.27
  126.9 3.4 %collective-permute-done.28 = bf16[272,256]{1,0:T(8,128)(2,1)S(1)} collective-permute-done((bf16[272,256]{1,0:T(8,128)(2,1)S(1)}, bf16[272,256]{1,0:T(8,128)(2,1)S(1)}, u32[]{:S(2)}, u32[]{:S(2)}) %collective-permute-start.28) | collective-permute-done | bytes 139296 | tf_op jit(solution)/shard_map/ppermute | solution.py:52
  130.4 1.5 %collective-permute-done.29 = bf16[272,256]{1,0:T(8,128)(2,1)S(1)} collective-permute-done((bf16[272,256]{1,0:T(8,128)(2,1)S(1)}, bf16[272,256]{1,0:T(8,128)(2,1)S(1)}, u32[]{:S(2)}, u32[]{:S(2)}) %collective-permute-start.29) | collective-permute-done | bytes 139296 | tf_op jit(solution)/shard_map/ppermute | solution.py:52
  131.9 0.1 collective-permute-start.30
  132.0 1.9 %collective-permute-done.30.part_ref = bf16[1088,256]{1,0:T(8,128)(2,1)S(1)} collective-permute-done((bf16[1088,256]{1,0:T(8,128)(2,1)S(1)}, bf16[1088,256]{1,0:T(8,128)(2,1)S(1)}, u32[]{:S(2)}, u32[]{:S(2)}) %collective-permute-start.30) | collective-permute-done | bytes 557088 | tf_op jit(solution)/shard_map/ppermute | solution.py:52
  134.0 0.4 shard_map.192
  134.4 2.1 %collective-permute-start.31 = (bf16[64,256]{1,0:T(8,128)(2,1)S(1)}, bf16[64,256]{1,0:T(8,128)(2,1)S(1)}, u32[]{:S(2)}, u32[]{:S(2)}) collective-permute-start(bf16[64,256]{1,0:T(8,128)(2,1)S(1)} %get-tuple-element.107), channel_id=1, source_target_pairs={{0,8},{8,0},{16,24},{24,16},{1,9},{9,1},{17,25},{25,17},{2,10},{10... | collective-permute-start | bytes 98312 | tf_op jit(solution)/shard_map/ppermute | solution.py:52
  136.5 1.5 %collective-permute-start.32 = (bf16[64,256]{1,0:T(8,128)(2,1)S(1)}, bf16[64,256]{1,0:T(8,128)(2,1)S(1)}, u32[]{:S(2)}, u32[]{:S(2)}) collective-permute-start(bf16[64,256]{1,0:T(8,128)(2,1)S(1)} %get-tuple-element.108), channel_id=1, source_target_pairs={{0,24},{8,16},{16,8},{24,0},{1,25},{9,17},{17,9},{25,1},{2,26},{10... | collective-permute-start | bytes 98312 | tf_op jit(solution)/shard_map/ppermute | solution.py:52
  138.0 0.7 collective-permute-start.33
  138.7 1.1 shard_map.194
  139.7 0.7 collective-permute-done.32.refs_2_
  140.4 3.0 %collective-permute-done.33.refs_3_ = bf16[64,256]{1,0:T(8,128)(2,1)S(1)} collective-permute-done((bf16[64,256]{1,0:T(8,128)(2,1)S(1)}, bf16[64,256]{1,0:T(8,128)(2,1)S(1)}, u32[]{:S(2)}, u32[]{:S(2)}) %collective-permute-start.33) | collective-permute-done | bytes 32800 | tf_op jit(solution)/shard_map/ppermute | solution.py:52
  143.4 0.6 shard_map.193
  (40 shorter events, 0.3 us)
Async XLA Ops:
  30.3 10.5 %collective-permute-start.3 = (bf16[512,256]{1,0:T(8,128)(2,1)S(1)}, bf16[512,256]{1,0:T(8,128)(2,1)S(1)}, u32[]{:S(2)}, u32[]{:S(2)}) collective-permute-start(bf16[512,256]{1,0:T(8,128)(2,1)S(1)} %bitcast.30), channel_id=1, source_target_pairs={{0,6},{2,4},{4,2},{6,0},{1,7},{3,5},{5,3},{7,1},{8,14},{10,12},{12... | collective-permute-start | bytes 786440 | tf_op jit(solution)/shard_map/ppermute | solution.py:52
  33.4 9.2 %collective-permute-start.4 = (bf16[512,256]{1,0:T(8,128)(2,1)S(1)}, bf16[512,256]{1,0:T(8,128)(2,1)S(1)}, u32[]{:S(2)}, u32[]{:S(2)}) collective-permute-start(bf16[512,256]{1,0:T(8,128)(2,1)S(1)} %bitcast.26), channel_id=1, source_target_pairs={{0,2},{2,0},{4,6},{6,4},{1,3},{3,1},{5,7},{7,5},{8,10},{10,8},{12,... | collective-permute-start | bytes 786440 | tf_op jit(solution)/shard_map/ppermute | solution.py:52
  33.6 10.5 %collective-permute-start.11 = (bf16[512,256]{1,0:T(8,128)(2,1)S(1)}, bf16[512,256]{1,0:T(8,128)(2,1)S(1)}, u32[]{:S(2)}, u32[]{:S(2)}) collective-permute-start(bf16[512,256]{1,0:T(8,128)(2,1)S(1)} %bitcast.27), channel_id=1, source_target_pairs={{0,6},{2,4},{4,2},{6,0},{1,7},{3,5},{5,3},{7,1},{8,14},{10,12},{12... | collective-permute-start | bytes 786440 | tf_op jit(solution)/shard_map/ppermute | solution.py:52
  34.6 10.9 %collective-permute-start.2 = (bf16[512,256]{1,0:T(8,128)(2,1)S(1)}, bf16[512,256]{1,0:T(8,128)(2,1)S(1)}, u32[]{:S(2)}, u32[]{:S(2)}) collective-permute-start(bf16[512,256]{1,0:T(8,128)(2,1)S(1)} %bitcast.31), channel_id=1, source_target_pairs={{0,2},{2,0},{4,6},{6,4},{1,3},{3,1},{5,7},{7,5},{8,10},{10,8},{12,... | collective-permute-start | bytes 786440 | tf_op jit(solution)/shard_map/ppermute | solution.py:52
  35.4 10.1 %collective-permute-start = (bf16[512,256]{1,0:T(8,128)(2,1)S(1)}, bf16[512,256]{1,0:T(8,128)(2,1)S(1)}, u32[]{:S(2)}, u32[]{:S(2)}) collective-permute-start(bf16[512,256]{1,0:T(8,128)(2,1)S(1)} %bitcast.32), channel_id=1, source_target_pairs={{0,1},{1,0},{2,3},{3,2},{4,5},{5,4},{6,7},{7,6},{8,9},{9,8},{10,11... | collective-permute-start | bytes 786440 | tf_op jit(solution)/shard_map/ppermute | solution.py:52
  40.8 5.2 %collective-permute-start.1 = (bf16[512,256]{1,0:T(8,128)(2,1)S(1)}, bf16[512,256]{1,0:T(8,128)(2,1)S(1)}, u32[]{:S(2)}, u32[]{:S(2)}) collective-permute-start(bf16[512,256]{1,0:T(8,128)(2,1)S(1)} %bitcast.28), channel_id=1, source_target_pairs={{0,1},{1,0},{2,3},{3,2},{4,5},{5,4},{6,7},{7,6},{8,9},{9,8},{10,11... | collective-permute-start | bytes 786440 | tf_op jit(solution)/shard_map/ppermute | solution.py:52
  42.6 8.2 %collective-permute-start.8 = (bf16[512,256]{1,0:T(8,128)(2,1)S(1)}, bf16[512,256]{1,0:T(8,128)(2,1)S(1)}, u32[]{:S(2)}, u32[]{:S(2)}) collective-permute-start(bf16[512,256]{1,0:T(8,128)(2,1)S(1)} %collective-permute-done.4.refs_5_), channel_id=1, source_target_pairs={{0,6},{2,4},{4,2},{6,0},{1,7},{3,5},{5,3},{7,1},{8,14},{10,12},{12... | collective-permute-start | bytes 786440 | tf_op jit(solution)/shard_map/ppermute | solution.py:52
  44.1 8.2 %collective-permute-start.7 = (bf16[512,256]{1,0:T(8,128)(2,1)S(1)}, bf16[512,256]{1,0:T(8,128)(2,1)S(1)}, u32[]{:S(2)}, u32[]{:S(2)}) collective-permute-start(bf16[512,256]{1,0:T(8,128)(2,1)S(1)} %collective-permute-done.3.refs_12_), channel_id=1, source_target_pairs={{0,2},{2,0},{4,6},{6,4},{1,3},{3,1},{5,7},{7,5},{8,10},{10,8},{12,... | collective-permute-start | bytes 786440 | tf_op jit(solution)/shard_map/ppermute | solution.py:52
  45.5 6.7 %collective-permute-start.12 = (bf16[512,256]{1,0:T(8,128)(2,1)S(1)}, bf16[512,256]{1,0:T(8,128)(2,1)S(1)}, u32[]{:S(2)}, u32[]{:S(2)}) collective-permute-start(bf16[512,256]{1,0:T(8,128)(2,1)S(1)} %collective-permute-done.3.refs_12_), channel_id=1, source_target_pairs={{0,1},{1,0},{2,3},{3,2},{4,5},{5,4},{6,7},{7,6},{8,9},{9,8},{10,11... | collective-permute-start | bytes 786440 | tf_op jit(solution)/shard_map/ppermute | solution.py:52
  45.5 7.3 %collective-permute-start.6 = (bf16[512,256]{1,0:T(8,128)(2,1)S(1)}, bf16[512,256]{1,0:T(8,128)(2,1)S(1)}, u32[]{:S(2)}, u32[]{:S(2)}) collective-permute-start(bf16[512,256]{1,0:T(8,128)(2,1)S(1)} %collective-permute-done.4.refs_5_), channel_id=1, source_target_pairs={{0,1},{1,0},{2,3},{3,2},{4,5},{5,4},{6,7},{7,6},{8,9},{9,8},{10,11... | collective-permute-start | bytes 786440 | tf_op jit(solution)/shard_map/ppermute | solution.py:52
  46.0 6.7 %collective-permute-start.13 = (bf16[512,256]{1,0:T(8,128)(2,1)S(1)}, bf16[512,256]{1,0:T(8,128)(2,1)S(1)}, u32[]{:S(2)}, u32[]{:S(2)}) collective-permute-start(bf16[512,256]{1,0:T(8,128)(2,1)S(1)} %collective-permute-done.11.refs_13_), channel_id=1, source_target_pairs={{0,1},{1,0},{2,3},{3,2},{4,5},{5,4},{6,7},{7,6},{8,9},{9,8},{10,11... | collective-permute-start | bytes 786440 | tf_op jit(solution)/shard_map/ppermute | solution.py:52
  50.8 2.0 %collective-permute-start.5 = (bf16[512,256]{1,0:T(8,128)(2,1)S(1)}, bf16[512,256]{1,0:T(8,128)(2,1)S(1)}, u32[]{:S(2)}, u32[]{:S(2)}) collective-permute-start(bf16[512,256]{1,0:T(8,128)(2,1)S(1)} %collective-permute-done.2.refs_4_), channel_id=1, source_target_pairs={{0,1},{1,0},{2,3},{3,2},{4,5},{5,4},{6,7},{7,6},{8,9},{9,8},{10,11... | collective-permute-start | bytes 786440 | tf_op jit(solution)/shard_map/ppermute | solution.py:52
  52.3 1.5 %collective-permute-start.10 = (bf16[512,256]{1,0:T(8,128)(2,1)S(1)}, bf16[512,256]{1,0:T(8,128)(2,1)S(1)}, u32[]{:S(2)}, u32[]{:S(2)}) collective-permute-start(bf16[512,256]{1,0:T(8,128)(2,1)S(1)} %collective-permute-done.8.refs_9_), channel_id=1, source_target_pairs={{0,1},{1,0},{2,3},{3,2},{4,5},{5,4},{6,7},{7,6},{8,9},{9,8},{10,11... | collective-permute-start | bytes 786440 | tf_op jit(solution)/shard_map/ppermute | solution.py:52
  52.3 1.9 %collective-permute-start.9 = (bf16[512,256]{1,0:T(8,128)(2,1)S(1)}, bf16[512,256]{1,0:T(8,128)(2,1)S(1)}, u32[]{:S(2)}, u32[]{:S(2)}) collective-permute-start(bf16[512,256]{1,0:T(8,128)(2,1)S(1)} %collective-permute-done.7.refs_8_), channel_id=1, source_target_pairs={{0,1},{1,0},{2,3},{3,2},{4,5},{5,4},{6,7},{7,6},{8,9},{9,8},{10,11... | collective-permute-start | bytes 786440 | tf_op jit(solution)/shard_map/ppermute | solution.py:52
  58.3 20.6 %collective-permute-start.14 = (bf16[4,512,256]{2,1,0:T(8,128)(2,1)S(1)}, bf16[4,512,256]{2,1,0:T(8,128)(2,1)S(1)}, u32[]{:S(2)}, u32[]{:S(2)}) collective-permute-start(bf16[4,512,256]{2,1,0:T(8,128)(2,1)S(1)} %get-tuple-element.75), channel_id=1, source_target_pairs={{0,1},{1,0},{2,3},{3,2},{4,5},{5,4},{6,7},{7,6},{8,9},{9,8},{10,11... | collective-permute-start | bytes 3145736 | tf_op jit(solution)/shard_map/ppermute | solution.py:52
  59.6 9.2 %collective-permute-start.21 = (bf16[128,256]{1,0:T(8,128)(2,1)S(1)}, bf16[128,256]{1,0:T(8,128)(2,1)S(1)}, u32[]{:S(2)}, u32[]{:S(2)}) collective-permute-start(bf16[128,256]{1,0:T(8,128)(2,1)S(1)} %shard_map.187), channel_id=1, source_target_pairs={{0,128},{32,160},{64,192},{96,224},{128,0},{160,32},{192,64},{224,... | collective-permute-start | bytes 196616 | tf_op jit(solution)/shard_map/ppermute | solution.py:253
  68.8 8.9 %collective-permute-start.22 = (bf16[256,256]{1,0:T(8,128)(2,1)S(1)}, bf16[256,256]{1,0:T(8,128)(2,1)S(1)}, u32[]{:S(2)}, u32[]{:S(2)}) collective-permute-start(bf16[256,256]{1,0:T(8,128)(2,1)S(1)} %pad_maximum_fusion.3), channel_id=1, source_target_pairs={{0,64},{32,96},{64,0},{96,32},{128,192},{160,224},{192,128},{224,1... | collective-permute-start | bytes 393224 | tf_op jit(solution)/shard_map/ppermute | solution.py:253
  77.8 7.9 %collective-permute-start.23 = (bf16[512,256]{1,0:T(8,128)(2,1)S(1)}, bf16[512,256]{1,0:T(8,128)(2,1)S(1)}, u32[]{:S(2)}, u32[]{:S(2)}) collective-permute-start(bf16[512,256]{1,0:T(8,128)(2,1)S(1)} %pad_maximum_fusion.2), channel_id=1, source_target_pairs={{0,32},{32,0},{64,96},{96,64},{128,160},{160,128},{192,224},{224,1... | collective-permute-start | bytes 786440 | tf_op jit(solution)/shard_map/ppermute | solution.py:253
  79.2 7.6 %collective-permute-start.19 = (bf16[256,256]{1,0:T(8,128)(2,1)S(1)}, bf16[256,256]{1,0:T(8,128)(2,1)S(1)}, u32[]{:S(2)}, u32[]{:S(2)}) collective-permute-start(bf16[256,256]{1,0:T(8,128)(2,1)S(1)} %get-tuple-element.81), channel_id=1, source_target_pairs={{0,2},{2,0},{4,6},{6,4},{1,3},{3,1},{5,7},{7,5},{8,10},{10,8},{12,... | collective-permute-start | bytes 393224 | tf_op jit(solution)/shard_map/ppermute | solution.py:52
  79.6 10.0 %collective-permute-start.17 = (bf16[256,256]{1,0:T(8,128)(2,1)S(1)}, bf16[256,256]{1,0:T(8,128)(2,1)S(1)}, u32[]{:S(2)}, u32[]{:S(2)}) collective-permute-start(bf16[256,256]{1,0:T(8,128)(2,1)S(1)} %get-tuple-element.79), channel_id=1, source_target_pairs={{0,6},{2,4},{4,2},{6,0},{1,7},{3,5},{5,3},{7,1},{8,14},{10,12},{12... | collective-permute-start | bytes 393224 | tf_op jit(solution)/shard_map/ppermute | solution.py:52
  85.8 8.2 %collective-permute-start.15 = (bf16[256,256]{1,0:T(8,128)(2,1)S(1)}, bf16[256,256]{1,0:T(8,128)(2,1)S(1)}, u32[]{:S(2)}, u32[]{:S(2)}) collective-permute-start(bf16[256,256]{1,0:T(8,128)(2,1)S(1)} %get-tuple-element.76), channel_id=1, source_target_pairs={{0,2},{2,0},{4,6},{6,4},{1,3},{3,1},{5,7},{7,5},{8,10},{10,8},{12,... | collective-permute-start | bytes 393224 | tf_op jit(solution)/shard_map/ppermute | solution.py:52
  86.2 7.8 %collective-permute-start.16 = (bf16[256,256]{1,0:T(8,128)(2,1)S(1)}, bf16[256,256]{1,0:T(8,128)(2,1)S(1)}, u32[]{:S(2)}, u32[]{:S(2)}) collective-permute-start(bf16[256,256]{1,0:T(8,128)(2,1)S(1)} %get-tuple-element.77), channel_id=1, source_target_pairs={{0,6},{2,4},{4,2},{6,0},{1,7},{3,5},{5,3},{7,1},{8,14},{10,12},{12... | collective-permute-start | bytes 393224 | tf_op jit(solution)/shard_map/ppermute | solution.py:52
  86.8 7.4 %collective-permute-start.20 = (bf16[256,256]{1,0:T(8,128)(2,1)S(1)}, bf16[256,256]{1,0:T(8,128)(2,1)S(1)}, u32[]{:S(2)}, u32[]{:S(2)}) collective-permute-start(bf16[256,256]{1,0:T(8,128)(2,1)S(1)} %shard_map.186), channel_id=1, source_target_pairs={{0,6},{2,4},{4,2},{6,0},{1,7},{3,5},{5,3},{7,1},{8,14},{10,12},{12... | collective-permute-start | bytes 393224 | tf_op jit(solution)/shard_map/ppermute | solution.py:52
  89.6 5.1 %collective-permute-start.18 = (bf16[256,256]{1,0:T(8,128)(2,1)S(1)}, bf16[256,256]{1,0:T(8,128)(2,1)S(1)}, u32[]{:S(2)}, u32[]{:S(2)}) collective-permute-start(bf16[256,256]{1,0:T(8,128)(2,1)S(1)} %shard_map.185), channel_id=1, source_target_pairs={{0,2},{2,0},{4,6},{6,4},{1,3},{3,1},{5,7},{7,5},{8,10},{10,8},{12,... | collective-permute-start | bytes 393224 | tf_op jit(solution)/shard_map/ppermute | solution.py:52
  94.0 16.2 %copy-start.1 = (bf16[128,256]{1,0:T(8,128)(2,1)S(1)}, bf16[128,256]{1,0:T(8,128)(2,1)}, u32[]{:S(2)}) copy-start(bf16[128,256]{1,0:T(8,128)(2,1)} %b_ref.2) | copy-start | bytes 196612
  94.0 16.2 %copy-start.3 = (bf16[128,256]{1,0:T(8,128)(2,1)S(1)}, bf16[128,256]{1,0:T(8,128)(2,1)}, u32[]{:S(2)}) copy-start(bf16[128,256]{1,0:T(8,128)(2,1)} %og_ref.3) | copy-start | bytes 196612
  110.4 8.4 %collective-permute-start.24 = (bf16[128,256]{1,0:T(8,128)(2,1)S(1)}, bf16[128,256]{1,0:T(8,128)(2,1)S(1)}, u32[]{:S(2)}, u32[]{:S(2)}) collective-permute-start(bf16[128,256]{1,0:T(8,128)(2,1)S(1)} %get-tuple-element.102.dh_ref), channel_id=1, source_target_pairs={{0,0},{1,32},{2,64},{3,96},{4,128},{5,160},{6,192},{7,224},{32,1},... | collective-permute-start | bytes 196616 | tf_op jit(solution)/shard_map/ppermute | solution.py:343
  111.1 4.7 %collective-permute-start.25 = (bf16[2,256]{1,0:T(2,128)(2,1)S(1)}, bf16[2,256]{1,0:T(2,128)(2,1)S(1)}, u32[]{:S(2)}, u32[]{:S(2)}) collective-permute-start(bf16[2,256]{1,0:T(2,128)(2,1)S(1)} %get-tuple-element.103), channel_id=1, source_target_pairs={{0,8},{8,0},{16,24},{24,16},{32,40},{40,32},{48,56},{56,48},{64,72... | collective-permute-start | bytes 3080 | tf_op jit(solution)/shard_map/ppermute | solution.py:247
  113.4 5.5 %collective-permute-start.26 = (bf16[2,256]{1,0:T(2,128)(2,1)S(1)}, bf16[2,256]{1,0:T(2,128)(2,1)S(1)}, u32[]{:S(2)}, u32[]{:S(2)}) collective-permute-start(bf16[2,256]{1,0:T(2,128)(2,1)S(1)} %get-tuple-element.104), channel_id=1, source_target_pairs={{8,16},{16,8},{24,32},{32,24},{40,48},{48,40},{56,64},{64,56},{72,... | collective-permute-start | bytes 3080 | tf_op jit(solution)/shard_map/ppermute | solution.py:248
  118.9 19.8 %copy-start = (bf16[2048,256]{1,0:T(8,128)(2,1)S(1)}, bf16[2048,256]{1,0:T(8,128)(2,1)}, u32[]{:S(2)}) copy-start(bf16[2048,256]{1,0:T(8,128)(2,1)} %w_ref.1) | copy-start | bytes 3145732
  118.9 19.8 %copy-start.2 = (bf16[128,256]{1,0:T(8,128)(2,1)S(1)}, bf16[128,256]{1,0:T(8,128)(2,1)}, u32[]{:S(2)}) copy-start(bf16[128,256]{1,0:T(8,128)(2,1)} %co_ref.1) | copy-start | bytes 196612
  118.9 19.8 %copy-start.4 = (bf16[128,256]{1,0:T(8,128)(2,1)S(1)}, bf16[128,256]{1,0:T(8,128)(2,1)}, u32[]{:S(2)}) copy-start(bf16[128,256]{1,0:T(8,128)(2,1)} %v_ref.1) | copy-start | bytes 196612
  118.9 19.7 %copy-start.5 = (bf16[128,256]{1,0:T(8,128)(2,1)S(1)}, bf16[128,256]{1,0:T(8,128)(2,1)}, u32[]{:S(2)}) copy-start(bf16[128,256]{1,0:T(8,128)(2,1)} %g_ref.1) | copy-start | bytes 196612
  118.9 19.7 %copy-start.6 = (f32[3,256]{1,0:T(4,128)S(1)}, f32[3,256]{1,0:T(4,128)}, u32[]{:S(2)}) copy-start(f32[3,256]{1,0:T(4,128)} %t_ref.1) | copy-start | bytes 9220
  118.9 8.0 %collective-permute-start.27 = (bf16[272,256]{1,0:T(8,128)(2,1)S(1)}, bf16[272,256]{1,0:T(8,128)(2,1)S(1)}, u32[]{:S(2)}, u32[]{:S(2)}) collective-permute-start(bf16[272,256]{1,0:T(8,128)(2,1)S(1)} %shard_map.191), channel_id=1, source_target_pairs={{0,2},{2,0},{4,6},{6,4},{1,3},{3,1},{5,7},{7,5},{8,10},{10,8},{12,... | collective-permute-start | bytes 417800 | tf_op jit(solution)/shard_map/ppermute | solution.py:52
  122.7 7.7 %collective-permute-start.28 = (bf16[272,256]{1,0:T(8,128)(2,1)S(1)}, bf16[272,256]{1,0:T(8,128)(2,1)S(1)}, u32[]{:S(2)}, u32[]{:S(2)}) collective-permute-start(bf16[272,256]{1,0:T(8,128)(2,1)S(1)} %shard_map.191), channel_id=1, source_target_pairs={{0,4},{2,6},{4,0},{6,2},{1,5},{3,7},{5,1},{7,3},{8,12},{10,14},{12... | collective-permute-start | bytes 417800 | tf_op jit(solution)/shard_map/ppermute | solution.py:52
  125.3 6.6 %collective-permute-start.29 = (bf16[272,256]{1,0:T(8,128)(2,1)S(1)}, bf16[272,256]{1,0:T(8,128)(2,1)S(1)}, u32[]{:S(2)}, u32[]{:S(2)}) collective-permute-start(bf16[272,256]{1,0:T(8,128)(2,1)S(1)} %shard_map.191), channel_id=1, source_target_pairs={{0,6},{2,4},{4,2},{6,0},{1,7},{3,5},{5,3},{7,1},{8,14},{10,12},{12... | collective-permute-start | bytes 417800 | tf_op jit(solution)/shard_map/ppermute | solution.py:52
  131.9 2.0 %collective-permute-start.30 = (bf16[1088,256]{1,0:T(8,128)(2,1)S(1)}, bf16[1088,256]{1,0:T(8,128)(2,1)S(1)}, u32[]{:S(2)}, u32[]{:S(2)}) collective-permute-start(bf16[1088,256]{1,0:T(8,128)(2,1)S(1)} %pad_maximum_fusion.own_ref), channel_id=1, source_target_pairs={{0,1},{1,0},{2,3},{3,2},{4,5},{5,4},{6,7},{7,6},{8,9},{9,8},{10,11... | collective-permute-start | bytes 1671176 | tf_op jit(solution)/shard_map/ppermute | solution.py:52
  134.4 5.4 %collective-permute-start.31 = (bf16[64,256]{1,0:T(8,128)(2,1)S(1)}, bf16[64,256]{1,0:T(8,128)(2,1)S(1)}, u32[]{:S(2)}, u32[]{:S(2)}) collective-permute-start(bf16[64,256]{1,0:T(8,128)(2,1)S(1)} %get-tuple-element.107), channel_id=1, source_target_pairs={{0,8},{8,0},{16,24},{24,16},{1,9},{9,1},{17,25},{25,17},{2,10},{10... | collective-permute-start | bytes 98312 | tf_op jit(solution)/shard_map/ppermute | solution.py:52
  136.5 3.9 %collective-permute-start.32 = (bf16[64,256]{1,0:T(8,128)(2,1)S(1)}, bf16[64,256]{1,0:T(8,128)(2,1)S(1)}, u32[]{:S(2)}, u32[]{:S(2)}) collective-permute-start(bf16[64,256]{1,0:T(8,128)(2,1)S(1)} %get-tuple-element.108), channel_id=1, source_target_pairs={{0,24},{8,16},{16,8},{24,0},{1,25},{9,17},{17,9},{25,1},{2,26},{10... | collective-permute-start | bytes 98312 | tf_op jit(solution)/shard_map/ppermute | solution.py:52
  138.0 5.4 %collective-permute-start.33 = (bf16[64,256]{1,0:T(8,128)(2,1)S(1)}, bf16[64,256]{1,0:T(8,128)(2,1)S(1)}, u32[]{:S(2)}, u32[]{:S(2)}) collective-permute-start(bf16[64,256]{1,0:T(8,128)(2,1)S(1)} %get-tuple-element.109), channel_id=1, source_target_pairs={{0,16},{8,24},{16,0},{24,8},{1,17},{9,25},{17,1},{25,9},{2,18},{10... | collective-permute-start | bytes 98312 | tf_op jit(solution)/shard_map/ppermute | solution.py:52

commit v3 on v2

--- a/solution.py
+++ b/solution.py
@@ -167,10 +167,13 @@
     refs[-1][...] = total.astype(refs[-1].dtype)
 
 
-def weights_kernel(x_ref, dy_ref, hid_ref, dgu_ref, gg_ref, gu_ref, gd_ref):
-    f = hid_ref.shape[0]
+def weights_kernel(x_ref, dgu_ref, gg_ref, gu_ref):
+    f = gg_ref.shape[0]
     gg_ref[...] = nn(dgu_ref[:f], x_ref[...]).astype(BF)
     gu_ref[...] = nn(dgu_ref[f:], x_ref[...]).astype(BF)
+
+
+def down_kernel(hid_ref, dy_ref, gd_ref):
     gd_ref[...] = nn(hid_ref[...], dy_ref[...]).astype(BF)
 
 
@@ -324,16 +327,8 @@
     (hi1,) = call(sum_kernel, [(half, ch)], 0, (hi1, via3))
     out1 = shift(hi1, "y", 4, 1)
     parts = (in1, in3, out1, out3)
-    gate_t, up_t, grad_down = call(
-        weights_kernel,
-        [(f, d)] * 3,
-        0,
-        (xin, dyin, hidden, dgu),
-        flops=6 * total * d * f,
-        hbm_outs=(0, 1, 2),
-        limit=24,
-    )
-    parts, mix, gate_t, up_t, grad_down = lax.optimization_barrier((parts, mix, gate_t, up_t, grad_down))
+    gate_t, up_t = call(weights_kernel, [(f, d)] * 2, 0, (xin, dgu), flops=4 * total * d * f, hbm_outs=(0, 1), limit=24)
+    parts, mix, gate_t, up_t = lax.optimization_barrier((parts, mix, gate_t, up_t))
     (summed,) = call(halves_kernel, [(total, ch)], 0, (keep, *parts))
     back = lax.all_to_all(summed.reshape(n_exp, cap, ch), SP, 0, 0, tiled=True)
     dh, one, two = call(
@@ -341,6 +336,9 @@
     )
     swap = [(z * 8 + y * 2 + c, (y * 2 + c) * 8 + z) for z in range(8) for y in range(4) for c in range(2)]
     turned = lax.ppermute(dh, ("z", "y", "c"), swap)
+    (grad_down,) = call(
+        down_kernel, [(f, d)], 0, (hidden, dyin), flops=2 * total * d * f, hbm_outs=(0,), limit=12
+    )
     one, two = edges(one, two)
     (stack,) = call(stack_kernel, [(2 * tok + 16, ch)], 0, (turned, dh, one, two))
     own, part = over_tp(stack)

time: 144 us -> 144 us (level)
    pallas_call x15 -> x16, Pallas kernels: 16.2 us -> 17.5 us  [call(): pl.pallas_call(body, out_shape=outs, in_specs=[SMEM if i < n_smem else AN...]
  transfers between devices with their start and end apart: 34 -> 34, of which waited for: 20 -> 19; matrix products, arithmetic and copies ran while one was open for 0% -> 0% of each run, Pallas kernels for 6% -> 7%
where the time goes in v3:
time: 144 us
  waiting for transfers between devices  49.6 us (34%)
  blocking collectives  43.7 us (30%)
  starting transfers between devices  32.2 us (22%)
  Pallas kernels  17.5 us (12%)
    all_to_all x1, blocking collectives, local(): recv = lax.all_to_all(send, SP, 0, 0, tiled=True)  28.3 us
    ppermute x28, waiting for transfers between devices, shift(): return lax.ppermute(x, axis, [(i, i ^ k) for i in range(n)])  25.1 us
    ppermute x28, starting transfers between devices, shift(): return lax.ppermute(x, axis, [(i, i ^ k) for i in range(n)])  24.9 us
    ppermute x3, waiting for transfers between devices, widen(): lax.ppermute(x, 'z', [(i, i ^ bit) for i in range(8)])  21.5 us
    pallas_call x16, Pallas kernels, call(): pl.pallas_call(body, out_shape=outs, in_specs=[SMEM if i < n_smem else AN...  17.5 us
    all_to_all x1, blocking collectives, local(): back = lax.all_to_all(summed.reshape(n_exp, cap, ch), SP, 0, 0, tiled=True)  15.4 us
    ppermute x1, waiting for transfers between devices, edges(): lax.ppermute(two, SP, [(i, i + 1 if i % 2 else i - 1) for i in range(1, n...  3.03 us
  transfers between devices with their start and end apart: 34, of which 19 were waited for; matrix products, arithmetic and copies ran while one was open for 0% of the time, Pallas kernels for 7%

profile of v3, /device:TPU:2, one launch (start us, length us, event | category | flops | bytes accessed | tf_op | source)
XLA Modules:
  0.0 144.0 jit_solution(5052300595896716149)
XLA Ops:
  0.6 1.4 shard_map.180
  2.0 28.3 %all_to_all.10 = bf16[32,32,256]{2,1,0:T(8,128)(2,1)S(1)} all-to-all(bf16[32,32,256]{2,1,0:T(8,128)(2,1)S(1)} %get-tuple-element.61), channel_id=1, replica_groups=mesh['z'=8,'x'=4,'y'=4,'c'=2] {'z','x'}, dimensions={0} | all-to-all | bytes 1048576 | tf_op jit(solution)/shard_map/all_to_all | solution.py:279
  30.3 3.1 %collective-permute-start.3 = (bf16[512,256]{1,0:T(8,128)(2,1)S(1)}, bf16[512,256]{1,0:T(8,128)(2,1)S(1)}, u32[]{:S(2)}, u32[]{:S(2)}) collective-permute-start(bf16[512,256]{1,0:T(8,128)(2,1)S(1)} %bitcast.30), channel_id=1, source_target_pairs={{0,6},{2,4},{4,2},{6,0},{1,7},{3,5},{5,3},{7,1},{8,14},{10,12},{12... | collective-permute-start | bytes 786440 | tf_op jit(solution)/shard_map/ppermute | solution.py:52
  33.4 0.1 collective-permute-start.4
  33.6 1.1 collective-permute-start.11
  34.6 0.8 collective-permute-start.2
  35.5 2.3 %shard_map.181 = (bf16[704,2048]{1,0:T(8,128)(2,1)S(1)}, bf16[352,2048]{1,0:T(8,128)(2,1)S(1)}) custom-call(bf16[352,2048]{1,0:T(8,128)(2,1)} %bitcast.34, bf16[352,2048]{1,0:T(8,128)(2,1)} %bitcast.35, bf16[352,2048]{1,0:T(8,128)(2,1)} %bitcast.36), custom_call_target="tpu_custom_call" | custom-call | tf_op jit(solution)/shard_map/pallas_call | solution.py:28
  37.7 3.1 %collective-permute-done.3.refs_12_ = bf16[512,256]{1,0:T(8,128)(2,1)S(1)} collective-permute-done((bf16[512,256]{1,0:T(8,128)(2,1)S(1)}, bf16[512,256]{1,0:T(8,128)(2,1)S(1)}, u32[]{:S(2)}, u32[]{:S(2)}) %collective-permute-start.3) | collective-permute-done | bytes 262176 | tf_op jit(solution)/shard_map/ppermute | solution.py:52
  40.8 1.8 %collective-permute-done.4.refs_5_ = bf16[512,256]{1,0:T(8,128)(2,1)S(1)} collective-permute-done((bf16[512,256]{1,0:T(8,128)(2,1)S(1)}, bf16[512,256]{1,0:T(8,128)(2,1)S(1)}, u32[]{:S(2)}, u32[]{:S(2)}) %collective-permute-start.4) | collective-permute-done | bytes 262176 | tf_op jit(solution)/shard_map/ppermute | solution.py:52
  42.6 1.2 collective-permute-start.8
  43.8 0.2 collective-permute-done.11.refs_13_
  44.1 0.4 collective-permute-start.7
  44.4 1.1 collective-permute-done.2.refs_4_
  45.5 0.5 collective-permute-start.6
  46.0 0.1 collective-permute-start.13
  46.1 4.7 %collective-permute-done.8.refs_9_ = bf16[512,256]{1,0:T(8,128)(2,1)S(1)} collective-permute-done((bf16[512,256]{1,0:T(8,128)(2,1)S(1)}, bf16[512,256]{1,0:T(8,128)(2,1)S(1)}, u32[]{:S(2)}, u32[]{:S(2)}) %collective-permute-start.8) | collective-permute-done | bytes 262176 | tf_op jit(solution)/shard_map/ppermute | solution.py:52
  50.8 1.5 %collective-permute-done.7.refs_8_ = bf16[512,256]{1,0:T(8,128)(2,1)S(1)} collective-permute-done((bf16[512,256]{1,0:T(8,128)(2,1)S(1)}, bf16[512,256]{1,0:T(8,128)(2,1)S(1)}, u32[]{:S(2)}, u32[]{:S(2)}) %collective-permute-start.7) | collective-permute-done | bytes 262176 | tf_op jit(solution)/shard_map/ppermute | solution.py:52
  52.3 0.5 collective-permute-start.9
  52.8 1.0 collective-permute-done.10.refs_11_
  53.8 0.4 collective-permute-done.9.refs_10_
  54.2 4.1 %shard_map.182 = (bf16[4,512,256]{2,1,0:T(8,128)(2,1)S(1)}, bf16[512,2048]{1,0:T(8,128)(2,1)S(1)}, bf16[512,2048]{1,0:T(8,128)(2,1)S(1)}, bf16[352,512]{1,0:T(8,...) custom-call(s32[1]{0:T(128)} %bitcast.y_ref, s32[1]{0:T(128)} %bitcast.1.c_ref, ...), custom_call_target="tpu_custom_call" | custom-call | flops 2952790016 | tf_op jit(solution)/shard_map/pallas_call | solution.py:28
  58.3 0.4 collective-permute-start.14
  58.7 0.9 shard_map.187
  59.6 1.7 %collective-permute-start.21 = (bf16[128,256]{1,0:T(8,128)(2,1)S(1)}, bf16[128,256]{1,0:T(8,128)(2,1)S(1)}, u32[]{:S(2)}, u32[]{:S(2)}) collective-permute-start(bf16[128,256]{1,0:T(8,128)(2,1)S(1)} %shard_map.187), channel_id=1, source_target_pairs={{0,128},{32,160},{64,192},{96,224},{128,0},{160,32},{192,64},{224,... | collective-permute-start | bytes 196616 | tf_op jit(solution)/shard_map/ppermute | solution.py:256
  61.3 7.6 %collective-permute-done.21 = bf16[128,256]{1,0:T(8,128)(2,1)S(1)} collective-permute-done((bf16[128,256]{1,0:T(8,128)(2,1)S(1)}, bf16[128,256]{1,0:T(8,128)(2,1)S(1)}, u32[]{:S(2)}, u32[]{:S(2)}) %collective-permute-start.21) | collective-permute-done | bytes 65568 | tf_op jit(solution)/shard_map/ppermute | solution.py:256
  68.8 0.1 collective-permute-start.22
  68.9 8.8 %collective-permute-done.22 = bf16[256,256]{1,0:T(8,128)(2,1)S(1)} collective-permute-done((bf16[256,256]{1,0:T(8,128)(2,1)S(1)}, bf16[256,256]{1,0:T(8,128)(2,1)S(1)}, u32[]{:S(2)}, u32[]{:S(2)}) %collective-permute-start.22) | collective-permute-done | bytes 131104 | tf_op jit(solution)/shard_map/ppermute | solution.py:256
  77.8 0.1 collective-permute-start.23
  77.9 1.0 shard_map.183.mine_ref
  78.9 0.2 shard_map.184
  79.2 0.4 collective-permute-start.19
  79.6 1.1 collective-permute-start.17
  80.7 5.1 %collective-permute-done.23 = bf16[512,256]{1,0:T(8,128)(2,1)S(1)} collective-permute-done((bf16[512,256]{1,0:T(8,128)(2,1)S(1)}, bf16[512,256]{1,0:T(8,128)(2,1)S(1)}, u32[]{:S(2)}, u32[]{:S(2)}) %collective-permute-start.23) | collective-permute-done | bytes 262176 | tf_op jit(solution)/shard_map/ppermute | solution.py:256
  85.8 0.4 collective-permute-start.15
  86.2 0.5 collective-permute-start.16
  86.8 2.8 %collective-permute-start.20 = (bf16[256,256]{1,0:T(8,128)(2,1)S(1)}, bf16[256,256]{1,0:T(8,128)(2,1)S(1)}, u32[]{:S(2)}, u32[]{:S(2)}) collective-permute-start(bf16[256,256]{1,0:T(8,128)(2,1)S(1)} %shard_map.186), channel_id=1, source_target_pairs={{0,6},{2,4},{4,2},{6,0},{1,7},{3,5},{5,3},{7,1},{8,14},{10,12},{12... | collective-permute-start | bytes 393224 | tf_op jit(solution)/shard_map/ppermute | solution.py:52
  89.6 0.6 collective-permute-start.18
  90.2 3.0 %shard_map.188 = (bf16[352,2048]{1,0:T(8,128)(2,1)}, bf16[352,2048]{1,0:T(8,128)(2,1)}) custom-call(bf16[512,2048]{1,0:T(8,128)(2,1)S(1)} %get-tuple-element.82.x_ref, bf16[704,512]{1,0:T(8,128)(2,1)S(1)} %get-tuple-element.83.dgu_ref), custom_call_target="tpu_custom_call" | custom-call | flops 1476395008 | tf_op jit(solution)/shard_map/pallas_call | solution.py:28
  93.2 1.0 collective-permute-done.20.out3_ref
  94.2 0.5 collective-permute-done.18.out1_ref
  94.7 0.1 shard_map.190
  94.8 15.4 %all_to_all.11 = bf16[32,16,256]{2,1,0:T(8,128)(2,1)S(1)} all-to-all(bf16[32,16,256]{2,1,0:T(8,128)(2,1)S(1)} %bitcast.25), channel_id=1, replica_groups=mesh['z'=8,'x'=4,'y'=4,'c'=2] {'z','x'}, dimensions={0} | all-to-all | bytes 524288 | tf_op jit(solution)/shard_map/all_to_all | solution.py:333
  110.2 0.2 shard_map.191
  110.4 0.7 collective-permute-start.24
  111.1 2.3 %collective-permute-start.25 = (bf16[2,256]{1,0:T(2,128)(2,1)S(1)}, bf16[2,256]{1,0:T(2,128)(2,1)S(1)}, u32[]{:S(2)}, u32[]{:S(2)}) collective-permute-start(bf16[2,256]{1,0:T(2,128)(2,1)S(1)} %get-tuple-element.99), channel_id=1, source_target_pairs={{0,8},{8,0},{16,24},{24,16},{32,40},{40,32},{48,56},{56,48},{64,72... | collective-permute-start | bytes 3080 | tf_op jit(solution)/shard_map/ppermute | solution.py:250
  113.4 2.4 %collective-permute-start.26 = (bf16[2,256]{1,0:T(2,128)(2,1)S(1)}, bf16[2,256]{1,0:T(2,128)(2,1)S(1)}, u32[]{:S(2)}, u32[]{:S(2)}) collective-permute-start(bf16[2,256]{1,0:T(2,128)(2,1)S(1)} %get-tuple-element.100), channel_id=1, source_target_pairs={{8,16},{16,8},{24,32},{32,24},{40,48},{48,40},{56,64},{64,56},{72,... | collective-permute-start | bytes 3080 | tf_op jit(solution)/shard_map/ppermute | solution.py:251
  115.8 3.0 %collective-permute-done.26.high_ref.bh_ref = bf16[2,256]{1,0:T(2,128)(2,1)S(1)} collective-permute-done((bf16[2,256]{1,0:T(2,128)(2,1)S(1)}, bf16[2,256]{1,0:T(2,128)(2,1)S(1)}, u32[]{:S(2)}, u32[]{:S(2)}) %collective-permute-start.26) | collective-permute-done | bytes 1056 | tf_op jit(solution)/shard_map/ppermute | solution.py:251
  118.9 3.7 %collective-permute-start.27 = (bf16[272,256]{1,0:T(8,128)(2,1)S(1)}, bf16[272,256]{1,0:T(8,128)(2,1)S(1)}, u32[]{:S(2)}, u32[]{:S(2)}) collective-permute-start(bf16[272,256]{1,0:T(8,128)(2,1)S(1)} %shard_map.192), channel_id=1, source_target_pairs={{0,2},{2,0},{4,6},{6,4},{1,3},{3,1},{5,7},{7,5},{8,10},{10,8},{12,... | collective-permute-start | bytes 417800 | tf_op jit(solution)/shard_map/ppermute | solution.py:52
  122.6 2.4 %collective-permute-start.28 = (bf16[272,256]{1,0:T(8,128)(2,1)S(1)}, bf16[272,256]{1,0:T(8,128)(2,1)S(1)}, u32[]{:S(2)}, u32[]{:S(2)}) collective-permute-start(bf16[272,256]{1,0:T(8,128)(2,1)S(1)} %shard_map.192), channel_id=1, source_target_pairs={{0,4},{2,6},{4,0},{6,2},{1,5},{3,7},{5,1},{7,3},{8,12},{10,14},{12... | collective-permute-start | bytes 417800 | tf_op jit(solution)/shard_map/ppermute | solution.py:52
  125.0 0.5 collective-permute-start.29
  125.5 1.4 collective-permute-done.27
  126.9 3.4 %collective-permute-done.28 = bf16[272,256]{1,0:T(8,128)(2,1)S(1)} collective-permute-done((bf16[272,256]{1,0:T(8,128)(2,1)S(1)}, bf16[272,256]{1,0:T(8,128)(2,1)S(1)}, u32[]{:S(2)}, u32[]{:S(2)}) %collective-permute-start.28) | collective-permute-done | bytes 139296 | tf_op jit(solution)/shard_map/ppermute | solution.py:52
  130.3 1.6 %collective-permute-done.29 = bf16[272,256]{1,0:T(8,128)(2,1)S(1)} collective-permute-done((bf16[272,256]{1,0:T(8,128)(2,1)S(1)}, bf16[272,256]{1,0:T(8,128)(2,1)S(1)}, u32[]{:S(2)}, u32[]{:S(2)}) %collective-permute-start.29) | collective-permute-done | bytes 139296 | tf_op jit(solution)/shard_map/ppermute | solution.py:52
  131.9 0.1 collective-permute-start.30
  132.0 1.9 %collective-permute-done.30.part_ref = bf16[1088,256]{1,0:T(8,128)(2,1)S(1)} collective-permute-done((bf16[1088,256]{1,0:T(8,128)(2,1)S(1)}, bf16[1088,256]{1,0:T(8,128)(2,1)S(1)}, u32[]{:S(2)}, u32[]{:S(2)}) %collective-permute-start.30) | collective-permute-done | bytes 557088 | tf_op jit(solution)/shard_map/ppermute | solution.py:52
  134.0 0.4 shard_map.193
  134.4 2.0 %collective-permute-start.31 = (bf16[64,256]{1,0:T(8,128)(2,1)S(1)}, bf16[64,256]{1,0:T(8,128)(2,1)S(1)}, u32[]{:S(2)}, u32[]{:S(2)}) collective-permute-start(bf16[64,256]{1,0:T(8,128)(2,1)S(1)} %get-tuple-element.103), channel_id=1, source_target_pairs={{0,8},{8,0},{16,24},{24,16},{1,9},{9,1},{17,25},{25,17},{2,10},{10... | collective-permute-start | bytes 98312 | tf_op jit(solution)/shard_map/ppermute | solution.py:52
  136.3 1.6 %collective-permute-start.32 = (bf16[64,256]{1,0:T(8,128)(2,1)S(1)}, bf16[64,256]{1,0:T(8,128)(2,1)S(1)}, u32[]{:S(2)}, u32[]{:S(2)}) collective-permute-start(bf16[64,256]{1,0:T(8,128)(2,1)S(1)} %get-tuple-element.104), channel_id=1, source_target_pairs={{0,24},{8,16},{16,8},{24,0},{1,25},{9,17},{17,9},{25,1},{2,26},{10... | collective-permute-start | bytes 98312 | tf_op jit(solution)/shard_map/ppermute | solution.py:52
  137.9 0.6 collective-permute-start.33
  138.6 0.0 copy-start.6
  138.6 2.0 %shard_map.189 = bf16[352,2048]{1,0:T(8,128)(2,1)} custom-call(bf16[352,512]{1,0:T(8,128)(2,1)S(1)} %get-tuple-element.88.hid_ref, bf16[512,2048]{1,0:T(8,128)(2,1)S(1)} %get-tuple-element.89.dy_ref), custom_call_target="tpu_custom_call" | custom-call | flops 738197504 | tf_op jit(solution)/shard_map/pallas_call | solution.py:28
  140.6 1.0 shard_map.195
  141.7 1.7 %collective-permute-done.33.refs_3_ = bf16[64,256]{1,0:T(8,128)(2,1)S(1)} collective-permute-done((bf16[64,256]{1,0:T(8,128)(2,1)S(1)}, bf16[64,256]{1,0:T(8,128)(2,1)S(1)}, u32[]{:S(2)}, u32[]{:S(2)}) %collective-permute-start.33) | collective-permute-done | bytes 32800 | tf_op jit(solution)/shard_map/ppermute | solution.py:52
  143.3 0.6 shard_map.194
  (41 shorter events, 0.3 us)
Async XLA Ops:
  30.3 10.5 %collective-permute-start.3 = (bf16[512,256]{1,0:T(8,128)(2,1)S(1)}, bf16[512,256]{1,0:T(8,128)(2,1)S(1)}, u32[]{:S(2)}, u32[]{:S(2)}) collective-permute-start(bf16[512,256]{1,0:T(8,128)(2,1)S(1)} %bitcast.30), channel_id=1, source_target_pairs={{0,6},{2,4},{4,2},{6,0},{1,7},{3,5},{5,3},{7,1},{8,14},{10,12},{12... | collective-permute-start | bytes 786440 | tf_op jit(solution)/shard_map/ppermute | solution.py:52
  33.4 9.2 %collective-permute-start.4 = (bf16[512,256]{1,0:T(8,128)(2,1)S(1)}, bf16[512,256]{1,0:T(8,128)(2,1)S(1)}, u32[]{:S(2)}, u32[]{:S(2)}) collective-permute-start(bf16[512,256]{1,0:T(8,128)(2,1)S(1)} %bitcast.26), channel_id=1, source_target_pairs={{0,2},{2,0},{4,6},{6,4},{1,3},{3,1},{5,7},{7,5},{8,10},{10,8},{12,... | collective-permute-start | bytes 786440 | tf_op jit(solution)/shard_map/ppermute | solution.py:52
  33.6 10.5 %collective-permute-start.11 = (bf16[512,256]{1,0:T(8,128)(2,1)S(1)}, bf16[512,256]{1,0:T(8,128)(2,1)S(1)}, u32[]{:S(2)}, u32[]{:S(2)}) collective-permute-start(bf16[512,256]{1,0:T(8,128)(2,1)S(1)} %bitcast.27), channel_id=1, source_target_pairs={{0,6},{2,4},{4,2},{6,0},{1,7},{3,5},{5,3},{7,1},{8,14},{10,12},{12... | collective-permute-start | bytes 786440 | tf_op jit(solution)/shard_map/ppermute | solution.py:52
  34.6 10.9 %collective-permute-start.2 = (bf16[512,256]{1,0:T(8,128)(2,1)S(1)}, bf16[512,256]{1,0:T(8,128)(2,1)S(1)}, u32[]{:S(2)}, u32[]{:S(2)}) collective-permute-start(bf16[512,256]{1,0:T(8,128)(2,1)S(1)} %bitcast.31), channel_id=1, source_target_pairs={{0,2},{2,0},{4,6},{6,4},{1,3},{3,1},{5,7},{7,5},{8,10},{10,8},{12,... | collective-permute-start | bytes 786440 | tf_op jit(solution)/shard_map/ppermute | solution.py:52
  35.4 10.1 %collective-permute-start = (bf16[512,256]{1,0:T(8,128)(2,1)S(1)}, bf16[512,256]{1,0:T(8,128)(2,1)S(1)}, u32[]{:S(2)}, u32[]{:S(2)}) collective-permute-start(bf16[512,256]{1,0:T(8,128)(2,1)S(1)} %bitcast.32), channel_id=1, source_target_pairs={{0,1},{1,0},{2,3},{3,2},{4,5},{5,4},{6,7},{7,6},{8,9},{9,8},{10,11... | collective-permute-start | bytes 786440 | tf_op jit(solution)/shard_map/ppermute | solution.py:52
  40.8 5.2 %collective-permute-start.1 = (bf16[512,256]{1,0:T(8,128)(2,1)S(1)}, bf16[512,256]{1,0:T(8,128)(2,1)S(1)}, u32[]{:S(2)}, u32[]{:S(2)}) collective-permute-start(bf16[512,256]{1,0:T(8,128)(2,1)S(1)} %bitcast.28), channel_id=1, source_target_pairs={{0,1},{1,0},{2,3},{3,2},{4,5},{5,4},{6,7},{7,6},{8,9},{9,8},{10,11... | collective-permute-start | bytes 786440 | tf_op jit(solution)/shard_map/ppermute | solution.py:52
  42.6 8.2 %collective-permute-start.8 = (bf16[512,256]{1,0:T(8,128)(2,1)S(1)}, bf16[512,256]{1,0:T(8,128)(2,1)S(1)}, u32[]{:S(2)}, u32[]{:S(2)}) collective-permute-start(bf16[512,256]{1,0:T(8,128)(2,1)S(1)} %collective-permute-done.4.refs_5_), channel_id=1, source_target_pairs={{0,6},{2,4},{4,2},{6,0},{1,7},{3,5},{5,3},{7,1},{8,14},{10,12},{12... | collective-permute-start | bytes 786440 | tf_op jit(solution)/shard_map/ppermute | solution.py:52
  44.1 8.2 %collective-permute-start.7 = (bf16[512,256]{1,0:T(8,128)(2,1)S(1)}, bf16[512,256]{1,0:T(8,128)(2,1)S(1)}, u32[]{:S(2)}, u32[]{:S(2)}) collective-permute-start(bf16[512,256]{1,0:T(8,128)(2,1)S(1)} %collective-permute-done.3.refs_12_), channel_id=1, source_target_pairs={{0,2},{2,0},{4,6},{6,4},{1,3},{3,1},{5,7},{7,5},{8,10},{10,8},{12,... | collective-permute-start | bytes 786440 | tf_op jit(solution)/shard_map/ppermute | solution.py:52
  45.5 6.7 %collective-permute-start.12 = (bf16[512,256]{1,0:T(8,128)(2,1)S(1)}, bf16[512,256]{1,0:T(8,128)(2,1)S(1)}, u32[]{:S(2)}, u32[]{:S(2)}) collective-permute-start(bf16[512,256]{1,0:T(8,128)(2,1)S(1)} %collective-permute-done.3.refs_12_), channel_id=1, source_target_pairs={{0,1},{1,0},{2,3},{3,2},{4,5},{5,4},{6,7},{7,6},{8,9},{9,8},{10,11... | collective-permute-start | bytes 786440 | tf_op jit(solution)/shard_map/ppermute | solution.py:52
  45.5 7.3 %collective-permute-start.6 = (bf16[512,256]{1,0:T(8,128)(2,1)S(1)}, bf16[512,256]{1,0:T(8,128)(2,1)S(1)}, u32[]{:S(2)}, u32[]{:S(2)}) collective-permute-start(bf16[512,256]{1,0:T(8,128)(2,1)S(1)} %collective-permute-done.4.refs_5_), channel_id=1, source_target_pairs={{0,1},{1,0},{2,3},{3,2},{4,5},{5,4},{6,7},{7,6},{8,9},{9,8},{10,11... | collective-permute-start | bytes 786440 | tf_op jit(solution)/shard_map/ppermute | solution.py:52
  46.0 6.7 %collective-permute-start.13 = (bf16[512,256]{1,0:T(8,128)(2,1)S(1)}, bf16[512,256]{1,0:T(8,128)(2,1)S(1)}, u32[]{:S(2)}, u32[]{:S(2)}) collective-permute-start(bf16[512,256]{1,0:T(8,128)(2,1)S(1)} %collective-permute-done.11.refs_13_), channel_id=1, source_target_pairs={{0,1},{1,0},{2,3},{3,2},{4,5},{5,4},{6,7},{7,6},{8,9},{9,8},{10,11... | collective-permute-start | bytes 786440 | tf_op jit(solution)/shard_map/ppermute | solution.py:52
  50.8 2.0 %collective-permute-start.5 = (bf16[512,256]{1,0:T(8,128)(2,1)S(1)}, bf16[512,256]{1,0:T(8,128)(2,1)S(1)}, u32[]{:S(2)}, u32[]{:S(2)}) collective-permute-start(bf16[512,256]{1,0:T(8,128)(2,1)S(1)} %collective-permute-done.2.refs_4_), channel_id=1, source_target_pairs={{0,1},{1,0},{2,3},{3,2},{4,5},{5,4},{6,7},{7,6},{8,9},{9,8},{10,11... | collective-permute-start | bytes 786440 | tf_op jit(solution)/shard_map/ppermute | solution.py:52
  52.3 1.5 %collective-permute-start.10 = (bf16[512,256]{1,0:T(8,128)(2,1)S(1)}, bf16[512,256]{1,0:T(8,128)(2,1)S(1)}, u32[]{:S(2)}, u32[]{:S(2)}) collective-permute-start(bf16[512,256]{1,0:T(8,128)(2,1)S(1)} %collective-permute-done.8.refs_9_), channel_id=1, source_target_pairs={{0,1},{1,0},{2,3},{3,2},{4,5},{5,4},{6,7},{7,6},{8,9},{9,8},{10,11... | collective-permute-start | bytes 786440 | tf_op jit(solution)/shard_map/ppermute | solution.py:52
  52.3 1.9 %collective-permute-start.9 = (bf16[512,256]{1,0:T(8,128)(2,1)S(1)}, bf16[512,256]{1,0:T(8,128)(2,1)S(1)}, u32[]{:S(2)}, u32[]{:S(2)}) collective-permute-start(bf16[512,256]{1,0:T(8,128)(2,1)S(1)} %collective-permute-done.7.refs_8_), channel_id=1, source_target_pairs={{0,1},{1,0},{2,3},{3,2},{4,5},{5,4},{6,7},{7,6},{8,9},{9,8},{10,11... | collective-permute-start | bytes 786440 | tf_op jit(solution)/shard_map/ppermute | solution.py:52
  58.3 20.6 %collective-permute-start.14 = (bf16[4,512,256]{2,1,0:T(8,128)(2,1)S(1)}, bf16[4,512,256]{2,1,0:T(8,128)(2,1)S(1)}, u32[]{:S(2)}, u32[]{:S(2)}) collective-permute-start(bf16[4,512,256]{2,1,0:T(8,128)(2,1)S(1)} %get-tuple-element.73), channel_id=1, source_target_pairs={{0,1},{1,0},{2,3},{3,2},{4,5},{5,4},{6,7},{7,6},{8,9},{9,8},{10,11... | collective-permute-start | bytes 3145736 | tf_op jit(solution)/shard_map/ppermute | solution.py:52
  59.6 9.2 %collective-permute-start.21 = (bf16[128,256]{1,0:T(8,128)(2,1)S(1)}, bf16[128,256]{1,0:T(8,128)(2,1)S(1)}, u32[]{:S(2)}, u32[]{:S(2)}) collective-permute-start(bf16[128,256]{1,0:T(8,128)(2,1)S(1)} %shard_map.187), channel_id=1, source_target_pairs={{0,128},{32,160},{64,192},{96,224},{128,0},{160,32},{192,64},{224,... | collective-permute-start | bytes 196616 | tf_op jit(solution)/shard_map/ppermute | solution.py:256
  68.8 8.9 %collective-permute-start.22 = (bf16[256,256]{1,0:T(8,128)(2,1)S(1)}, bf16[256,256]{1,0:T(8,128)(2,1)S(1)}, u32[]{:S(2)}, u32[]{:S(2)}) collective-permute-start(bf16[256,256]{1,0:T(8,128)(2,1)S(1)} %pad_maximum_fusion.3), channel_id=1, source_target_pairs={{0,64},{32,96},{64,0},{96,32},{128,192},{160,224},{192,128},{224,1... | collective-permute-start | bytes 393224 | tf_op jit(solution)/shard_map/ppermute | solution.py:256
  77.8 7.9 %collective-permute-start.23 = (bf16[512,256]{1,0:T(8,128)(2,1)S(1)}, bf16[512,256]{1,0:T(8,128)(2,1)S(1)}, u32[]{:S(2)}, u32[]{:S(2)}) collective-permute-start(bf16[512,256]{1,0:T(8,128)(2,1)S(1)} %pad_maximum_fusion.2), channel_id=1, source_target_pairs={{0,32},{32,0},{64,96},{96,64},{128,160},{160,128},{192,224},{224,1... | collective-permute-start | bytes 786440 | tf_op jit(solution)/shard_map/ppermute | solution.py:256
  79.2 7.6 %collective-permute-start.19 = (bf16[256,256]{1,0:T(8,128)(2,1)S(1)}, bf16[256,256]{1,0:T(8,128)(2,1)S(1)}, u32[]{:S(2)}, u32[]{:S(2)}) collective-permute-start(bf16[256,256]{1,0:T(8,128)(2,1)S(1)} %get-tuple-element.79), channel_id=1, source_target_pairs={{0,2},{2,0},{4,6},{6,4},{1,3},{3,1},{5,7},{7,5},{8,10},{10,8},{12,... | collective-permute-start | bytes 393224 | tf_op jit(solution)/shard_map/ppermute | solution.py:52
  79.6 10.0 %collective-permute-start.17 = (bf16[256,256]{1,0:T(8,128)(2,1)S(1)}, bf16[256,256]{1,0:T(8,128)(2,1)S(1)}, u32[]{:S(2)}, u32[]{:S(2)}) collective-permute-start(bf16[256,256]{1,0:T(8,128)(2,1)S(1)} %get-tuple-element.77), channel_id=1, source_target_pairs={{0,6},{2,4},{4,2},{6,0},{1,7},{3,5},{5,3},{7,1},{8,14},{10,12},{12... | collective-permute-start | bytes 393224 | tf_op jit(solution)/shard_map/ppermute | solution.py:52
  85.8 7.4 %collective-permute-start.15 = (bf16[256,256]{1,0:T(8,128)(2,1)S(1)}, bf16[256,256]{1,0:T(8,128)(2,1)S(1)}, u32[]{:S(2)}, u32[]{:S(2)}) collective-permute-start(bf16[256,256]{1,0:T(8,128)(2,1)S(1)} %get-tuple-element.74), channel_id=1, source_target_pairs={{0,2},{2,0},{4,6},{6,4},{1,3},{3,1},{5,7},{7,5},{8,10},{10,8},{12,... | collective-permute-start | bytes 393224 | tf_op jit(solution)/shard_map/ppermute | solution.py:52
  86.2 7.0 %collective-permute-start.16 = (bf16[256,256]{1,0:T(8,128)(2,1)S(1)}, bf16[256,256]{1,0:T(8,128)(2,1)S(1)}, u32[]{:S(2)}, u32[]{:S(2)}) collective-permute-start(bf16[256,256]{1,0:T(8,128)(2,1)S(1)} %get-tuple-element.75), channel_id=1, source_target_pairs={{0,6},{2,4},{4,2},{6,0},{1,7},{3,5},{5,3},{7,1},{8,14},{10,12},{12... | collective-permute-start | bytes 393224 | tf_op jit(solution)/shard_map/ppermute | solution.py:52
  86.8 7.4 %collective-permute-start.20 = (bf16[256,256]{1,0:T(8,128)(2,1)S(1)}, bf16[256,256]{1,0:T(8,128)(2,1)S(1)}, u32[]{:S(2)}, u32[]{:S(2)}) collective-permute-start(bf16[256,256]{1,0:T(8,128)(2,1)S(1)} %shard_map.186), channel_id=1, source_target_pairs={{0,6},{2,4},{4,2},{6,0},{1,7},{3,5},{5,3},{7,1},{8,14},{10,12},{12... | collective-permute-start | bytes 393224 | tf_op jit(solution)/shard_map/ppermute | solution.py:52
  89.6 5.1 %collective-permute-start.18 = (bf16[256,256]{1,0:T(8,128)(2,1)S(1)}, bf16[256,256]{1,0:T(8,128)(2,1)S(1)}, u32[]{:S(2)}, u32[]{:S(2)}) collective-permute-start(bf16[256,256]{1,0:T(8,128)(2,1)S(1)} %shard_map.185), channel_id=1, source_target_pairs={{0,2},{2,0},{4,6},{6,4},{1,3},{3,1},{5,7},{7,5},{8,10},{10,8},{12,... | collective-permute-start | bytes 393224 | tf_op jit(solution)/shard_map/ppermute | solution.py:52
  93.2 17.0 %copy-start.1 = (bf16[128,256]{1,0:T(8,128)(2,1)S(1)}, bf16[128,256]{1,0:T(8,128)(2,1)}, u32[]{:S(2)}) copy-start(bf16[128,256]{1,0:T(8,128)(2,1)} %b_ref.2) | copy-start | bytes 196612
  93.2 17.0 %copy-start.3 = (bf16[128,256]{1,0:T(8,128)(2,1)S(1)}, bf16[128,256]{1,0:T(8,128)(2,1)}, u32[]{:S(2)}) copy-start(bf16[128,256]{1,0:T(8,128)(2,1)} %og_ref.3) | copy-start | bytes 196612
  110.4 8.4 %collective-permute-start.24 = (bf16[128,256]{1,0:T(8,128)(2,1)S(1)}, bf16[128,256]{1,0:T(8,128)(2,1)S(1)}, u32[]{:S(2)}, u32[]{:S(2)}) collective-permute-start(bf16[128,256]{1,0:T(8,128)(2,1)S(1)} %get-tuple-element.98.dh_ref), channel_id=1, source_target_pairs={{0,0},{1,32},{2,64},{3,96},{4,128},{5,160},{6,192},{7,224},{32,1},... | collective-permute-start | bytes 196616 | tf_op jit(solution)/shard_map/ppermute | solution.py:338
  111.1 4.7 %collective-permute-start.25 = (bf16[2,256]{1,0:T(2,128)(2,1)S(1)}, bf16[2,256]{1,0:T(2,128)(2,1)S(1)}, u32[]{:S(2)}, u32[]{:S(2)}) collective-permute-start(bf16[2,256]{1,0:T(2,128)(2,1)S(1)} %get-tuple-element.99), channel_id=1, source_target_pairs={{0,8},{8,0},{16,24},{24,16},{32,40},{40,32},{48,56},{56,48},{64,72... | collective-permute-start | bytes 3080 | tf_op jit(solution)/shard_map/ppermute | solution.py:250
  113.4 5.5 %collective-permute-start.26 = (bf16[2,256]{1,0:T(2,128)(2,1)S(1)}, bf16[2,256]{1,0:T(2,128)(2,1)S(1)}, u32[]{:S(2)}, u32[]{:S(2)}) collective-permute-start(bf16[2,256]{1,0:T(2,128)(2,1)S(1)} %get-tuple-element.100), channel_id=1, source_target_pairs={{8,16},{16,8},{24,32},{32,24},{40,48},{48,40},{56,64},{64,56},{72,... | collective-permute-start | bytes 3080 | tf_op jit(solution)/shard_map/ppermute | solution.py:251
  118.9 8.0 %collective-permute-start.27 = (bf16[272,256]{1,0:T(8,128)(2,1)S(1)}, bf16[272,256]{1,0:T(8,128)(2,1)S(1)}, u32[]{:S(2)}, u32[]{:S(2)}) collective-permute-start(bf16[272,256]{1,0:T(8,128)(2,1)S(1)} %shard_map.192), channel_id=1, source_target_pairs={{0,2},{2,0},{4,6},{6,4},{1,3},{3,1},{5,7},{7,5},{8,10},{10,8},{12,... | collective-permute-start | bytes 417800 | tf_op jit(solution)/shard_map/ppermute | solution.py:52
  122.6 7.7 %collective-permute-start.28 = (bf16[272,256]{1,0:T(8,128)(2,1)S(1)}, bf16[272,256]{1,0:T(8,128)(2,1)S(1)}, u32[]{:S(2)}, u32[]{:S(2)}) collective-permute-start(bf16[272,256]{1,0:T(8,128)(2,1)S(1)} %shard_map.192), channel_id=1, source_target_pairs={{0,4},{2,6},{4,0},{6,2},{1,5},{3,7},{5,1},{7,3},{8,12},{10,14},{12... | collective-permute-start | bytes 417800 | tf_op jit(solution)/shard_map/ppermute | solution.py:52
  125.0 6.8 %collective-permute-start.29 = (bf16[272,256]{1,0:T(8,128)(2,1)S(1)}, bf16[272,256]{1,0:T(8,128)(2,1)S(1)}, u32[]{:S(2)}, u32[]{:S(2)}) collective-permute-start(bf16[272,256]{1,0:T(8,128)(2,1)S(1)} %shard_map.192), channel_id=1, source_target_pairs={{0,6},{2,4},{4,2},{6,0},{1,7},{3,5},{5,3},{7,1},{8,14},{10,12},{12... | collective-permute-start | bytes 417800 | tf_op jit(solution)/shard_map/ppermute | solution.py:52
  131.9 2.0 %collective-permute-start.30 = (bf16[1088,256]{1,0:T(8,128)(2,1)S(1)}, bf16[1088,256]{1,0:T(8,128)(2,1)S(1)}, u32[]{:S(2)}, u32[]{:S(2)}) collective-permute-start(bf16[1088,256]{1,0:T(8,128)(2,1)S(1)} %pad_maximum_fusion.own_ref), channel_id=1, source_target_pairs={{0,1},{1,0},{2,3},{3,2},{4,5},{5,4},{6,7},{7,6},{8,9},{9,8},{10,11... | collective-permute-start | bytes 1671176 | tf_op jit(solution)/shard_map/ppermute | solution.py:52
  134.4 7.3 %collective-permute-start.31 = (bf16[64,256]{1,0:T(8,128)(2,1)S(1)}, bf16[64,256]{1,0:T(8,128)(2,1)S(1)}, u32[]{:S(2)}, u32[]{:S(2)}) collective-permute-start(bf16[64,256]{1,0:T(8,128)(2,1)S(1)} %get-tuple-element.103), channel_id=1, source_target_pairs={{0,8},{8,0},{16,24},{24,16},{1,9},{9,1},{17,25},{25,17},{2,10},{10... | collective-permute-start | bytes 98312 | tf_op jit(solution)/shard_map/ppermute | solution.py:52
  136.3 5.4 %collective-permute-start.32 = (bf16[64,256]{1,0:T(8,128)(2,1)S(1)}, bf16[64,256]{1,0:T(8,128)(2,1)S(1)}, u32[]{:S(2)}, u32[]{:S(2)}) collective-permute-start(bf16[64,256]{1,0:T(8,128)(2,1)S(1)} %get-tuple-element.104), channel_id=1, source_target_pairs={{0,24},{8,16},{16,8},{24,0},{1,25},{9,17},{17,9},{25,1},{2,26},{10... | collective-permute-start | bytes 98312 | tf_op jit(solution)/shard_map/ppermute | solution.py:52
  137.9 5.4 %collective-permute-start.33 = (bf16[64,256]{1,0:T(8,128)(2,1)S(1)}, bf16[64,256]{1,0:T(8,128)(2,1)S(1)}, u32[]{:S(2)}, u32[]{:S(2)}) collective-permute-start(bf16[64,256]{1,0:T(8,128)(2,1)S(1)} %get-tuple-element.105), channel_id=1, source_target_pairs={{0,16},{8,24},{16,0},{24,8},{1,17},{9,25},{17,1},{25,9},{2,18},{10... | collective-permute-start | bytes 98312 | tf_op jit(solution)/shard_map/ppermute | solution.py:52
  138.5 2.1 %copy-start = (bf16[2048,256]{1,0:T(8,128)(2,1)S(1)}, bf16[2048,256]{1,0:T(8,128)(2,1)}, u32[]{:S(2)}) copy-start(bf16[2048,256]{1,0:T(8,128)(2,1)} %w_ref.1) | copy-start | bytes 3145732
  138.5 2.1 %copy-start.2 = (bf16[128,256]{1,0:T(8,128)(2,1)S(1)}, bf16[128,256]{1,0:T(8,128)(2,1)}, u32[]{:S(2)}) copy-start(bf16[128,256]{1,0:T(8,128)(2,1)} %co_ref.1) | copy-start | bytes 196612
  138.5 2.1 %copy-start.4 = (bf16[128,256]{1,0:T(8,128)(2,1)S(1)}, bf16[128,256]{1,0:T(8,128)(2,1)}, u32[]{:S(2)}) copy-start(bf16[128,256]{1,0:T(8,128)(2,1)} %v_ref.1) | copy-start | bytes 196612
  138.5 2.1 %copy-start.5 = (bf16[128,256]{1,0:T(8,128)(2,1)S(1)}, bf16[128,256]{1,0:T(8,128)(2,1)}, u32[]{:S(2)}) copy-start(bf16[128,256]{1,0:T(8,128)(2,1)} %g_ref.1) | copy-start | bytes 196612
  138.6 2.1 %copy-start.6 = (f32[3,256]{1,0:T(4,128)S(1)}, f32[3,256]{1,0:T(4,128)}, u32[]{:S(2)}) copy-start(f32[3,256]{1,0:T(4,128)} %t_ref.1) | copy-start | bytes 9220
